TPU v7x, 256 devices: a whole 4x4x8 slice. The times are simulated.
256 devices in a mesh: sp: 128 (over z, y, x), tp: 2 (over core).
Axes of the slice: x: 4, y: 4, z: 8, core: 2. Of those that a mesh axis runs over, the one named last changes fastest.
Arguments:
- conv_value: bfloat16 [65536, 1536], P('sp', 'tp'), may hold values from -6 to 6
- conv_gate: bfloat16 [65536, 1536], P('sp', 'tp'), may hold values from -8 to 8
- conv_out: bfloat16 [65536, 1536], P('sp', 'tp'), may hold values from -40 to 40
- conv_taps: bfloat16 [31, 1536], P(None, 'tp'), may hold values from -1 to 1
- norm_gain: float32 [1536], P('tp'), may hold values from 0.1 to 1.9
- norm_shift: float32 [1536], P('tp'), may hold values from -3 to 3
- proj_weight: bfloat16 [2048, 1536], P(None, 'tp'), may hold values from -0.15625 to 0.15625
- out_grad: bfloat16 [65536, 2048], P('sp'), may hold values from -24 to 24
Outputs:
- grad_value: bfloat16 [65536, 1536], P('sp', 'tp')
- grad_gate: bfloat16 [65536, 1536], P('sp', 'tp')
- grad_taps: float32 [31, 1536], P(None, 'tp')
- grad_gain: float32 [1536], P('tp')
- grad_shift: float32 [1536], P('tp')
- grad_proj: float32 [2048, 1536], P('sp', 'tp')
All inputs are finite; a program needn't handle non-finite values.
Results may differ from a plain program's by a relative error of at most 0.005.
Values may be sent and summed in bfloat16 or wider, within the bound.
No kernel may reach another device: no remote copies, remote signals or barrier semaphores. Data moves between devices by JAX's collectives and lax.ppermute only.
A program may use at most 64 MiB of HBM per device.

v0:
```python
import functools

import jax
import jax.numpy as jnp
from jax import lax
from jax.sharding import Mesh
from jax.sharding import PartitionSpec as P

SP = ("sp_0", "sp_1", "sp_2")


norm_eps = 1e-05


def own_rows_2(running, axes):
    for axis in axes:
        running = lax.psum_scatter(running, axis, scatter_dimension=0, tiled=True)
    return running


def shifted_2(block, axis, distance):
    devices = range(lax.axis_size(axis))
    route = [(i - distance, i) for i in devices if i - distance in devices]
    return lax.ppermute(block, axis, route)


def one_axis_at_a_time(array, axes):
    return functools.reduce(lax.psum, axes, array)


def project_rows(out_grad, active):
    return own_rows_2(
        lax.dot_general(
            out_grad, active, (((0,), (0,)), ((), ())), preferred_element_type=jnp.float32
        ),
        SP,
    )


def local(conv_value, conv_gate, conv_out, conv_taps, norm_gain, norm_shift, proj_weight, out_grad):
    seq_rows, chan_local = conv_value.shape
    tap_reach = conv_taps.shape[0] - 1
    chan_total = chan_local * lax.axis_size("tp")
    height = conv_out.astype(jnp.float32)
    center = lax.psum(jnp.sum(height, axis=1), "tp") / chan_total
    centered = height - center[:, None]
    variance = lax.psum(jnp.sum(centered * centered, axis=1), "tp") / chan_total
    inv_std = lax.rsqrt(variance + norm_eps)[:, None]
    normed = centered * inv_std
    shifted = normed * norm_gain + norm_shift
    sig_norm = jax.nn.sigmoid(shifted)
    active = (shifted * sig_norm).astype(jnp.bfloat16)
    act_grad = jnp.dot(out_grad, proj_weight, preferred_element_type=jnp.float32)
    norm_grad = act_grad * (sig_norm * (1.0 + shifted * (1.0 - sig_norm)))
    scaled = norm_grad * norm_gain
    grad_sum, grad_dot = lax.psum((jnp.sum(scaled, axis=1), jnp.sum(scaled * normed, axis=1)), "tp")
    height_grad = inv_std * (
        scaled - grad_sum[:, None] / chan_total - normed * (grad_dot[:, None] / chan_total)
    )
    sig_gate = jax.nn.sigmoid(conv_gate.astype(jnp.float32))
    value_float = conv_value.astype(jnp.float32)
    gated_rows = (value_float * sig_gate).astype(jnp.bfloat16)
    tap_values = conv_taps.astype(jnp.float32)
    earlier = shifted_2(gated_rows[seq_rows - tap_reach :], SP, 1)
    extended = jnp.concatenate([earlier, gated_rows], axis=0).astype(jnp.float32)
    padded_grad = jnp.pad(height_grad, ((tap_reach, tap_reach), (0, 0)))
    spill_rows = jnp.zeros((seq_rows + tap_reach, chan_local), jnp.float32)
    for tap_index in range(tap_reach + 1):
        begin = tap_reach - tap_index
        spill_rows = (
            spill_rows + tap_values[tap_index] * padded_grad[begin : begin + seq_rows + tap_reach]
        )
    returned = shifted_2(spill_rows[:tap_reach], SP, -1)
    gated_grad = spill_rows[tap_reach:] + jnp.pad(returned, ((seq_rows - tap_reach, 0), (0, 0)))
    tap_rows = jnp.stack(
        [
            jnp.sum(height_grad * extended[tap_index : tap_index + seq_rows], axis=0)
            for tap_index in range(tap_reach + 1)
        ]
    )
    gain_row = jnp.sum(norm_grad * normed, axis=0)
    shift_row = jnp.sum(norm_grad, axis=0)
    grad_taps, grad_gain, grad_shift = (
        one_axis_at_a_time(tap_rows, SP),
        one_axis_at_a_time(gain_row, SP),
        one_axis_at_a_time(shift_row, SP),
    )
    grad_value = (gated_grad * sig_gate).astype(jnp.bfloat16)
    grad_gate = (gated_grad * value_float * sig_gate * (1.0 - sig_gate)).astype(jnp.bfloat16)
    grad_proj = project_rows(out_grad, active)
    return (grad_value, grad_gate, grad_taps, grad_gain, grad_shift, grad_proj)


def solution(mesh):
    split = Mesh(mesh.devices.reshape(8, 4, 4, mesh.shape["tp"]), ("sp_0", "sp_1", "sp_2", "tp"))
    placed = (
        P(SP, "tp"),
        P(SP, "tp"),
        P(SP, "tp"),
        P(None, "tp"),
        P("tp"),
        P("tp"),
        P(None, "tp"),
        P(SP, None),
    )
    return jax.shard_map(
        local,
        mesh=split,
        in_specs=placed,
        out_specs=(P(SP, "tp"), P(SP, "tp"), P(None, "tp"), P("tp"), P("tp"), P(SP, "tp")),
        check_vma=False,
    )
```

profile of v0, /device:TPU:8, one launch (start us, length us, event | category | flops | bytes accessed | tf_op | source)
XLA Modules:
  0.0 350.7 jit_solution(18354876950033820677)
XLA Ops:
  7.3 2.0 fusion.54
  9.2 0.9 copy-done.5
  10.1 3.4 collective-permute-start.1
  13.6 0.2 convert_reduce_fusion
  13.7 2.5 psum.91
  16.2 1.5 fusion.50
  17.7 2.5 psum.92
  20.2 5.4 %fusion.49 = (f32[768]{0:T(1024)S(1)}, f32[512]{0:T(512)S(1)}, f32[512]{0:T(512)S(1)}, f32[768]{0:T(1024)S(1)}, f32[512,768]{1,0:T(8,128)}) fusion(bf16[512,768]{1,0:T(8,128)(2,1)} %param.10, f32[512]{0:T(512)S(1)} %add_rsqrt_fusion, f32[512]{0:T(512)S(1)} %broadcast_multiply_fusion.2, f32[768]{0:T(1024)S(1)} %copy-done.8, f32[768]{0:T(1024)S(1)} %copy-done.9, ...), kind=kOutput, calls=%fused_computation.70 | convolution fusion | flops 1618474496 | bytes 7622656 | tf_op jit(solution)/shard_map/dot_general | solution.py:53
  25.6 2.4 all-reduce.5
  28.0 1.4 maximum_convert_fusion
  29.5 0.4 copy-done.6
  29.9 4.8 %fusion.55 = (f32[768]{0:T(1024)S(1)}, f32[768]{0:T(1024)S(1)}, f32[768]{0:T(1024)S(1)}, f32[768]{0:T(1024)S(1)}, f32[768]{0:T(1024)S(1)}, /*index=5*/f32[768]{0...) fusion(f32[542,768]{1,0:T(8,128)S(1)} %maximum_convert_fusion, ...), kind=kLoop, calls=%fused_computation.77 | loop fusion | flops 17287680 | bytes 32310272 | tf_op jit(solution)/shard_map/reduce_sum | solution.py:77
  34.7 2.5 fusion.73
  37.7 2.6 stack.127
  40.3 6.6 %convolution_bitcast_fusion = f32[2048,768]{0,1:T(8,128)} fusion(bf16[512,2048]{1,0:T(8,128)(2,1)} %param.15, bf16[512,768]{1,0:T(8,128)(2,1)} %param.10, f32[768]{0:T(1024)S(1)} %copy-done.9, f32[768]{0:T(1024)S(1)} %copy-done.8, f32[512]{0:T(512)S(1)} %add_rsqrt_fusion, f32[512]{0:T(512)S(1)} %broadcast_multiply_fusion.2), kind=kOutput, calls=%fused_computation | convolution fusion | flops 1614544896 | bytes 9185280 | tf_op jit(solution)/shard_map/dot_general | solution.py:33
  47.0 68.5 %all-reduce.10.cloned.1.call-done = f32[31,768]{1,0:T(8,128)} async-done(((f32[31,768]{1,0:T(8,128)}), f32[31,768]{1,0:T(8,128)}) %all-reduce.10.cloned.1.call-update) | async-done | bytes 95248 | tf_op jit(solution)/shard_map/psum | solution.py:28
  115.5 75.7 %reduce-scatter.8.cloned.1.call-done = f32[256,768]{0,1:T(8,128)} async-done(((f32[2048,768]{0,1:T(8,128)}), f32[256,768]{0,1:T(8,128)}) %reduce-scatter.8.cloned.1.call-update) | async-done | bytes 786448 | tf_op jit(solution)/shard_map/reduce_scatter | solution.py:17
  191.2 2.3 copy.16
  193.6 0.1 slice_reduce_fusion.29
  193.7 0.2 slice_reduce_fusion.30
  193.9 43.6 %all-reduce.12.cloned.1.call-done = f32[31,768]{1,0:T(8,128)} async-done(((f32[31,768]{1,0:T(8,128)}), f32[31,768]{1,0:T(8,128)}) %all-reduce.12.cloned.1.call-update) | async-done | bytes 95248 | tf_op jit(solution)/shard_map/psum | solution.py:28
  237.5 0.2 reduce-scatter.12.cloned.1.call-start
  237.7 25.3 %multiply_add_fusion = f32[542,768]{1,0:T(8,128)S(1)} fusion(f32[512,768]{1,0:T(8,128)} %copy-done.1, f32[768]{0:T(1024)S(1)} %get-tuple-element.54, f32[768]{0:T(1024)S(1)} %get-tuple-element.55, f32[768]{0:T(1024)S(1)} %get-tuple-element.56, f32[768]{0:T(1024)S(1)} %get-tuple-element.57, f32[768]{0:T(1024)S(1)} %get-tuple-element.58, ...), kind=kLoop, calls=%fused_computation.11 | loop fusion | flops 25391616 | bytes 3333120 | tf_op jit(solution)/shard_map/add | solution.py:71
  263.0 1.2 copy-done.4
  264.2 5.7 %collective-permute-start = (f32[30,768]{1,0:T(8,128)S(1)}, f32[30,768]{1,0:T(8,128)S(1)}, u32[]{:S(2)}, u32[]{:S(2)}) collective-permute-start(f32[30,768]{1,0:T(8,128)S(1)} %slice.416), channel_id=1, source_target_pairs={{2,0},{4,2},{6,4},{8,6},{10,8},{12,10},{14,12},{16,14},{18,16},{20... | collective-permute-start | bytes 276488 | tf_op jit(solution)/shard_map/ppermute | solution.py:24
  269.9 17.7 %all-reduce.2 = (f32[768]{0:T(1024)S(1)}, f32[768]{0:T(1024)S(1)}) all-reduce(f32[768]{0:T(1024)S(1)} %get-tuple-element.49, f32[768]{0:T(1024)S(1)} %get-tuple-element.52), channel_id=1, replica_groups=mesh['sp_0'=8,'sp_1'=4,'sp_2'=4,'tp'=2] {'sp_0'}, use_global_device_ids=true, to_apply=%region_43.44 | all-reduce | flops 1536 | bytes 12288 | tf_op jit(solution)/shard_map/psum | solution.py:28
  287.7 10.2 %all-reduce.4 = (f32[768]{0:T(1024)S(1)}, f32[768]{0:T(1024)S(1)}) all-reduce(f32[768]{0:T(1024)S(1)} %get-tuple-element.84, f32[768]{0:T(1024)S(1)} %get-tuple-element.85), channel_id=1, replica_groups=mesh['sp_0'=8,'sp_1'=4,'sp_2'=4,'tp'=2] {'sp_1'}, use_global_device_ids=true, to_apply=%region_44.45 | all-reduce | flops 1536 | bytes 12288 | tf_op jit(solution)/shard_map/psum | solution.py:28
  297.8 8.4 %all-reduce.3 = (f32[768]{0:T(1024)}, f32[768]{0:T(1024)}) all-reduce(f32[768]{0:T(1024)S(1)} %get-tuple-element.88, f32[768]{0:T(1024)S(1)} %get-tuple-element.89), channel_id=1, replica_groups=mesh['sp_0'=8,'sp_1'=4,'sp_2'=4,'tp'=2] {'sp_2'}, use_global_device_ids=true, to_apply=%region_45.46 | all-reduce | flops 1536 | bytes 12288 | tf_op jit(solution)/shard_map/psum | solution.py:28
  306.3 3.7 %fusion.53 = (bf16[512,768]{1,0:T(8,128)(2,1)}, bf16[512,768]{1,0:T(8,128)(2,1)}) fusion(bf16[512,768]{1,0:T(8,128)(2,1)} %param.8, f32[30,768]{1,0:T(8,128)S(1)} %collective-permute-done, f32[542,768]{1,0:T(8,128)} %copy-done.4, bf16[512,768]{1,0:T(8,128)(2,1)} %param.9), kind=kLoop, calls=%fused_computation.74 | loop fusion | flops 5111808 | bytes 4810752 | tf_op jit(solution)/shard_map/convert_element_type | solution.py:89
  310.0 5.6 %all-reduce.14.cloned.1.call-done = f32[31,768]{1,0:T(8,128)} async-done(((f32[31,768]{1,0:T(8,128)}), f32[31,768]{1,0:T(8,128)}) %all-reduce.14.cloned.1.call-update) | async-done | bytes 95248 | tf_op jit(solution)/shard_map/psum | solution.py:28
  315.6 26.7 %reduce-scatter.12.cloned.1.call-done = f32[16,768]{1,0:T(8,128)} async-done(((f32[64,768]{1,0:T(8,128)}), f32[16,768]{1,0:T(8,128)}) %reduce-scatter.12.cloned.1.call-update) | async-done | bytes 49168
  342.3 1.5 copy.23
  (68 shorter events, 0.5 us)
Async XLA Ops:
  7.2 13.0 %copy-start = (bf16[2048,768]{1,0:T(8,128)(2,1)S(1)}, bf16[2048,768]{1,0:T(8,128)(2,1)}, u32[]{:S(2)}) copy-start(bf16[2048,768]{1,0:T(8,128)(2,1)} %param.14) | copy-start | bytes 9437188
  7.2 13.0 %copy-start.8 = (f32[768]{0:T(1024)S(1)}, f32[768]{0:T(1024)}, u32[]{:S(2)}) copy-start(f32[768]{0:T(1024)} %param.12) | copy-start | bytes 9220
  7.2 13.0 %copy-start.9 = (f32[768]{0:T(1024)S(1)}, f32[768]{0:T(1024)}, u32[]{:S(2)}) copy-start(f32[768]{0:T(1024)} %param.13) | copy-start | bytes 9220
  7.2 108.2 %all-reduce.10.cloned.1.call-start = ((), (), s32[]{:S(2)}) async-start(), calls=%async_computation.3 | async-start | bytes 196608 | tf_op jit(solution)/shard_map/psum | solution.py:28
  7.2 6.3 %copy-start.2 = (bf16[512,768]{1,0:T(8,128)(2,1)S(1)}, bf16[512,768]{1,0:T(8,128)(2,1)}, u32[]{:S(2)}) copy-start(bf16[512,768]{1,0:T(8,128)(2,1)} %param.10) | copy-start | bytes 2359300
  9.2 0.9 copy-start.5
  10.1 17.9 %collective-permute-start.1 = (bf16[30,768]{1,0:T(8,128)(2,1)S(1)}, bf16[30,768]{1,0:T(8,128)(2,1)S(1)}, u32[]{:S(2)}, u32[]{:S(2)}) collective-permute-start(bf16[30,768]{1,0:T(8,128)(2,1)S(1)} %slice.417), channel_id=1, source_target_pairs={{0,2},{2,4},{4,6},{6,8},{8,10},{10,12},{12,14},{14,16},{16,18},{18... | collective-permute-start | bytes 138248 | tf_op jit(solution)/shard_map/ppermute | solution.py:24
  28.0 1.5 copy-start.3
  28.0 1.9 copy-start.6
  34.7 2.6 copy-start.1
  40.3 150.9 %reduce-scatter.8.cloned.1.call-start = ((), (), s32[]{:S(2)}) async-start(), calls=%async_computation.6 | async-start | bytes 7077888 | tf_op jit(solution)/shard_map/reduce_scatter | solution.py:17
  46.9 146.6 %copy-start.7 = (bf16[31,768]{1,0:T(8,128)(2,1)S(1)}, bf16[31,768]{1,0:T(8,128)(2,1)}, u32[]{:S(2)}) copy-start(bf16[31,768]{1,0:T(8,128)(2,1)} %param.11) | copy-start | bytes 142852
  46.9 190.5 %all-reduce.12.cloned.1.call-start = ((), (), s32[]{:S(2)}) async-start(), calls=%async_computation.4 | async-start | bytes 196608 | tf_op jit(solution)/shard_map/psum | solution.py:28
  115.5 190.8 %reduce-scatter.10.cloned.1.call-start = ((), (), s32[]{:S(2)}) async-start(), calls=%async_computation.7 | async-start | bytes 983040
  193.5 122.1 %all-reduce.14.cloned.1.call-start = ((), (), s32[]{:S(2)}) async-start(), calls=%async_computation.5 | async-start | bytes 196608 | tf_op jit(solution)/shard_map/psum | solution.py:28
  237.5 104.8 %reduce-scatter.12.cloned.1.call-start = ((), (), s32[]{:S(2)}) async-start(), calls=%async_computation.8 | async-start | bytes 245760
  263.0 1.2 copy-start.4
  264.2 42.1 %collective-permute-start = (f32[30,768]{1,0:T(8,128)S(1)}, f32[30,768]{1,0:T(8,128)S(1)}, u32[]{:S(2)}, u32[]{:S(2)}) collective-permute-start(f32[30,768]{1,0:T(8,128)S(1)} %slice.416), channel_id=1, source_target_pairs={{2,0},{4,2},{6,4},{8,6},{10,8},{12,10},{14,12},{16,14},{18,16},{20... | collective-permute-start | bytes 276488 | tf_op jit(solution)/shard_map/ppermute | solution.py:24
Sparse Core Ops, SparseCore 0:
  40.4 75.0 all-reduce.9
  118.0 73.1 reduce-scatter.7
  193.5 43.8 all-reduce.11
  240.4 24.4 reduce-scatter.9
  267.1 48.4 all-reduce.13
  318.6 23.7 reduce-scatter.11
where the time goes:
time: 351 us
  waiting for transfers between devices  220 us (63%)
  blocking collectives  43.7 us (12%)
  other arithmetic  41.4 us (12%)
  between operations  14.6 us (4%)
  matrix products  11.9 us (3%)
  starting transfers between devices  9.56 us (3%)
  local copies, waits for them, and re-layouts  9.34 us (3%)
    psum x3, waiting for transfers between devices, one_axis_at_a_time(): return functools.reduce(lax.psum, axes, array)  118 us
    reduce_scatter x1, waiting for transfers between devices, own_rows_2(): running = lax.psum_scatter(running, axis, scatter_dimension=0, tiled=True)  75.7 us
    psum x3, blocking collectives, one_axis_at_a_time(): return functools.reduce(lax.psum, axes, array)  36.3 us
    unnamed x8, waiting for transfers between devices  26.8 us
    add x1, other arithmetic, local(): spill_rows + tap_values[tap_index] * padded_grad[begin:begin + seq_rows +...  25.3 us
    ppermute x2, starting transfers between devices, shifted_2(): return lax.ppermute(block, axis, route)  9.14 us
    reduce_sum x2, other arithmetic, local(): jnp.sum(height_grad * extended[tap_index:tap_index + seq_rows], axis=0)  7.32 us
  transfers between devices with their start and end apart: 8, of which 5 were waited for; matrix products, arithmetic and copies ran while one was open for 13% of the time, Pallas kernels for 0%

commit v1 on v0

v1 whole, which is shorter than its diff:
```python
import functools

import jax
import jax.numpy as jnp
from jax import lax
from jax.experimental import pallas as pl
from jax.experimental.pallas import tpu as pltpu
from jax.sharding import Mesh
from jax.sharding import PartitionSpec as P


SP = ("sp_0", "sp_1", "sp_2")
ALL = SP + ("tp",)
EPS = 1e-05
F32 = jnp.float32
BF16 = jnp.bfloat16
LANES = 128
MIB = 1024 * 1024


def vmem(count):
    return [pl.BlockSpec(memory_space=pltpu.VMEM)] * count


def call(kernel, outs, *args, flops, scratch=(), specs=None, limit=8):
    moved = sum(a.size * a.dtype.itemsize for a in args) + sum(
        o.size * o.dtype.itemsize for o in outs
    )
    return pl.pallas_call(
        kernel,
        out_shape=outs,
        in_specs=specs or vmem(len(args)),
        out_specs=vmem(len(outs)),
        scratch_shapes=list(scratch),
        cost_estimate=pl.CostEstimate(flops=flops, bytes_accessed=moved, transcendentals=0),
        compiler_params=pltpu.CompilerParams(vmem_limit_bytes=limit * MIB),
    )(*args)


def shape(dims, dtype):
    return jax.ShapeDtypeStruct(dims, dtype)


def left_half(rows):
    return lax.broadcasted_iota(jnp.int32, (rows, LANES), 1) < LANES // 2


def both(packed):
    left = left_half(packed.shape[0])
    turned = pltpu.roll(packed, LANES // 2, 1)
    return jnp.where(left, packed, turned), jnp.where(left, turned, packed)


def tiles(chans):
    return [slice(at, at + LANES) for at in range(0, chans, LANES)]


def front_kernel(
    place_ref, conv_hbm, grad_hbm, weight_hbm, stats_ref, act_grad_ref, conv_ref, grad_ref,
    weight_ref, conv_sem, grad_sem, weight_sem,
):
    loads = [
        pltpu.make_async_copy(conv_hbm, conv_ref, conv_sem),
        pltpu.make_async_copy(weight_hbm, weight_ref, weight_sem),
        pltpu.make_async_copy(grad_hbm, grad_ref, grad_sem),
    ]
    for load in loads:
        load.start()
    loads[0].wait()
    rows, chans = conv_ref.shape
    step = 128
    left = left_half(step)
    for begin in range(0, rows, step):
        at = slice(begin, begin + step)
        total = jnp.sum(
            sum(conv_ref[at, c].astype(F32) for c in tiles(chans)), axis=1, keepdims=True
        )
        mean = jnp.broadcast_to(total * (1.0 / chans), (step, LANES))
        spread = 0.0
        for c in tiles(chans):
            off = conv_ref[at, c].astype(F32) - mean
            spread = spread + off * off
        stats_ref[at, :] = jnp.where(left, total, jnp.sum(spread, axis=1, keepdims=True))
    for load in loads[1:]:
        load.wait()
    act_grad_ref[...] = jnp.dot(grad_ref[...], weight_ref[...], preferred_element_type=F32)


def turn_kernel(place_ref, grad_ref, turned_ref):
    _, width = grad_ref.shape
    piece = width // place_ref.shape[0]
    span = LANES
    each = span // piece

    def body(b, carry):
        columns = pl.ds(pl.multiple_of(b * span, span), span)
        turned = grad_ref[:, columns].T
        for p in range(each):
            to = place_ref[b * each + p]
            turned_ref[pl.ds(pl.multiple_of(to, piece), piece), :] = turned[
                p * piece : (p + 1) * piece, :
            ]
        return carry

    lax.fori_loop(0, width // span, body, 0, unroll=4)


def middle_kernel(
    conv_ref, own_ref, peer_ref, gain_ref, shift_ref, act_grad_ref,
    active_ref, lifted_ref, normed_ref, inv_ref, sums_ref, params_ref,
    center_ref, total_ref, dot_ref,
):
    rows, chans = conv_ref.shape
    wide = 128
    for begin in range(0, rows, wide):
        at = slice(begin, begin + wide)
        sum_a, dev_a = both(own_ref[at, :])
        sum_b, dev_b = both(peer_ref[at, :])
        apart = (sum_a - sum_b) * (1.0 / chans)
        variance = (dev_a + dev_b + apart * apart * (0.5 * chans)) * (0.5 / chans)
        center_ref[at, :] = (sum_a + sum_b) * (0.5 / chans)
        inv_ref[at, :] = lax.rsqrt(variance + EPS)
    step = 32

    def fold(x):
        return jnp.sum(x.reshape(step // 8, 8, LANES), axis=0)

    def body(i, carry):
        out = []
        at = pl.ds(pl.multiple_of(i * step, step), step)
        center, inv = center_ref[at, :], inv_ref[at, :]
        total, dot = 0.0, 0.0
        for k, c in enumerate(tiles(chans)):
            gain, shift = gain_ref[c].reshape(1, LANES), shift_ref[c].reshape(1, LANES)
            normed = (conv_ref[at, c].astype(F32) - center) * inv
            shifted = normed * gain + shift
            sig = jax.nn.sigmoid(shifted)
            active = shifted * sig
            active_ref[at, c] = active.astype(BF16)
            norm_grad = act_grad_ref[at, c] * (sig + active * (1.0 - sig))
            scaled = norm_grad * gain
            lifted_ref[at, c] = scaled * inv
            normed_ref[at, c] = normed
            total = total + scaled
            dot = dot + scaled * normed
            out.append(carry[2 * k] + fold(norm_grad * normed))
            out.append(carry[2 * k + 1] + fold(norm_grad))
        total_ref[at, :] = total
        dot_ref[at, :] = dot
        return tuple(out)

    zero = jnp.zeros((8, LANES), F32)
    folded = lax.fori_loop(0, rows // step, body, (zero,) * (2 * len(tiles(chans))))
    for k, c in enumerate(tiles(chans)):
        params_ref[0:1, c] = jnp.sum(folded[2 * k], axis=0, keepdims=True)
        params_ref[1:2, c] = jnp.sum(folded[2 * k + 1], axis=0, keepdims=True)
    left = left_half(wide)
    for begin in range(0, rows, wide):
        at = slice(begin, begin + wide)
        sums_ref[at, :] = jnp.where(
            left,
            jnp.sum(total_ref[at, :], axis=1, keepdims=True),
            jnp.sum(dot_ref[at, :], axis=1, keepdims=True),
        )


def project_kernel(turned_ref, active_ref, *out_refs):
    rows = out_refs[0].shape[0]
    for k, out_ref in enumerate(out_refs):
        out_ref[...] = jnp.dot(
            turned_ref[k * rows : (k + 1) * rows, :], active_ref[...], preferred_element_type=F32
        ).astype(BF16)


def head_kernel(
    lifted_ref, normed_ref, inv_ref, sums_ref, sums_peer_ref, mean_ref, slope_ref, head_ref
):
    rows, chans = lifted_ref.shape
    wide = 128
    for begin in range(0, rows, wide):
        at = slice(begin, begin + wide)
        total, dot = both(sums_ref[at, :] + sums_peer_ref[at, :])
        scale = inv_ref[at, :] * (0.5 / chans)
        mean_ref[at, :] = total * scale
        slope_ref[at, :] = dot * scale
    at = slice(0, head_ref.shape[0])
    for c in tiles(chans):
        head_ref[at, c] = lifted_ref[at, c] - mean_ref[at, :] - normed_ref[at, c] * slope_ref[at, :]


def fill_moved(moved, lanes, lifted_ref, normed_ref, mean_ref, slope_ref, halo_ref):
    rows = lifted_ref.shape[0]
    tail = halo_ref.shape[0]
    moved[0, 0:rows, :] = (
        lifted_ref[:, lanes] - mean_ref[...] - normed_ref[:, lanes] * slope_ref[...]
    )
    moved[0, rows : rows + tail, :] = halo_ref[:, lanes]
    for s in range(1, 8):
        moved[s, 0 : rows + tail - 8, :] = moved[0, s : s + rows + tail - 8, :]


def strips(body, chans):
    def step(i, carry):
        body(pl.ds(pl.multiple_of(i * LANES, LANES), LANES))
        return carry

    lax.fori_loop(0, chans // LANES, step, 0)


GROUP = 4


def taps_kernel(
    value_ref, gate_ref, lifted_ref, normed_ref, mean_ref, slope_ref, halo_ref, params_ref,
    out_ref, moved, gated, rows_ref,
):
    rows, chans = value_ref.shape
    taps = halo_ref.shape[0] - 1
    reach = taps - 1
    step = 8 * GROUP

    def one(lanes):
        fill_moved(moved, lanes, lifted_ref, normed_ref, mean_ref, slope_ref, halo_ref)
        sig = jax.nn.sigmoid(gate_ref[:, lanes].astype(F32))
        gated[...] = (value_ref[:, lanes].astype(F32) * sig).astype(BF16).astype(F32)

        def body(i, sums):
            at = pl.multiple_of(i * step, step)
            held = [gated[pl.ds(at + 8 * b, 8), :] for b in range(GROUP)]
            out = list(sums)
            for s in range(8):
                overs = range(s, taps, 8)
                there = [
                    moved[s, pl.ds(at + 8 * m, 8), :] for m in range(GROUP + len(overs) - 1)
                ]
                for q, over in enumerate(overs):
                    j = reach - over
                    products = [held[b] * there[b + q] for b in range(GROUP)]
                    out[j] = out[j] + ((products[0] + products[1]) + (products[2] + products[3]))
            return tuple(out)

        zero = jnp.zeros((8, LANES), F32)
        sums = lax.fori_loop(0, rows // step, body, (zero,) * taps)
        for j in range(taps):
            rows_ref[j : j + 1, :] = jnp.sum(sums[j], axis=0, keepdims=True)
        rows_ref[taps : taps + 2, :] = params_ref[:, lanes]
        rows_ref[taps + 2 :, :] = jnp.zeros((rows_ref.shape[0] - taps - 2, LANES), F32)
        out_ref[:, lanes] = rows_ref[...].astype(BF16)

    strips(one, chans)


def spread_kernel(
    value_ref, gate_ref, lifted_ref, normed_ref, mean_ref, slope_ref, halo_ref, taps_ref,
    grad_value_ref, grad_gate_ref, moved, spread,
):
    rows, chans = value_ref.shape
    taps = taps_ref.shape[0]
    reach = taps - 1
    step = 8 * GROUP

    def one(lanes):
        fill_moved(moved, lanes, lifted_ref, normed_ref, mean_ref, slope_ref, halo_ref)
        weights = taps_ref[:, lanes].astype(F32)
        for j in range(taps):
            spread[j] = jnp.broadcast_to(weights[j : j + 1, :], (8, LANES))

        def body(i, carry):
            at = pl.multiple_of(i * step, step)
            total = [None] * GROUP
            for s in range(8):
                overs = range(s, taps, 8)
                there = [
                    moved[s, pl.ds(at + 8 * m, 8), :] for m in range(GROUP + len(overs) - 1)
                ]
                for q, over in enumerate(overs):
                    weight = spread[reach - over]
                    for b in range(GROUP):
                        term = weight * there[b + q]
                        total[b] = term if total[b] is None else total[b] + term
            here = pl.ds(at, step)
            gated_grad = jnp.concatenate(total, axis=0)
            sig = jax.nn.sigmoid(gate_ref[here, lanes].astype(F32))
            grad_value = gated_grad * sig
            grad_value_ref[here, lanes] = grad_value.astype(BF16)
            grad_gate_ref[here, lanes] = (
                grad_value * value_ref[here, lanes].astype(F32) * (1.0 - sig)
            ).astype(BF16)
            return carry

        lax.fori_loop(0, rows // step, body, 0)

    strips(one, chans)


def added(refs, at=slice(None)):
    return functools.reduce(lambda a, b: a + b, [r[at, :].astype(F32) for r in refs])


def second_kernel(n, *refs):
    landed, small, outs = refs[:n], refs[n : 2 * n], refs[2 * n :]
    rows = landed[0].shape[0] // n
    more = added(small).astype(BF16)
    for k, out in enumerate(outs):
        out[0:rows, :] = added(landed, slice(k * rows, (k + 1) * rows)).astype(BF16)
        out[rows:, :] = more


def third_kernel(*refs):
    landed, (keep_ref, send_ref) = refs[:-2], refs[-2:]
    rows = keep_ref.shape[0]
    keep_ref[...] = added(landed, slice(0, rows))
    send_ref[...] = added(landed, slice(rows, None)).astype(BF16)


def fourth_kernel(keep_ref, sent_ref, came_ref, *outs):
    rows = keep_ref.shape[0]
    own = rows // len(outs)
    small = added((sent_ref, came_ref), slice(rows, None)).astype(BF16)
    for k, out in enumerate(outs):
        at = slice(k * own, (k + 1) * own)
        out[0:own, :] = added((keep_ref, came_ref), at).astype(out.dtype)
        out[own:, :] = small.astype(out.dtype)


def last_kernel(taps, *refs):
    landed, (project_ref, taps_ref, params_ref) = refs[:-3], refs[-3:]
    own = project_ref.shape[0]
    total = added(landed)
    project_ref[...] = total[:own, :]
    taps_ref[...] = total[own : own + taps, :]
    params_ref[...] = total[own + taps : own + taps + 2, :]


def local(conv_value, conv_gate, conv_out, conv_taps, norm_gain, norm_shift, proj_weight, out_grad):
    rows, chans = conv_value.shape
    width = out_grad.shape[1]
    taps = conv_taps.shape[0]
    nz, n, _, cores = (lax.axis_size(a) for a in ALL)
    tail = taps + 1
    extra = -(-(taps + 2) // 8) * 8
    own = width // (nz * n * n)

    z, y, x, core = (lax.axis_index(a) for a in ALL)
    group = lax.iota(jnp.int32, nz * n * n)
    away_y, away_x = (group // n + n - y) % n, (group + n - x) % n
    to_z = group // (n * n)
    away_z = (to_z + nz - z) % nz
    odd = (to_z + z) % 2
    slot_z = odd * (nz // 2) + jnp.where(odd == 1, (to_z + nz - (z ^ 1)) % nz, away_z) // 2
    ahead = jnp.where(core == 0, away_x, away_y) * n + jnp.where(core == 0, away_y, away_x)
    place = (ahead * nz + slot_z) * own

    places = [
        (z, y, x, c) for z in range(nz) for y in range(n) for x in range(n) for c in range(cores)
    ]

    def index(z, y, x, c):
        return ((z * n + y) * n + x) * cores + c

    def hop(array, k, stage):
        def to(z, y, x, c):
            if (c == 0) == (stage == 1):
                return index(z, y, (x + k) % n, c)
            return index(z, (y + k) % n, x, c)

        return lax.ppermute(array, ALL, [(index(*at), to(*at)) for at in places])

    def hop_z(array, k):
        return lax.ppermute(array, "sp_0", [(i, (i + k) % nz) for i in range(nz)])

    def swap_z(array):
        return lax.ppermute(array, "sp_0", [(i, i ^ 1) for i in range(nz)])

    def other_core(array):
        return lax.ppermute(array, "tp", [(0, 1), (1, 0)])

    def previous(array):
        return lax.ppermute(array, SP, [(i, i - 1) for i in range(1, nz * n * n)])

    stats, act_grad, height, grads = call(
        front_kernel,
        (
            shape((rows, LANES), F32), shape((rows, chans), F32),
            shape(conv_out.shape, BF16), shape(out_grad.shape, BF16),
        ),
        place, *(pltpu.with_memory_space_constraint(a, pltpu.HBM) for a in (conv_out, out_grad, proj_weight)),
        flops=2 * rows * width * chans,
        scratch=[pltpu.VMEM(proj_weight.shape, BF16)] + [pltpu.SemaphoreType.DMA] * 3,
        specs=[pl.BlockSpec(memory_space=pltpu.SMEM)] + [pl.BlockSpec(memory_space=pltpu.HBM)] * 3,
        limit=12,
    )
    stats_peer = other_core(stats)
    (turned,) = call(
        turn_kernel,
        (shape((width, rows), BF16),),
        place, grads,
        flops=rows * width * chans,
        specs=[pl.BlockSpec(memory_space=pltpu.SMEM)] + vmem(1),
        limit=4,
    )
    active, lifted, normed, inv, sums, params = call(
        middle_kernel,
        (
            shape((rows, chans), BF16), shape((rows, chans), F32), shape((rows, chans), F32),
            shape((rows, LANES), F32), shape((rows, LANES), F32), shape((2, chans), F32),
        ),
        height, stats, stats_peer, norm_gain, norm_shift, act_grad,
        flops=rows * chans * 1000,
        scratch=[pltpu.VMEM((rows, LANES), F32)] * 3,
    )
    sums_peer = other_core(sums)
    blocks = call(
        project_kernel,
        (shape((width // n, chans), BF16),) * n,
        turned, active,
        flops=2 * rows * width * chans,
    )
    mean, slope, head = call(
        head_kernel,
        (shape((rows, LANES), F32), shape((rows, LANES), F32), shape((tail, chans), F32)),
        lifted, normed, inv, sums, sums_peer,
        flops=rows * chans * 10,
    )
    halo = previous(head)
    landed = [blocks[0]] + [hop(blocks[k], k, 1) for k in range(1, n)]
    heights = (lifted, normed, mean, slope, halo)
    (small,) = call(
        taps_kernel,
        (shape((extra, chans), BF16),),
        conv_value, conv_gate, *heights, params,
        flops=taps * rows * chans * 40,
        scratch=[pltpu.VMEM((8, rows + tail, LANES), F32), pltpu.VMEM((rows, LANES), F32),
            pltpu.VMEM((extra, LANES), F32),
        ],
    )
    grad_value, grad_gate = call(
        spread_kernel,
        (shape((rows, chans), BF16),) * 2,
        conv_value, conv_gate, *heights, conv_taps,
        flops=taps * rows * chans * 40,
        scratch=[pltpu.VMEM((8, rows + tail, LANES), F32), pltpu.VMEM((taps, 8, LANES), F32)],
    )
    smalls = [small] + [hop(small, k, 1) for k in range(1, n)]
    part = width // (n * n)
    second = call(
        functools.partial(second_kernel, n),
        (shape((part + extra, chans), BF16),) * n,
        *landed, *smalls,
        flops=width * chans * 100,
    )
    then = [second[0]] + [hop(second[k], k, 2) for k in range(1, n)]
    keep, send = call(
        third_kernel,
        (shape((part // 2, chans), F32), shape((part // 2 + extra, chans), BF16)),
        *then,
        flops=width * chans * 10,
    )
    came = swap_z(send)
    fourth = call(
        fourth_kernel,
        (shape((own + extra, chans), F32),) + (shape((own + extra, chans), BF16),) * (nz // 2 - 1),
        keep, send, came,
        flops=width * chans * 10,
    )
    fars = [fourth[0]] + [hop_z(fourth[k], 2 * k) for k in range(1, nz // 2)]
    grad_proj, grad_taps, grad_params = call(
        functools.partial(last_kernel, taps),
        (shape((own, chans), F32), shape((taps, chans), F32), shape((2, chans), F32)),
        *fars,
        flops=width * chans * 10,
    )
    return grad_value, grad_gate, grad_taps, grad_params[0], grad_params[1], grad_proj


def solution(mesh):
    split = Mesh(mesh.devices.reshape(8, 4, 4, mesh.shape["tp"]), ALL)
    placed = (
        P(SP, "tp"),
        P(SP, "tp"),
        P(SP, "tp"),
        P(None, "tp"),
        P("tp"),
        P("tp"),
        P(None, "tp"),
        P(SP, None),
    )
    return jax.shard_map(
        local,
        mesh=split,
        in_specs=placed,
        out_specs=(P(SP, "tp"), P(SP, "tp"), P(None, "tp"), P("tp"), P("tp"), P(SP, "tp")),
        check_vma=False,
    )
```

time: 351 us -> 94.3 us (0.27)
  waiting for transfers between devices: 220 us -> 34.2 us
  blocking collectives: 43.7 us -> 0 us
  other arithmetic: 41.4 us -> 0.03 us
  Pallas kernels: 0 us -> 25.5 us
  starting transfers between devices: 9.56 us -> 33 us
  between operations: 14.6 us -> 0.77 us
  matrix products: 11.9 us -> 0 us
  local copies, waits for them, and re-layouts: 9.34 us -> 0.64 us
    psum x3 -> x0, waiting for transfers between devices: 118 us -> none  [one_axis_at_a_time(): return functools.reduce(lax.psum, axes, array)]
    reduce_scatter x1 -> x0, waiting for transfers between devices: 75.7 us -> none  [own_rows_2(): running = lax.psum_scatter(running, axis, scatter_dimension=0, tiled=True)]
    psum x6 -> x0, blocking collectives: 43.7 us -> none  [the longest x3 36.3 us: one_axis_at_a_time(): return functools.reduce(lax.psum, axes, array)]
    ppermute x2 -> x16, waiting for transfers between devices: 0.01 us -> 34.2 us  [the longest x9 15.7 us: hop(): return lax.ppermute(array, ALL, [(index(*at), to(*at)) for at in places])]
    unnamed x8 -> x0, waiting for transfers between devices: 26.8 us -> none
    pallas_call x0 -> x11, Pallas kernels: none -> 25.5 us  [call(): pl.pallas_call(kernel, out_shape=outs, in_specs=specs or vmem(len(args)),...]
    add x1 -> x0, other arithmetic: 25.3 us -> none  [local(): spill_rows + tap_values[tap_index] * padded_grad[begin:begin + seq_rows +...]
    ppermute x2 -> x16, starting transfers between devices: 9.14 us -> 33 us  [the longest x9 15.7 us: hop(): return lax.ppermute(array, ALL, [(index(*at), to(*at)) for at in places])]
  transfers between devices with their start and end apart: 8 -> 16, of which waited for: 5 -> 9; matrix products, arithmetic and copies ran while one was open for 13% -> 0% of each run, Pallas kernels for 0% -> 17%
where the time goes in v1:
time: 94.3 us; the launch traced here: 94.2 us
  waiting for transfers between devices  34.2 us (36%)
  starting transfers between devices  33 us (35%)
  Pallas kernels  25.5 us (27%)
    pallas_call x11, Pallas kernels, call(): pl.pallas_call(kernel, out_shape=outs, in_specs=specs or vmem(len(args)),...  25.5 us
    ppermute x9, starting transfers between devices, hop(): return lax.ppermute(array, ALL, [(index(*at), to(*at)) for at in places])  15.7 us
    ppermute x9, waiting for transfers between devices, hop(): return lax.ppermute(array, ALL, [(index(*at), to(*at)) for at in places])  15.7 us
    ppermute x1, waiting for transfers between devices, previous(): return lax.ppermute(array, SP, [(i, i - 1) for i in range(1, nz * n * n)])  13.4 us
    ppermute x3, starting transfers between devices, hop_z(): return lax.ppermute(array, 'sp_0', [(i, (i + k) % nz) for i in range(nz)])  11.4 us
    ppermute x1, starting transfers between devices, previous(): return lax.ppermute(array, SP, [(i, i - 1) for i in range(1, nz * n * n)])  3.83 us
    ppermute x1, waiting for transfers between devices, swap_z(): return lax.ppermute(array, 'sp_0', [(i, i ^ 1) for i in range(nz)])  3.37 us
    ppermute x1, starting transfers between devices, swap_z(): return lax.ppermute(array, 'sp_0', [(i, i ^ 1) for i in range(nz)])  1.99 us
  transfers between devices with their start and end apart: 16, of which 9 were waited for; matrix products, arithmetic and copies ran while one was open for 0% of the time, Pallas kernels for 17%

profile of v1, /device:TPU:8, one launch (start us, length us, event | category | flops | bytes accessed | tf_op | source)
XLA Modules:
  0.0 94.2 jit_solution(4740354804491669216)
XLA Ops:
  0.7 5.2 %shard_map.127 = (f32[512,128]{1,0:T(8,128)S(1)}, f32[512,768]{1,0:T(8,128)S(1)}, bf16[512,768]{1,0:T(8,128)(2,1)S(1)}, bf16[512,2048]{1,0:T(8,128)(2,1)S(1)}) custom-call(s32[128]{0:T(128)S(1)} %add_multiply_fusion.place_ref, bf16[512,768]{1,0:T(8,128)(2,1)} %conv_hbm.1, bf16[512,2048]{1,0:T(8,128)(2,1)} %grad_hbm.1, bf16[2048,768]{1,0:T(8,128)(2,1)} %weight_hbm.1), custom_call_target="tpu_custom_call" | custom-call | flops 1610612736 | bytes 10748416 | tf_op jit(solution)/shard_map/pallas_call | solution.py:29
  6.0 1.3 %shard_map.131.turned_ref = bf16[2048,512]{1,0:T(8,128)(2,1)S(1)} custom-call(s32[128]{0:T(128)S(1)} %add_multiply_fusion.place_ref, bf16[512,2048]{1,0:T(8,128)(2,1)S(1)} %get-tuple-element.50.grad_ref), custom_call_target="tpu_custom_call" | custom-call | flops 805306368 | bytes 4194816 | tf_op jit(solution)/shard_map/pallas_call | solution.py:29
  7.3 0.2 collective-permute-done.peer_ref
  7.5 1.6 %shard_map.128 = (bf16[512,768]{1,0:T(8,128)(2,1)S(1)}, f32[512,768]{1,0:T(8,128)S(1)}, f32[512,768]{1,0:T(8,128)S(1)}, f32[512,128]{1,0:T(8,128)S(1)}, f32[512,128]{1,0:T(8,128)S(1)}, /*index=5*/f32[2,768]{1,0:T(2,128)S(1)}) custom-call(bf16[512,768]{1,0:T(8,128)(2,1)S(1)} %get-tuple-element.38.conv_ref, f32[512,128]{1,0:T(8,128)S(1)} %get-tuple-element.39.own_ref, ...), custom_call_target="tpu_custom_call" | custom-call | flops 393216000 | bytes 7352320 | tf_op jit(solution)/shard_map/pallas_call | solution.py:29
  9.1 1.8 %shard_map.132 = (bf16[512,768]{1,0:T(8,128)(2,1)S(1)}, bf16[512,768]{1,0:T(8,128)(2,1)S(1)}, bf16[512,768]{1,0:T(8,128)(2,1)S(1)}, bf16[512,768]{1,0:T(8,128)(2,1)S(1)}) custom-call(bf16[2048,512]{1,0:T(8,128)(2,1)S(1)} %shard_map.131.turned_ref, bf16[512,768]{1,0:T(8,128)(2,1)S(1)} %get-tuple-element.51.active_ref), custom_call_target="tpu_custom_call" | custom-call | flops 1610612736 | bytes 6029312 | tf_op jit(solution)/shard_map/pallas_call | solution.py:29
  10.9 1.6 %collective-permute-start.3 = (bf16[512,768]{1,0:T(8,128)(2,1)S(1)}, bf16[512,768]{1,0:T(8,128)(2,1)S(1)}, u32[]{:S(2)}, u32[]{:S(2)}) collective-permute-start(bf16[512,768]{1,0:T(8,128)(2,1)S(1)} %get-tuple-element.53), channel_id=1, source_target_pairs={{0,2},{1,9},{2,4},{3,11},{4,6},{5,13},{6,0},{7,15},{8,10},{9,17},{... | collective-permute-start | bytes 2359304 | tf_op jit(solution)/shard_map/ppermute | solution.py:367
  12.5 2.7 %collective-permute-start.4 = (bf16[512,768]{1,0:T(8,128)(2,1)S(1)}, bf16[512,768]{1,0:T(8,128)(2,1)S(1)}, u32[]{:S(2)}, u32[]{:S(2)}) collective-permute-start(bf16[512,768]{1,0:T(8,128)(2,1)S(1)} %get-tuple-element.54), channel_id=1, source_target_pairs={{0,4},{1,17},{2,6},{3,19},{4,0},{5,21},{6,2},{7,23},{8,12},{9,25},... | collective-permute-start | bytes 2359304 | tf_op jit(solution)/shard_map/ppermute | solution.py:367
  15.2 1.4 %collective-permute-start.5 = (bf16[512,768]{1,0:T(8,128)(2,1)S(1)}, bf16[512,768]{1,0:T(8,128)(2,1)S(1)}, u32[]{:S(2)}, u32[]{:S(2)}) collective-permute-start(bf16[512,768]{1,0:T(8,128)(2,1)S(1)} %get-tuple-element.55), channel_id=1, source_target_pairs={{0,6},{1,25},{2,0},{3,27},{4,2},{5,29},{6,4},{7,31},{8,14},{9,1},{... | collective-permute-start | bytes 2359304 | tf_op jit(solution)/shard_map/ppermute | solution.py:367
  16.7 1.5 %collective-permute-done.1.sums_peer_ref = f32[512,128]{1,0:T(8,128)S(1)} collective-permute-done((f32[512,128]{1,0:T(8,128)S(1)}, f32[512,128]{1,0:T(8,128)S(1)}, u32[]{:S(2)}, u32[]{:S(2)}) %collective-permute-start.1) | collective-permute-done | bytes 262176 | tf_op jit(solution)/shard_map/ppermute | solution.py:376
  18.2 0.1 shard_map.129
  18.3 3.8 %collective-permute-start.2 = (f32[32,768]{1,0:T(8,128)S(1)}, f32[32,768]{1,0:T(8,128)S(1)}, u32[]{:S(2)}, u32[]{:S(2)}) collective-permute-start(f32[32,768]{1,0:T(8,128)S(1)} %get-tuple-element.47), channel_id=1, source_target_pairs={{2,0},{4,2},{6,4},{8,6},{10,8},{12,10},{14,12},{16,14},{18,16},{20... | collective-permute-start | bytes 294920 | tf_op jit(solution)/shard_map/ppermute | solution.py:379
  22.2 13.4 %collective-permute-done.2.halo_ref = f32[32,768]{1,0:T(8,128)S(1)} collective-permute-done((f32[32,768]{1,0:T(8,128)S(1)}, f32[32,768]{1,0:T(8,128)S(1)}, u32[]{:S(2)}, u32[]{:S(2)}) %collective-permute-start.2) | collective-permute-done | bytes 98336 | tf_op jit(solution)/shard_map/ppermute | solution.py:379
  35.6 6.2 %shard_map.133.refs_4_ = bf16[40,768]{1,0:T(8,128)(2,1)S(1)} custom-call(bf16[512,768]{1,0:T(8,128)(2,1)S(1)} %copy-done, bf16[512,768]{1,0:T(8,128)(2,1)S(1)} %copy-done.1, f32[512,768]{1,0:T(8,128)S(1)} %get-tuple-element.41.lifted_ref, f32[512,768]{1,0:T(8,128)S(1)} %get-tuple-element.42.normed_ref, f32[512,128]{1,0:T(8,128)S(1)} %get-tuple-element.45.mean_ref, ...), custom_call_target="tpu_custom_call" | custom-call | flops 487587840 | bytes 5408768 | tf_op jit(solution)/shard_map/pallas_call | solution.py:29
  41.8 3.7 %collective-permute-start.8 = (bf16[40,768]{1,0:T(8,128)(2,1)S(1)}, bf16[40,768]{1,0:T(8,128)(2,1)S(1)}, u32[]{:S(2)}, u32[]{:S(2)}) collective-permute-start(bf16[40,768]{1,0:T(8,128)(2,1)S(1)} %shard_map.133.refs_4_), channel_id=1, source_target_pairs={{0,6},{1,25},{2,0},{3,27},{4,2},{5,29},{6,4},{7,31},{8,14},{9,1},{... | collective-permute-start | bytes 184328 | tf_op jit(solution)/shard_map/ppermute | solution.py:367
  45.5 0.4 collective-permute-start.7
  45.9 3.6 %collective-permute-done.8.refs_7_ = bf16[40,768]{1,0:T(8,128)(2,1)S(1)} collective-permute-done((bf16[40,768]{1,0:T(8,128)(2,1)S(1)}, bf16[40,768]{1,0:T(8,128)(2,1)S(1)}, u32[]{:S(2)}, u32[]{:S(2)}) %collective-permute-start.8) | collective-permute-done | bytes 61472 | tf_op jit(solution)/shard_map/ppermute | solution.py:367
  49.6 2.3 %collective-permute-start.6 = (bf16[40,768]{1,0:T(8,128)(2,1)S(1)}, bf16[40,768]{1,0:T(8,128)(2,1)S(1)}, u32[]{:S(2)}, u32[]{:S(2)}) collective-permute-start(bf16[40,768]{1,0:T(8,128)(2,1)S(1)} %shard_map.133.refs_4_), channel_id=1, source_target_pairs={{0,2},{1,9},{2,4},{3,11},{4,6},{5,13},{6,0},{7,15},{8,10},{9,17},{... | collective-permute-start | bytes 184328 | tf_op jit(solution)/shard_map/ppermute | solution.py:367
  51.9 3.7 %collective-permute-done.6.refs_5_ = bf16[40,768]{1,0:T(8,128)(2,1)S(1)} collective-permute-done((bf16[40,768]{1,0:T(8,128)(2,1)S(1)}, bf16[40,768]{1,0:T(8,128)(2,1)S(1)}, u32[]{:S(2)}, u32[]{:S(2)}) %collective-permute-start.6) | collective-permute-done | bytes 61472 | tf_op jit(solution)/shard_map/ppermute | solution.py:367
  55.6 0.4 shard_map.134
  56.0 1.3 %collective-permute-start.9 = (bf16[168,768]{1,0:T(8,128)(2,1)S(1)}, bf16[168,768]{1,0:T(8,128)(2,1)S(1)}, u32[]{:S(2)}, u32[]{:S(2)}) collective-permute-start(bf16[168,768]{1,0:T(8,128)(2,1)S(1)} %get-tuple-element.58), channel_id=1, source_target_pairs={{0,8},{1,3},{2,10},{3,5},{4,12},{5,7},{6,14},{7,1},{8,16},{9,11},{... | collective-permute-start | bytes 774152 | tf_op jit(solution)/shard_map/ppermute | solution.py:367
  57.3 2.2 %collective-permute-start.10 = (bf16[168,768]{1,0:T(8,128)(2,1)S(1)}, bf16[168,768]{1,0:T(8,128)(2,1)S(1)}, u32[]{:S(2)}, u32[]{:S(2)}) collective-permute-start(bf16[168,768]{1,0:T(8,128)(2,1)S(1)} %get-tuple-element.59), channel_id=1, source_target_pairs={{0,16},{1,5},{2,18},{3,7},{4,20},{5,1},{6,22},{7,3},{8,24},{9,13},... | collective-permute-start | bytes 774152 | tf_op jit(solution)/shard_map/ppermute | solution.py:367
  59.6 2.9 %collective-permute-done.9.refs_1_ = bf16[168,768]{1,0:T(8,128)(2,1)S(1)} collective-permute-done((bf16[168,768]{1,0:T(8,128)(2,1)S(1)}, bf16[168,768]{1,0:T(8,128)(2,1)S(1)}, u32[]{:S(2)}, u32[]{:S(2)}) %collective-permute-start.9) | collective-permute-done | bytes 258080 | tf_op jit(solution)/shard_map/ppermute | solution.py:367
  62.4 2.8 %collective-permute-done.10.refs_2_ = bf16[168,768]{1,0:T(8,128)(2,1)S(1)} collective-permute-done((bf16[168,768]{1,0:T(8,128)(2,1)S(1)}, bf16[168,768]{1,0:T(8,128)(2,1)S(1)}, u32[]{:S(2)}, u32[]{:S(2)}) %collective-permute-start.10) | collective-permute-done | bytes 258080 | tf_op jit(solution)/shard_map/ppermute | solution.py:367
  65.3 2.7 %collective-permute-done.11.refs_3_ = bf16[168,768]{1,0:T(8,128)(2,1)S(1)} collective-permute-done((bf16[168,768]{1,0:T(8,128)(2,1)S(1)}, bf16[168,768]{1,0:T(8,128)(2,1)S(1)}, u32[]{:S(2)}, u32[]{:S(2)}) %collective-permute-start.11) | collective-permute-done | bytes 258080 | tf_op jit(solution)/shard_map/ppermute | solution.py:367
  68.0 2.0 %collective-permute-start.12 = (bf16[104,768]{1,0:T(8,128)(2,1)S(1)}, bf16[104,768]{1,0:T(8,128)(2,1)S(1)}, u32[]{:S(2)}, u32[]{:S(2)}) collective-permute-start(bf16[104,768]{1,0:T(8,128)(2,1)S(1)} %get-tuple-element.62.sent_ref), channel_id=1, source_target_pairs={{0,32},{32,0},{64,96},{96,64},{128,160},{160,128},{192,224},{224,1... | collective-permute-start | bytes 479240 | tf_op jit(solution)/shard_map/ppermute | solution.py:373
  70.0 3.4 %collective-permute-done.12.came_ref = bf16[104,768]{1,0:T(8,128)(2,1)S(1)} collective-permute-done((bf16[104,768]{1,0:T(8,128)(2,1)S(1)}, bf16[104,768]{1,0:T(8,128)(2,1)S(1)}, u32[]{:S(2)}, u32[]{:S(2)}) %collective-permute-start.12) | collective-permute-done | bytes 159776 | tf_op jit(solution)/shard_map/ppermute | solution.py:373
  73.5 3.3 %collective-permute-start.13 = (bf16[56,768]{1,0:T(8,128)(2,1)S(1)}, bf16[56,768]{1,0:T(8,128)(2,1)S(1)}, u32[]{:S(2)}, u32[]{:S(2)}) collective-permute-start(bf16[56,768]{1,0:T(8,128)(2,1)S(1)} %get-tuple-element.64), channel_id=1, source_target_pairs={{0,64},{32,96},{64,128},{96,160},{128,192},{160,224},{192,0},{224,... | collective-permute-start | bytes 258056 | tf_op jit(solution)/shard_map/ppermute | solution.py:370
  76.8 5.4 %collective-permute-start.14 = (bf16[56,768]{1,0:T(8,128)(2,1)S(1)}, bf16[56,768]{1,0:T(8,128)(2,1)S(1)}, u32[]{:S(2)}, u32[]{:S(2)}) collective-permute-start(bf16[56,768]{1,0:T(8,128)(2,1)S(1)} %get-tuple-element.65), channel_id=1, source_target_pairs={{0,128},{32,160},{64,192},{96,224},{128,0},{160,32},{192,64},{224,... | collective-permute-start | bytes 258056 | tf_op jit(solution)/shard_map/ppermute | solution.py:370
  82.2 2.7 %collective-permute-start.15 = (bf16[56,768]{1,0:T(8,128)(2,1)S(1)}, bf16[56,768]{1,0:T(8,128)(2,1)S(1)}, u32[]{:S(2)}, u32[]{:S(2)}) collective-permute-start(bf16[56,768]{1,0:T(8,128)(2,1)S(1)} %get-tuple-element.66), channel_id=1, source_target_pairs={{0,192},{32,224},{64,0},{96,32},{128,64},{160,96},{192,128},{224,1... | collective-permute-start | bytes 258056 | tf_op jit(solution)/shard_map/ppermute | solution.py:370
  84.9 8.0 %shard_map.130 = (bf16[512,768]{1,0:T(8,128)(2,1)}, bf16[512,768]{1,0:T(8,128)(2,1)}) custom-call(bf16[512,768]{1,0:T(8,128)(2,1)S(1)} %copy-done, bf16[512,768]{1,0:T(8,128)(2,1)S(1)} %copy-done.1, f32[512,768]{1,0:T(8,128)S(1)} %get-tuple-element.41.lifted_ref, f32[512,768]{1,0:T(8,128)S(1)} %get-tuple-element.42.normed_ref, ...), custom_call_target="tpu_custom_call" | custom-call | flops 487587840 | bytes 6961664 | tf_op jit(solution)/shard_map/pallas_call | solution.py:29
  92.9 0.7 shard_map.137
  93.6 0.6 slice_reduce_fusion
  (23 shorter events, 0.4 us)
Async XLA Ops:
  5.8 1.6 %collective-permute-start = (f32[512,128]{1,0:T(8,128)S(1)}, f32[512,128]{1,0:T(8,128)S(1)}, u32[]{:S(2)}, u32[]{:S(2)}) collective-permute-start(f32[512,128]{1,0:T(8,128)S(1)} %get-tuple-element.39.own_ref), channel_id=1, source_target_pairs={{0,1},{1,0},{2,3},{3,2},{4,5},{5,4},{6,7},{7,6},{8,9},{9,8},{10,11... | collective-permute-start | bytes 786440 | tf_op jit(solution)/shard_map/ppermute | solution.py:376
  5.9 1.5 %copy-start.3 = (f32[768]{0:T(1024)S(1)}, f32[768]{0:T(1024)}, u32[]{:S(2)}) copy-start(f32[768]{0:T(1024)} %gain_ref.1) | copy-start | bytes 9220
  6.0 1.5 %copy-start.4 = (f32[768]{0:T(1024)S(1)}, f32[768]{0:T(1024)}, u32[]{:S(2)}) copy-start(f32[768]{0:T(1024)} %shift_ref.1) | copy-start | bytes 9220
  10.9 24.7 %copy-start = (bf16[512,768]{1,0:T(8,128)(2,1)S(1)}, bf16[512,768]{1,0:T(8,128)(2,1)}, u32[]{:S(2)}) copy-start(bf16[512,768]{1,0:T(8,128)(2,1)} %value_ref.3) | copy-start | bytes 2359300
  10.9 24.7 %copy-start.1 = (bf16[512,768]{1,0:T(8,128)(2,1)S(1)}, bf16[512,768]{1,0:T(8,128)(2,1)}, u32[]{:S(2)}) copy-start(bf16[512,768]{1,0:T(8,128)(2,1)} %gate_ref.3) | copy-start | bytes 2359300
  10.9 44.7 %collective-permute-start.3 = (bf16[512,768]{1,0:T(8,128)(2,1)S(1)}, bf16[512,768]{1,0:T(8,128)(2,1)S(1)}, u32[]{:S(2)}, u32[]{:S(2)}) collective-permute-start(bf16[512,768]{1,0:T(8,128)(2,1)S(1)} %get-tuple-element.53), channel_id=1, source_target_pairs={{0,2},{1,9},{2,4},{3,11},{4,6},{5,13},{6,0},{7,15},{8,10},{9,17},{... | collective-permute-start | bytes 2359304 | tf_op jit(solution)/shard_map/ppermute | solution.py:367
  12.5 43.1 %collective-permute-start.4 = (bf16[512,768]{1,0:T(8,128)(2,1)S(1)}, bf16[512,768]{1,0:T(8,128)(2,1)S(1)}, u32[]{:S(2)}, u32[]{:S(2)}) collective-permute-start(bf16[512,768]{1,0:T(8,128)(2,1)S(1)} %get-tuple-element.54), channel_id=1, source_target_pairs={{0,4},{1,17},{2,6},{3,19},{4,0},{5,21},{6,2},{7,23},{8,12},{9,25},... | collective-permute-start | bytes 2359304 | tf_op jit(solution)/shard_map/ppermute | solution.py:367
  15.2 40.4 %collective-permute-start.5 = (bf16[512,768]{1,0:T(8,128)(2,1)S(1)}, bf16[512,768]{1,0:T(8,128)(2,1)S(1)}, u32[]{:S(2)}, u32[]{:S(2)}) collective-permute-start(bf16[512,768]{1,0:T(8,128)(2,1)S(1)} %get-tuple-element.55), channel_id=1, source_target_pairs={{0,6},{1,25},{2,0},{3,27},{4,2},{5,29},{6,4},{7,31},{8,14},{9,1},{... | collective-permute-start | bytes 2359304 | tf_op jit(solution)/shard_map/ppermute | solution.py:367
  16.7 1.5 %collective-permute-start.1 = (f32[512,128]{1,0:T(8,128)S(1)}, f32[512,128]{1,0:T(8,128)S(1)}, u32[]{:S(2)}, u32[]{:S(2)}) collective-permute-start(f32[512,128]{1,0:T(8,128)S(1)} %get-tuple-element.44.sums_ref), channel_id=1, source_target_pairs={{0,1},{1,0},{2,3},{3,2},{4,5},{5,4},{6,7},{7,6},{8,9},{9,8},{10,11... | collective-permute-start | bytes 786440 | tf_op jit(solution)/shard_map/ppermute | solution.py:376
  18.3 17.3 %collective-permute-start.2 = (f32[32,768]{1,0:T(8,128)S(1)}, f32[32,768]{1,0:T(8,128)S(1)}, u32[]{:S(2)}, u32[]{:S(2)}) collective-permute-start(f32[32,768]{1,0:T(8,128)S(1)} %get-tuple-element.47), channel_id=1, source_target_pairs={{2,0},{4,2},{6,4},{8,6},{10,8},{12,10},{14,12},{16,14},{18,16},{20... | collective-permute-start | bytes 294920 | tf_op jit(solution)/shard_map/ppermute | solution.py:379
  41.8 7.7 %collective-permute-start.8 = (bf16[40,768]{1,0:T(8,128)(2,1)S(1)}, bf16[40,768]{1,0:T(8,128)(2,1)S(1)}, u32[]{:S(2)}, u32[]{:S(2)}) collective-permute-start(bf16[40,768]{1,0:T(8,128)(2,1)S(1)} %shard_map.133.refs_4_), channel_id=1, source_target_pairs={{0,6},{1,25},{2,0},{3,27},{4,2},{5,29},{6,4},{7,31},{8,14},{9,1},{... | collective-permute-start | bytes 184328 | tf_op jit(solution)/shard_map/ppermute | solution.py:367
  45.5 6.4 %collective-permute-start.7 = (bf16[40,768]{1,0:T(8,128)(2,1)S(1)}, bf16[40,768]{1,0:T(8,128)(2,1)S(1)}, u32[]{:S(2)}, u32[]{:S(2)}) collective-permute-start(bf16[40,768]{1,0:T(8,128)(2,1)S(1)} %shard_map.133.refs_4_), channel_id=1, source_target_pairs={{0,4},{1,17},{2,6},{3,19},{4,0},{5,21},{6,2},{7,23},{8,12},{9,25},... | collective-permute-start | bytes 184328 | tf_op jit(solution)/shard_map/ppermute | solution.py:367
  49.6 6.0 %collective-permute-start.6 = (bf16[40,768]{1,0:T(8,128)(2,1)S(1)}, bf16[40,768]{1,0:T(8,128)(2,1)S(1)}, u32[]{:S(2)}, u32[]{:S(2)}) collective-permute-start(bf16[40,768]{1,0:T(8,128)(2,1)S(1)} %shard_map.133.refs_4_), channel_id=1, source_target_pairs={{0,2},{1,9},{2,4},{3,11},{4,6},{5,13},{6,0},{7,15},{8,10},{9,17},{... | collective-permute-start | bytes 184328 | tf_op jit(solution)/shard_map/ppermute | solution.py:367
  55.6 29.3 %copy-start.2 = (bf16[31,768]{1,0:T(8,128)(2,1)S(1)}, bf16[31,768]{1,0:T(8,128)(2,1)}, u32[]{:S(2)}) copy-start(bf16[31,768]{1,0:T(8,128)(2,1)} %taps_ref.1) | copy-start | bytes 142852
  56.0 6.4 %collective-permute-start.9 = (bf16[168,768]{1,0:T(8,128)(2,1)S(1)}, bf16[168,768]{1,0:T(8,128)(2,1)S(1)}, u32[]{:S(2)}, u32[]{:S(2)}) collective-permute-start(bf16[168,768]{1,0:T(8,128)(2,1)S(1)} %get-tuple-element.58), channel_id=1, source_target_pairs={{0,8},{1,3},{2,10},{3,5},{4,12},{5,7},{6,14},{7,1},{8,16},{9,11},{... | collective-permute-start | bytes 774152 | tf_op jit(solution)/shard_map/ppermute | solution.py:367
  57.3 7.9 %collective-permute-start.10 = (bf16[168,768]{1,0:T(8,128)(2,1)S(1)}, bf16[168,768]{1,0:T(8,128)(2,1)S(1)}, u32[]{:S(2)}, u32[]{:S(2)}) collective-permute-start(bf16[168,768]{1,0:T(8,128)(2,1)S(1)} %get-tuple-element.59), channel_id=1, source_target_pairs={{0,16},{1,5},{2,18},{3,7},{4,20},{5,1},{6,22},{7,3},{8,24},{9,13},... | collective-permute-start | bytes 774152 | tf_op jit(solution)/shard_map/ppermute | solution.py:367
  59.6 8.4 %collective-permute-start.11 = (bf16[168,768]{1,0:T(8,128)(2,1)S(1)}, bf16[168,768]{1,0:T(8,128)(2,1)S(1)}, u32[]{:S(2)}, u32[]{:S(2)}) collective-permute-start(bf16[168,768]{1,0:T(8,128)(2,1)S(1)} %get-tuple-element.60), channel_id=1, source_target_pairs={{0,24},{1,7},{2,26},{3,1},{4,28},{5,3},{6,30},{7,5},{8,0},{9,15},{... | collective-permute-start | bytes 774152 | tf_op jit(solution)/shard_map/ppermute | solution.py:367
  68.0 5.4 %collective-permute-start.12 = (bf16[104,768]{1,0:T(8,128)(2,1)S(1)}, bf16[104,768]{1,0:T(8,128)(2,1)S(1)}, u32[]{:S(2)}, u32[]{:S(2)}) collective-permute-start(bf16[104,768]{1,0:T(8,128)(2,1)S(1)} %get-tuple-element.62.sent_ref), channel_id=1, source_target_pairs={{0,32},{32,0},{64,96},{96,64},{128,160},{160,128},{192,224},{224,1... | collective-permute-start | bytes 479240 | tf_op jit(solution)/shard_map/ppermute | solution.py:373
  73.5 19.4 %collective-permute-start.13 = (bf16[56,768]{1,0:T(8,128)(2,1)S(1)}, bf16[56,768]{1,0:T(8,128)(2,1)S(1)}, u32[]{:S(2)}, u32[]{:S(2)}) collective-permute-start(bf16[56,768]{1,0:T(8,128)(2,1)S(1)} %get-tuple-element.64), channel_id=1, source_target_pairs={{0,64},{32,96},{64,128},{96,160},{128,192},{160,224},{192,0},{224,... | collective-permute-start | bytes 258056 | tf_op jit(solution)/shard_map/ppermute | solution.py:370
  76.8 16.1 %collective-permute-start.14 = (bf16[56,768]{1,0:T(8,128)(2,1)S(1)}, bf16[56,768]{1,0:T(8,128)(2,1)S(1)}, u32[]{:S(2)}, u32[]{:S(2)}) collective-permute-start(bf16[56,768]{1,0:T(8,128)(2,1)S(1)} %get-tuple-element.65), channel_id=1, source_target_pairs={{0,128},{32,160},{64,192},{96,224},{128,0},{160,32},{192,64},{224,... | collective-permute-start | bytes 258056 | tf_op jit(solution)/shard_map/ppermute | solution.py:370
  82.2 10.7 %collective-permute-start.15 = (bf16[56,768]{1,0:T(8,128)(2,1)S(1)}, bf16[56,768]{1,0:T(8,128)(2,1)S(1)}, u32[]{:S(2)}, u32[]{:S(2)}) collective-permute-start(bf16[56,768]{1,0:T(8,128)(2,1)S(1)} %get-tuple-element.66), channel_id=1, source_target_pairs={{0,192},{32,224},{64,0},{96,32},{128,64},{160,96},{192,128},{224,1... | collective-permute-start | bytes 258056 | tf_op jit(solution)/shard_map/ppermute | solution.py:370

commit v2 on v1

--- a/solution.py
+++ b/solution.py
@@ -57,13 +57,19 @@
 
 def front_kernel(
     place_ref, conv_hbm, grad_hbm, weight_hbm, stats_ref, act_grad_ref, conv_ref, grad_ref,
-    weight_ref, conv_sem, grad_sem, weight_sem,
+    weight_ref, conv_sem, grad_sem, weight_sems,
 ):
+    parts = weight_sems.shape[0]
+    wide = weight_ref.shape[1] // parts
+    columns = [slice(k * wide, (k + 1) * wide) for k in range(parts)]
     loads = [
         pltpu.make_async_copy(conv_hbm, conv_ref, conv_sem),
-        pltpu.make_async_copy(weight_hbm, weight_ref, weight_sem),
         pltpu.make_async_copy(grad_hbm, grad_ref, grad_sem),
     ]
+    for k, c in enumerate(columns):
+        loads.append(
+            pltpu.make_async_copy(weight_hbm.at[:, c], weight_ref.at[:, c], weight_sems.at[k])
+        )
     for load in loads:
         load.start()
     loads[0].wait()
@@ -81,9 +87,10 @@
             off = conv_ref[at, c].astype(F32) - mean
             spread = spread + off * off
         stats_ref[at, :] = jnp.where(left, total, jnp.sum(spread, axis=1, keepdims=True))
-    for load in loads[1:]:
+    loads[1].wait()
+    for load, c in zip(loads[2:], columns):
         load.wait()
-    act_grad_ref[...] = jnp.dot(grad_ref[...], weight_ref[...], preferred_element_type=F32)
+        act_grad_ref[:, c] = jnp.dot(grad_ref[...], weight_ref[:, c], preferred_element_type=F32)
 
 
 def turn_kernel(place_ref, grad_ref, turned_ref):
@@ -188,23 +195,25 @@
         head_ref[at, c] = lifted_ref[at, c] - mean_ref[at, :] - normed_ref[at, c] * slope_ref[at, :]
 
 
-def fill_moved(moved, lanes, lifted_ref, normed_ref, mean_ref, slope_ref, halo_ref):
+def fill_heights(heights, lanes, lifted_ref, normed_ref, mean_ref, slope_ref, halo_ref):
     rows = lifted_ref.shape[0]
     tail = halo_ref.shape[0]
-    moved[0, 0:rows, :] = (
+    heights[0:rows, :] = (
         lifted_ref[:, lanes] - mean_ref[...] - normed_ref[:, lanes] * slope_ref[...]
     )
-    moved[0, rows : rows + tail, :] = halo_ref[:, lanes]
-    for s in range(1, 8):
-        moved[s, 0 : rows + tail - 8, :] = moved[0, s : s + rows + tail - 8, :]
-
-
-def strips(body, chans):
+    heights[rows : rows + tail, :] = halo_ref[:, lanes]
+
+
+def strips(body, begin, end):
     def step(i, carry):
-        body(pl.ds(pl.multiple_of(i * LANES, LANES), LANES))
+        body(i * LANES)
         return carry
 
-    lax.fori_loop(0, chans // LANES, step, 0)
+    lax.fori_loop(begin // LANES, end // LANES, step, 0)
+
+
+def lanes_at(at):
+    return pl.ds(pl.multiple_of(at, LANES), LANES)
 
 
 GROUP = 4
@@ -212,7 +221,7 @@
 
 def taps_kernel(
     value_ref, gate_ref, lifted_ref, normed_ref, mean_ref, slope_ref, halo_ref, params_ref,
-    out_ref, moved, gated, rows_ref,
+    out_ref, heights, gated, rows_ref,
 ):
     rows, chans = value_ref.shape
     taps = halo_ref.shape[0] - 1
@@ -220,7 +229,7 @@
     step = 8 * GROUP
 
     def one(lanes):
-        fill_moved(moved, lanes, lifted_ref, normed_ref, mean_ref, slope_ref, halo_ref)
+        fill_heights(heights, lanes, lifted_ref, normed_ref, mean_ref, slope_ref, halo_ref)
         sig = jax.nn.sigmoid(gate_ref[:, lanes].astype(F32))
         gated[...] = (value_ref[:, lanes].astype(F32) * sig).astype(BF16).astype(F32)
 
@@ -231,7 +240,7 @@
             for s in range(8):
                 overs = range(s, taps, 8)
                 there = [
-                    moved[s, pl.ds(at + 8 * m, 8), :] for m in range(GROUP + len(overs) - 1)
+                    heights[pl.ds(at + (8 * m + s), 8), :] for m in range(GROUP + len(overs) - 1)
                 ]
                 for q, over in enumerate(overs):
                     j = reach - over
@@ -247,20 +256,21 @@
         rows_ref[taps + 2 :, :] = jnp.zeros((rows_ref.shape[0] - taps - 2, LANES), F32)
         out_ref[:, lanes] = rows_ref[...].astype(BF16)
 
-    strips(one, chans)
+    strips(lambda at: one(lanes_at(at)), 0, chans)
 
 
 def spread_kernel(
-    value_ref, gate_ref, lifted_ref, normed_ref, mean_ref, slope_ref, halo_ref, taps_ref,
-    grad_value_ref, grad_gate_ref, moved, spread,
+    begin, value_ref, gate_ref, lifted_ref, normed_ref, mean_ref, slope_ref, halo_ref, taps_ref, *refs
 ):
-    rows, chans = value_ref.shape
+    grad_value_ref, grad_gate_ref, heights, spread = refs[-4:]
+    rows = value_ref.shape[0]
     taps = taps_ref.shape[0]
     reach = taps - 1
     step = 8 * GROUP
 
-    def one(lanes):
-        fill_moved(moved, lanes, lifted_ref, normed_ref, mean_ref, slope_ref, halo_ref)
+    def one(at_lane):
+        lanes, there_lanes = lanes_at(at_lane), lanes_at(at_lane - begin)
+        fill_heights(heights, lanes, lifted_ref, normed_ref, mean_ref, slope_ref, halo_ref)
         weights = taps_ref[:, lanes].astype(F32)
         for j in range(taps):
             spread[j] = jnp.broadcast_to(weights[j : j + 1, :], (8, LANES))
@@ -271,7 +281,7 @@
             for s in range(8):
                 overs = range(s, taps, 8)
                 there = [
-                    moved[s, pl.ds(at + 8 * m, 8), :] for m in range(GROUP + len(overs) - 1)
+                    heights[pl.ds(at + (8 * m + s), 8), :] for m in range(GROUP + len(overs) - 1)
                 ]
                 for q, over in enumerate(overs):
                     weight = spread[reach - over]
@@ -282,15 +292,15 @@
             gated_grad = jnp.concatenate(total, axis=0)
             sig = jax.nn.sigmoid(gate_ref[here, lanes].astype(F32))
             grad_value = gated_grad * sig
-            grad_value_ref[here, lanes] = grad_value.astype(BF16)
-            grad_gate_ref[here, lanes] = (
+            grad_value_ref[here, there_lanes] = grad_value.astype(BF16)
+            grad_gate_ref[here, there_lanes] = (
                 grad_value * value_ref[here, lanes].astype(F32) * (1.0 - sig)
             ).astype(BF16)
             return carry
 
         lax.fori_loop(0, rows // step, body, 0)
 
-    strips(one, chans)
+    strips(one, begin, begin + grad_value_ref.shape[1])
 
 
 def added(refs, at=slice(None)):
@@ -324,12 +334,13 @@
 
 
 def last_kernel(taps, *refs):
-    landed, (project_ref, taps_ref, params_ref) = refs[:-3], refs[-3:]
+    landed, (project_ref, taps_ref, gain_ref, shift_ref) = refs[:-4], refs[-4:]
     own = project_ref.shape[0]
     total = added(landed)
     project_ref[...] = total[:own, :]
     taps_ref[...] = total[own : own + taps, :]
-    params_ref[...] = total[own + taps : own + taps + 2, :]
+    gain_ref[...] = total[own + taps, :]
+    shift_ref[...] = total[own + taps + 1, :]
 
 
 def local(conv_value, conv_gate, conv_out, conv_taps, norm_gain, norm_shift, proj_weight, out_grad):
@@ -386,7 +397,12 @@
         ),
         place, *(pltpu.with_memory_space_constraint(a, pltpu.HBM) for a in (conv_out, out_grad, proj_weight)),
         flops=2 * rows * width * chans,
-        scratch=[pltpu.VMEM(proj_weight.shape, BF16)] + [pltpu.SemaphoreType.DMA] * 3,
+        scratch=[
+            pltpu.VMEM(proj_weight.shape, BF16),
+            pltpu.SemaphoreType.DMA,
+            pltpu.SemaphoreType.DMA,
+            pltpu.SemaphoreType.DMA((3,)),
+        ],
         specs=[pl.BlockSpec(memory_space=pltpu.SMEM)] + [pl.BlockSpec(memory_space=pltpu.HBM)] * 3,
         limit=12,
     )
@@ -430,17 +446,34 @@
         (shape((extra, chans), BF16),),
         conv_value, conv_gate, *heights, params,
         flops=taps * rows * chans * 40,
-        scratch=[pltpu.VMEM((8, rows + tail, LANES), F32), pltpu.VMEM((rows, LANES), F32),
+        scratch=[pltpu.VMEM((rows + tail, LANES), F32), pltpu.VMEM((rows, LANES), F32),
             pltpu.VMEM((extra, LANES), F32),
         ],
     )
-    grad_value, grad_gate = call(
-        spread_kernel,
-        (shape((rows, chans), BF16),) * 2,
-        conv_value, conv_gate, *heights, conv_taps,
-        flops=taps * rows * chans * 40,
-        scratch=[pltpu.VMEM((8, rows + tail, LANES), F32), pltpu.VMEM((taps, 8, LANES), F32)],
-    )
+
+    def spread_part(part, before):
+        half = chans // 2
+        operands = (conv_value, conv_gate, *heights, conv_taps)
+        block = pl.BlockSpec((rows, half), lambda i: (0, part))
+        return pl.pallas_call(
+            functools.partial(spread_kernel, part * half),
+            grid=(1,),
+            out_shape=(shape((rows, chans), BF16),) * 2,
+            in_specs=vmem(len(operands)) + [pl.BlockSpec(memory_space=pl.ANY)] * len(before),
+            out_specs=(block, block),
+            input_output_aliases={len(operands) + k: k for k in range(len(before))},
+            scratch_shapes=[
+                pltpu.VMEM((rows + tail, LANES), F32), pltpu.VMEM((taps, 8, LANES), F32),
+            ],
+            cost_estimate=pl.CostEstimate(
+                flops=taps * rows * chans * 20, bytes_accessed=rows * chans * 10, transcendentals=0
+            ),
+            compiler_params=pltpu.CompilerParams(vmem_limit_bytes=8 * MIB),
+            name="spread",
+        )(*operands, *before)
+
+    halves = spread_part(0, ())
+    grad_value, grad_gate = spread_part(1, halves)
     smalls = [small] + [hop(small, k, 1) for k in range(1, n)]
     part = width // (n * n)
     second = call(
@@ -464,13 +497,13 @@
         flops=width * chans * 10,
     )
     fars = [fourth[0]] + [hop_z(fourth[k], 2 * k) for k in range(1, nz // 2)]
-    grad_proj, grad_taps, grad_params = call(
+    grad_proj, grad_taps, grad_gain, grad_shift = call(
         functools.partial(last_kernel, taps),
-        (shape((own, chans), F32), shape((taps, chans), F32), shape((2, chans), F32)),
+        (shape((own, chans), F32), shape((taps, chans), F32), shape((chans,), F32), shape((chans,), F32)),
         *fars,
         flops=width * chans * 10,
     )
-    return grad_value, grad_gate, grad_taps, grad_params[0], grad_params[1], grad_proj
+    return grad_value, grad_gate, grad_taps, grad_gain, grad_shift, grad_proj
 
 
 def solution(mesh):

time: 94.3 us -> 91.4 us (0.969)
  the two profiles are of different devices: /device:TPU:8 before, /device:TPU:4 now
where the time goes in v2:
time: 91.4 us; the launch traced here: 91.3 us
  waiting for transfers between devices  35.5 us (39%)
  starting transfers between devices  29.5 us (32%)
  Pallas kernels  25.5 us (28%)
    pallas_call x10, Pallas kernels, call(): pl.pallas_call(kernel, out_shape=outs, in_specs=specs or vmem(len(args)),...  17.7 us
    ppermute x1, waiting for transfers between devices, previous(): return lax.ppermute(array, SP, [(i, i - 1) for i in range(1, nz * n * n)])  15.6 us
    ppermute x9, starting transfers between devices, hop(): return lax.ppermute(array, ALL, [(index(*at), to(*at)) for at in places])  14.6 us
    ppermute x9, waiting for transfers between devices, hop(): return lax.ppermute(array, ALL, [(index(*at), to(*at)) for at in places])  13.7 us
    ppermute x3, starting transfers between devices, hop_z(): return lax.ppermute(array, 'sp_0', [(i, (i + k) % nz) for i in range(nz)])  9.91 us
    pallas_call x2, Pallas kernels, spread_part(): pl.pallas_call(functools.partial(spread_kernel, part * half), grid=(1,),...  7.79 us
    ppermute x1, waiting for transfers between devices, swap_z(): return lax.ppermute(array, 'sp_0', [(i, i ^ 1) for i in range(nz)])  4.85 us
    ppermute x1, starting transfers between devices, previous(): return lax.ppermute(array, SP, [(i, i - 1) for i in range(1, nz * n * n)])  2.44 us
  transfers between devices with their start and end apart: 16, of which 9 were waited for; matrix products, arithmetic and copies ran while one was open for 0% of the time, Pallas kernels for 16%

profile of v2, /device:TPU:4, one launch (start us, length us, event | category | flops | bytes accessed | tf_op | source)
XLA Modules:
  0.0 91.3 jit_solution(4019717001571173871)
XLA Ops:
  0.7 6.3 %shard_map.127 = (f32[512,128]{1,0:T(8,128)S(1)}, f32[512,768]{1,0:T(8,128)S(1)}, bf16[512,768]{1,0:T(8,128)(2,1)S(1)}, bf16[512,2048]{1,0:T(8,128)(2,1)S(1)}) custom-call(s32[128]{0:T(128)S(1)} %add_multiply_fusion.place_ref, bf16[512,768]{1,0:T(8,128)(2,1)} %conv_hbm.1, bf16[512,2048]{1,0:T(8,128)(2,1)} %grad_hbm.1, bf16[2048,768]{1,0:T(8,128)(2,1)} %weight_hbm.1), custom_call_target="tpu_custom_call" | custom-call | flops 1610612736 | bytes 10748416 | tf_op jit(solution)/shard_map/pallas_call | solution.py:29
  7.1 1.3 %shard_map.130.turned_ref = bf16[2048,512]{1,0:T(8,128)(2,1)S(1)} custom-call(s32[128]{0:T(128)S(1)} %add_multiply_fusion.place_ref, bf16[512,2048]{1,0:T(8,128)(2,1)S(1)} %get-tuple-element.55.grad_ref), custom_call_target="tpu_custom_call" | custom-call | flops 805306368 | bytes 4194816 | tf_op jit(solution)/shard_map/pallas_call | solution.py:29
  8.6 1.6 %shard_map.128 = (bf16[512,768]{1,0:T(8,128)(2,1)S(1)}, f32[512,768]{1,0:T(8,128)S(1)}, f32[512,768]{1,0:T(8,128)S(1)}, f32[512,128]{1,0:T(8,128)S(1)}, f32[512,128]{1,0:T(8,128)S(1)}, /*index=5*/f32[2,768]{1,0:T(2,128)S(1)}) custom-call(bf16[512,768]{1,0:T(8,128)(2,1)S(1)} %get-tuple-element.41.conv_ref, f32[512,128]{1,0:T(8,128)S(1)} %get-tuple-element.42.own_ref, ...), custom_call_target="tpu_custom_call" | custom-call | flops 393216000 | bytes 7352320 | tf_op jit(solution)/shard_map/pallas_call | solution.py:29
  10.2 1.8 %shard_map.131 = (bf16[512,768]{1,0:T(8,128)(2,1)S(1)}, bf16[512,768]{1,0:T(8,128)(2,1)S(1)}, bf16[512,768]{1,0:T(8,128)(2,1)S(1)}, bf16[512,768]{1,0:T(8,128)(2,1)S(1)}) custom-call(bf16[2048,512]{1,0:T(8,128)(2,1)S(1)} %shard_map.130.turned_ref, bf16[512,768]{1,0:T(8,128)(2,1)S(1)} %get-tuple-element.56.active_ref), custom_call_target="tpu_custom_call" | custom-call | flops 1610612736 | bytes 6029312 | tf_op jit(solution)/shard_map/pallas_call | solution.py:29
  12.0 1.3 %collective-permute-start.3 = (bf16[512,768]{1,0:T(8,128)(2,1)S(1)}, bf16[512,768]{1,0:T(8,128)(2,1)S(1)}, u32[]{:S(2)}, u32[]{:S(2)}) collective-permute-start(bf16[512,768]{1,0:T(8,128)(2,1)S(1)} %get-tuple-element.58), channel_id=1, source_target_pairs={{0,2},{1,9},{2,4},{3,11},{4,6},{5,13},{6,0},{7,15},{8,10},{9,17},{... | collective-permute-start | bytes 2359304 | tf_op jit(solution)/shard_map/ppermute | solution.py:378
  13.3 1.1 %collective-permute-start.4 = (bf16[512,768]{1,0:T(8,128)(2,1)S(1)}, bf16[512,768]{1,0:T(8,128)(2,1)S(1)}, u32[]{:S(2)}, u32[]{:S(2)}) collective-permute-start(bf16[512,768]{1,0:T(8,128)(2,1)S(1)} %get-tuple-element.59), channel_id=1, source_target_pairs={{0,4},{1,17},{2,6},{3,19},{4,0},{5,21},{6,2},{7,23},{8,12},{9,25},... | collective-permute-start | bytes 2359304 | tf_op jit(solution)/shard_map/ppermute | solution.py:378
  14.4 2.5 %collective-permute-start.5 = (bf16[512,768]{1,0:T(8,128)(2,1)S(1)}, bf16[512,768]{1,0:T(8,128)(2,1)S(1)}, u32[]{:S(2)}, u32[]{:S(2)}) collective-permute-start(bf16[512,768]{1,0:T(8,128)(2,1)S(1)} %get-tuple-element.60), channel_id=1, source_target_pairs={{0,6},{1,25},{2,0},{3,27},{4,2},{5,29},{6,4},{7,31},{8,14},{9,1},{... | collective-permute-start | bytes 2359304 | tf_op jit(solution)/shard_map/ppermute | solution.py:378
  17.0 0.5 collective-permute-start.1
  17.4 1.2 %collective-permute-done.1.sums_peer_ref = f32[512,128]{1,0:T(8,128)S(1)} collective-permute-done((f32[512,128]{1,0:T(8,128)S(1)}, f32[512,128]{1,0:T(8,128)S(1)}, u32[]{:S(2)}, u32[]{:S(2)}) %collective-permute-start.1) | collective-permute-done | bytes 262176 | tf_op jit(solution)/shard_map/ppermute | solution.py:387
  18.7 2.4 %collective-permute-start.2 = (f32[32,768]{1,0:T(8,128)S(1)}, f32[32,768]{1,0:T(8,128)S(1)}, u32[]{:S(2)}, u32[]{:S(2)}) collective-permute-start(f32[32,768]{1,0:T(8,128)S(1)} %get-tuple-element.50), channel_id=1, source_target_pairs={{2,0},{4,2},{6,4},{8,6},{10,8},{12,10},{14,12},{16,14},{18,16},{20... | collective-permute-start | bytes 294920 | tf_op jit(solution)/shard_map/ppermute | solution.py:390
  21.2 15.6 %collective-permute-done.2.halo_ref = f32[32,768]{1,0:T(8,128)S(1)} collective-permute-done((f32[32,768]{1,0:T(8,128)S(1)}, f32[32,768]{1,0:T(8,128)S(1)}, u32[]{:S(2)}, u32[]{:S(2)}) %collective-permute-start.2) | collective-permute-done | bytes 98336 | tf_op jit(solution)/shard_map/ppermute | solution.py:390
  36.8 5.2 %shard_map.132.refs_4_ = bf16[40,768]{1,0:T(8,128)(2,1)S(1)} custom-call(bf16[512,768]{1,0:T(8,128)(2,1)S(1)} %copy-done, bf16[512,768]{1,0:T(8,128)(2,1)S(1)} %copy-done.1, f32[512,768]{1,0:T(8,128)S(1)} %get-tuple-element.44.lifted_ref, f32[512,768]{1,0:T(8,128)S(1)} %get-tuple-element.45.normed_ref, f32[512,128]{1,0:T(8,128)S(1)} %get-tuple-element.48.mean_ref, ...), custom_call_target="tpu_custom_call" | custom-call | flops 487587840 | bytes 5408768 | tf_op jit(solution)/shard_map/pallas_call | solution.py:29
  42.0 2.2 %collective-permute-start.6 = (bf16[40,768]{1,0:T(8,128)(2,1)S(1)}, bf16[40,768]{1,0:T(8,128)(2,1)S(1)}, u32[]{:S(2)}, u32[]{:S(2)}) collective-permute-start(bf16[40,768]{1,0:T(8,128)(2,1)S(1)} %shard_map.132.refs_4_), channel_id=1, source_target_pairs={{0,2},{1,9},{2,4},{3,11},{4,6},{5,13},{6,0},{7,15},{8,10},{9,17},{... | collective-permute-start | bytes 184328 | tf_op jit(solution)/shard_map/ppermute | solution.py:378
  44.2 2.1 %collective-permute-start.7 = (bf16[40,768]{1,0:T(8,128)(2,1)S(1)}, bf16[40,768]{1,0:T(8,128)(2,1)S(1)}, u32[]{:S(2)}, u32[]{:S(2)}) collective-permute-start(bf16[40,768]{1,0:T(8,128)(2,1)S(1)} %shard_map.132.refs_4_), channel_id=1, source_target_pairs={{0,4},{1,17},{2,6},{3,19},{4,0},{5,21},{6,2},{7,23},{8,12},{9,25},... | collective-permute-start | bytes 184328 | tf_op jit(solution)/shard_map/ppermute | solution.py:378
  46.3 2.8 %collective-permute-done.6.refs_5_ = bf16[40,768]{1,0:T(8,128)(2,1)S(1)} collective-permute-done((bf16[40,768]{1,0:T(8,128)(2,1)S(1)}, bf16[40,768]{1,0:T(8,128)(2,1)S(1)}, u32[]{:S(2)}, u32[]{:S(2)}) %collective-permute-start.6) | collective-permute-done | bytes 61472 | tf_op jit(solution)/shard_map/ppermute | solution.py:378
  49.1 0.5 collective-permute-start.8
  49.6 0.9 %collective-permute-done.7.refs_6_ = bf16[40,768]{1,0:T(8,128)(2,1)S(1)} collective-permute-done((bf16[40,768]{1,0:T(8,128)(2,1)S(1)}, bf16[40,768]{1,0:T(8,128)(2,1)S(1)}, u32[]{:S(2)}, u32[]{:S(2)}) %collective-permute-start.7) | collective-permute-done | bytes 61472 | tf_op jit(solution)/shard_map/ppermute | solution.py:378
  50.5 2.8 %collective-permute-done.8.refs_7_ = bf16[40,768]{1,0:T(8,128)(2,1)S(1)} collective-permute-done((bf16[40,768]{1,0:T(8,128)(2,1)S(1)}, bf16[40,768]{1,0:T(8,128)(2,1)S(1)}, u32[]{:S(2)}, u32[]{:S(2)}) %collective-permute-start.8) | collective-permute-done | bytes 61472 | tf_op jit(solution)/shard_map/ppermute | solution.py:378
  53.4 0.4 shard_map.133
  53.8 2.4 %collective-permute-start.10 = (bf16[168,768]{1,0:T(8,128)(2,1)S(1)}, bf16[168,768]{1,0:T(8,128)(2,1)S(1)}, u32[]{:S(2)}, u32[]{:S(2)}) collective-permute-start(bf16[168,768]{1,0:T(8,128)(2,1)S(1)} %get-tuple-element.64), channel_id=1, source_target_pairs={{0,16},{1,5},{2,18},{3,7},{4,20},{5,1},{6,22},{7,3},{8,24},{9,13},... | collective-permute-start | bytes 774152 | tf_op jit(solution)/shard_map/ppermute | solution.py:378
  56.2 1.7 %collective-permute-start.11 = (bf16[168,768]{1,0:T(8,128)(2,1)S(1)}, bf16[168,768]{1,0:T(8,128)(2,1)S(1)}, u32[]{:S(2)}, u32[]{:S(2)}) collective-permute-start(bf16[168,768]{1,0:T(8,128)(2,1)S(1)} %get-tuple-element.65), channel_id=1, source_target_pairs={{0,24},{1,7},{2,26},{3,1},{4,28},{5,3},{6,30},{7,5},{8,0},{9,15},{... | collective-permute-start | bytes 774152 | tf_op jit(solution)/shard_map/ppermute | solution.py:378
  57.9 0.8 collective-permute-start.9
  58.7 3.0 %collective-permute-done.10.refs_2_ = bf16[168,768]{1,0:T(8,128)(2,1)S(1)} collective-permute-done((bf16[168,768]{1,0:T(8,128)(2,1)S(1)}, bf16[168,768]{1,0:T(8,128)(2,1)S(1)}, u32[]{:S(2)}, u32[]{:S(2)}) %collective-permute-start.10) | collective-permute-done | bytes 258080 | tf_op jit(solution)/shard_map/ppermute | solution.py:378
  61.7 4.1 %collective-permute-done.11.refs_3_ = bf16[168,768]{1,0:T(8,128)(2,1)S(1)} collective-permute-done((bf16[168,768]{1,0:T(8,128)(2,1)S(1)}, bf16[168,768]{1,0:T(8,128)(2,1)S(1)}, u32[]{:S(2)}, u32[]{:S(2)}) %collective-permute-start.11) | collective-permute-done | bytes 258080 | tf_op jit(solution)/shard_map/ppermute | solution.py:378
  66.0 2.0 %collective-permute-start.12 = (bf16[104,768]{1,0:T(8,128)(2,1)S(1)}, bf16[104,768]{1,0:T(8,128)(2,1)S(1)}, u32[]{:S(2)}, u32[]{:S(2)}) collective-permute-start(bf16[104,768]{1,0:T(8,128)(2,1)S(1)} %get-tuple-element.67.sent_ref), channel_id=1, source_target_pairs={{0,32},{32,0},{64,96},{96,64},{128,160},{160,128},{192,224},{224,1... | collective-permute-start | bytes 479240 | tf_op jit(solution)/shard_map/ppermute | solution.py:384
  68.0 4.9 %collective-permute-done.12.came_ref = bf16[104,768]{1,0:T(8,128)(2,1)S(1)} collective-permute-done((bf16[104,768]{1,0:T(8,128)(2,1)S(1)}, bf16[104,768]{1,0:T(8,128)(2,1)S(1)}, u32[]{:S(2)}, u32[]{:S(2)}) %collective-permute-start.12) | collective-permute-done | bytes 159776 | tf_op jit(solution)/shard_map/ppermute | solution.py:384
  72.9 1.9 %collective-permute-start.13 = (bf16[56,768]{1,0:T(8,128)(2,1)S(1)}, bf16[56,768]{1,0:T(8,128)(2,1)S(1)}, u32[]{:S(2)}, u32[]{:S(2)}) collective-permute-start(bf16[56,768]{1,0:T(8,128)(2,1)S(1)} %get-tuple-element.69), channel_id=1, source_target_pairs={{0,64},{32,96},{64,128},{96,160},{128,192},{160,224},{192,0},{224,... | collective-permute-start | bytes 258056 | tf_op jit(solution)/shard_map/ppermute | solution.py:381
  74.7 5.4 %collective-permute-start.14 = (bf16[56,768]{1,0:T(8,128)(2,1)S(1)}, bf16[56,768]{1,0:T(8,128)(2,1)S(1)}, u32[]{:S(2)}, u32[]{:S(2)}) collective-permute-start(bf16[56,768]{1,0:T(8,128)(2,1)S(1)} %get-tuple-element.70), channel_id=1, source_target_pairs={{0,128},{32,160},{64,192},{96,224},{128,0},{160,32},{192,64},{224,... | collective-permute-start | bytes 258056 | tf_op jit(solution)/shard_map/ppermute | solution.py:381
  80.1 2.7 %collective-permute-start.15 = (bf16[56,768]{1,0:T(8,128)(2,1)S(1)}, bf16[56,768]{1,0:T(8,128)(2,1)S(1)}, u32[]{:S(2)}, u32[]{:S(2)}) collective-permute-start(bf16[56,768]{1,0:T(8,128)(2,1)S(1)} %get-tuple-element.71), channel_id=1, source_target_pairs={{0,192},{32,224},{64,0},{96,32},{128,64},{160,96},{192,128},{224,1... | collective-permute-start | bytes 258056 | tf_op jit(solution)/shard_map/ppermute | solution.py:381
  82.8 3.9 %spread.2 = (bf16[512,768]{1,0:T(8,128)(2,1)}, bf16[512,768]{1,0:T(8,128)(2,1)}) custom-call(bf16[512,768]{1,0:T(8,128)(2,1)S(1)} %copy-done, bf16[512,768]{1,0:T(8,128)(2,1)S(1)} %copy-done.1, f32[512,768]{1,0:T(8,128)S(1)} %get-tuple-element.44.lifted_ref, f32[512,768]{1,0:T(8,128)S(1)} %get-tuple-element.45.normed_ref, ...), custom_call_target="tpu_custom_call" | custom-call | flops 243793920 | bytes 3932160 | tf_op jit(solution)/shard_map/spread/pallas_call | solution.py:458
  86.7 3.9 %spread.3 = (bf16[512,768]{1,0:T(8,128)(2,1)}, bf16[512,768]{1,0:T(8,128)(2,1)}) custom-call(bf16[512,768]{1,0:T(8,128)(2,1)S(1)} %copy-done, bf16[512,768]{1,0:T(8,128)(2,1)S(1)} %copy-done.1, f32[512,768]{1,0:T(8,128)S(1)} %get-tuple-element.44.lifted_ref, ...), custom_call_target="tpu_custom_call", output_to_operand_aliasing={{0}: (8, {}), {1}: (9, {})} | custom-call | flops 243793920 | bytes 3932160 | tf_op jit(solution)/shard_map/spread/pallas_call | solution.py:458
  90.6 0.7 shard_map.136
  (23 shorter events, 0.7 us)
Async XLA Ops:
  7.0 1.6 %collective-permute-start = (f32[512,128]{1,0:T(8,128)S(1)}, f32[512,128]{1,0:T(8,128)S(1)}, u32[]{:S(2)}, u32[]{:S(2)}) collective-permute-start(f32[512,128]{1,0:T(8,128)S(1)} %get-tuple-element.42.own_ref), channel_id=1, source_target_pairs={{0,1},{1,0},{2,3},{3,2},{4,5},{5,4},{6,7},{7,6},{8,9},{9,8},{10,11... | collective-permute-start | bytes 786440 | tf_op jit(solution)/shard_map/ppermute | solution.py:387
  7.1 1.5 %copy-start.3 = (f32[768]{0:T(1024)S(1)}, f32[768]{0:T(1024)}, u32[]{:S(2)}) copy-start(f32[768]{0:T(1024)} %gain_ref.1) | copy-start | bytes 9220
  7.1 1.5 %copy-start.4 = (f32[768]{0:T(1024)S(1)}, f32[768]{0:T(1024)}, u32[]{:S(2)}) copy-start(f32[768]{0:T(1024)} %shift_ref.1) | copy-start | bytes 9220
  12.0 24.7 %copy-start = (bf16[512,768]{1,0:T(8,128)(2,1)S(1)}, bf16[512,768]{1,0:T(8,128)(2,1)}, u32[]{:S(2)}) copy-start(bf16[512,768]{1,0:T(8,128)(2,1)} %value_ref.5) | copy-start | bytes 2359300
  12.0 24.7 %copy-start.1 = (bf16[512,768]{1,0:T(8,128)(2,1)S(1)}, bf16[512,768]{1,0:T(8,128)(2,1)}, u32[]{:S(2)}) copy-start(bf16[512,768]{1,0:T(8,128)(2,1)} %gate_ref.5) | copy-start | bytes 2359300
  12.0 41.3 %collective-permute-start.3 = (bf16[512,768]{1,0:T(8,128)(2,1)S(1)}, bf16[512,768]{1,0:T(8,128)(2,1)S(1)}, u32[]{:S(2)}, u32[]{:S(2)}) collective-permute-start(bf16[512,768]{1,0:T(8,128)(2,1)S(1)} %get-tuple-element.58), channel_id=1, source_target_pairs={{0,2},{1,9},{2,4},{3,11},{4,6},{5,13},{6,0},{7,15},{8,10},{9,17},{... | collective-permute-start | bytes 2359304 | tf_op jit(solution)/shard_map/ppermute | solution.py:378
  13.3 40.0 %collective-permute-start.4 = (bf16[512,768]{1,0:T(8,128)(2,1)S(1)}, bf16[512,768]{1,0:T(8,128)(2,1)S(1)}, u32[]{:S(2)}, u32[]{:S(2)}) collective-permute-start(bf16[512,768]{1,0:T(8,128)(2,1)S(1)} %get-tuple-element.59), channel_id=1, source_target_pairs={{0,4},{1,17},{2,6},{3,19},{4,0},{5,21},{6,2},{7,23},{8,12},{9,25},... | collective-permute-start | bytes 2359304 | tf_op jit(solution)/shard_map/ppermute | solution.py:378
  14.4 38.9 %collective-permute-start.5 = (bf16[512,768]{1,0:T(8,128)(2,1)S(1)}, bf16[512,768]{1,0:T(8,128)(2,1)S(1)}, u32[]{:S(2)}, u32[]{:S(2)}) collective-permute-start(bf16[512,768]{1,0:T(8,128)(2,1)S(1)} %get-tuple-element.60), channel_id=1, source_target_pairs={{0,6},{1,25},{2,0},{3,27},{4,2},{5,29},{6,4},{7,31},{8,14},{9,1},{... | collective-permute-start | bytes 2359304 | tf_op jit(solution)/shard_map/ppermute | solution.py:378
  17.0 1.6 %collective-permute-start.1 = (f32[512,128]{1,0:T(8,128)S(1)}, f32[512,128]{1,0:T(8,128)S(1)}, u32[]{:S(2)}, u32[]{:S(2)}) collective-permute-start(f32[512,128]{1,0:T(8,128)S(1)} %get-tuple-element.47.sums_ref), channel_id=1, source_target_pairs={{0,1},{1,0},{2,3},{3,2},{4,5},{5,4},{6,7},{7,6},{8,9},{9,8},{10,11... | collective-permute-start | bytes 786440 | tf_op jit(solution)/shard_map/ppermute | solution.py:387
  18.7 18.0 %collective-permute-start.2 = (f32[32,768]{1,0:T(8,128)S(1)}, f32[32,768]{1,0:T(8,128)S(1)}, u32[]{:S(2)}, u32[]{:S(2)}) collective-permute-start(f32[32,768]{1,0:T(8,128)S(1)} %get-tuple-element.50), channel_id=1, source_target_pairs={{2,0},{4,2},{6,4},{8,6},{10,8},{12,10},{14,12},{16,14},{18,16},{20... | collective-permute-start | bytes 294920 | tf_op jit(solution)/shard_map/ppermute | solution.py:390
  42.0 7.1 %collective-permute-start.6 = (bf16[40,768]{1,0:T(8,128)(2,1)S(1)}, bf16[40,768]{1,0:T(8,128)(2,1)S(1)}, u32[]{:S(2)}, u32[]{:S(2)}) collective-permute-start(bf16[40,768]{1,0:T(8,128)(2,1)S(1)} %shard_map.132.refs_4_), channel_id=1, source_target_pairs={{0,2},{1,9},{2,4},{3,11},{4,6},{5,13},{6,0},{7,15},{8,10},{9,17},{... | collective-permute-start | bytes 184328 | tf_op jit(solution)/shard_map/ppermute | solution.py:378
  44.2 6.4 %collective-permute-start.7 = (bf16[40,768]{1,0:T(8,128)(2,1)S(1)}, bf16[40,768]{1,0:T(8,128)(2,1)S(1)}, u32[]{:S(2)}, u32[]{:S(2)}) collective-permute-start(bf16[40,768]{1,0:T(8,128)(2,1)S(1)} %shard_map.132.refs_4_), channel_id=1, source_target_pairs={{0,4},{1,17},{2,6},{3,19},{4,0},{5,21},{6,2},{7,23},{8,12},{9,25},... | collective-permute-start | bytes 184328 | tf_op jit(solution)/shard_map/ppermute | solution.py:378
  49.1 4.2 %collective-permute-start.8 = (bf16[40,768]{1,0:T(8,128)(2,1)S(1)}, bf16[40,768]{1,0:T(8,128)(2,1)S(1)}, u32[]{:S(2)}, u32[]{:S(2)}) collective-permute-start(bf16[40,768]{1,0:T(8,128)(2,1)S(1)} %shard_map.132.refs_4_), channel_id=1, source_target_pairs={{0,6},{1,25},{2,0},{3,27},{4,2},{5,29},{6,4},{7,31},{8,14},{9,1},{... | collective-permute-start | bytes 184328 | tf_op jit(solution)/shard_map/ppermute | solution.py:378
  53.4 29.4 %copy-start.2 = (bf16[31,768]{1,0:T(8,128)(2,1)S(1)}, bf16[31,768]{1,0:T(8,128)(2,1)}, u32[]{:S(2)}) copy-start(bf16[31,768]{1,0:T(8,128)(2,1)} %taps_ref.3) | copy-start | bytes 142852
  53.8 7.9 %collective-permute-start.10 = (bf16[168,768]{1,0:T(8,128)(2,1)S(1)}, bf16[168,768]{1,0:T(8,128)(2,1)S(1)}, u32[]{:S(2)}, u32[]{:S(2)}) collective-permute-start(bf16[168,768]{1,0:T(8,128)(2,1)S(1)} %get-tuple-element.64), channel_id=1, source_target_pairs={{0,16},{1,5},{2,18},{3,7},{4,20},{5,1},{6,22},{7,3},{8,24},{9,13},... | collective-permute-start | bytes 774152 | tf_op jit(solution)/shard_map/ppermute | solution.py:378
  56.2 9.6 %collective-permute-start.11 = (bf16[168,768]{1,0:T(8,128)(2,1)S(1)}, bf16[168,768]{1,0:T(8,128)(2,1)S(1)}, u32[]{:S(2)}, u32[]{:S(2)}) collective-permute-start(bf16[168,768]{1,0:T(8,128)(2,1)S(1)} %get-tuple-element.65), channel_id=1, source_target_pairs={{0,24},{1,7},{2,26},{3,1},{4,28},{5,3},{6,30},{7,5},{8,0},{9,15},{... | collective-permute-start | bytes 774152 | tf_op jit(solution)/shard_map/ppermute | solution.py:378
  57.9 7.9 %collective-permute-start.9 = (bf16[168,768]{1,0:T(8,128)(2,1)S(1)}, bf16[168,768]{1,0:T(8,128)(2,1)S(1)}, u32[]{:S(2)}, u32[]{:S(2)}) collective-permute-start(bf16[168,768]{1,0:T(8,128)(2,1)S(1)} %get-tuple-element.63), channel_id=1, source_target_pairs={{0,8},{1,3},{2,10},{3,5},{4,12},{5,7},{6,14},{7,1},{8,16},{9,11},{... | collective-permute-start | bytes 774152 | tf_op jit(solution)/shard_map/ppermute | solution.py:378
  66.0 6.9 %collective-permute-start.12 = (bf16[104,768]{1,0:T(8,128)(2,1)S(1)}, bf16[104,768]{1,0:T(8,128)(2,1)S(1)}, u32[]{:S(2)}, u32[]{:S(2)}) collective-permute-start(bf16[104,768]{1,0:T(8,128)(2,1)S(1)} %get-tuple-element.67.sent_ref), channel_id=1, source_target_pairs={{0,32},{32,0},{64,96},{96,64},{128,160},{160,128},{192,224},{224,1... | collective-permute-start | bytes 479240 | tf_op jit(solution)/shard_map/ppermute | solution.py:384
  72.9 17.7 %collective-permute-start.13 = (bf16[56,768]{1,0:T(8,128)(2,1)S(1)}, bf16[56,768]{1,0:T(8,128)(2,1)S(1)}, u32[]{:S(2)}, u32[]{:S(2)}) collective-permute-start(bf16[56,768]{1,0:T(8,128)(2,1)S(1)} %get-tuple-element.69), channel_id=1, source_target_pairs={{0,64},{32,96},{64,128},{96,160},{128,192},{160,224},{192,0},{224,... | collective-permute-start | bytes 258056 | tf_op jit(solution)/shard_map/ppermute | solution.py:381
  74.7 15.9 %collective-permute-start.14 = (bf16[56,768]{1,0:T(8,128)(2,1)S(1)}, bf16[56,768]{1,0:T(8,128)(2,1)S(1)}, u32[]{:S(2)}, u32[]{:S(2)}) collective-permute-start(bf16[56,768]{1,0:T(8,128)(2,1)S(1)} %get-tuple-element.70), channel_id=1, source_target_pairs={{0,128},{32,160},{64,192},{96,224},{128,0},{160,32},{192,64},{224,... | collective-permute-start | bytes 258056 | tf_op jit(solution)/shard_map/ppermute | solution.py:381
  80.1 10.5 %collective-permute-start.15 = (bf16[56,768]{1,0:T(8,128)(2,1)S(1)}, bf16[56,768]{1,0:T(8,128)(2,1)S(1)}, u32[]{:S(2)}, u32[]{:S(2)}) collective-permute-start(bf16[56,768]{1,0:T(8,128)(2,1)S(1)} %get-tuple-element.71), channel_id=1, source_target_pairs={{0,192},{32,224},{64,0},{96,32},{128,64},{160,96},{192,128},{224,1... | collective-permute-start | bytes 258056 | tf_op jit(solution)/shard_map/ppermute | solution.py:381

commit v3 on v2

--- a/solution.py
+++ b/solution.py
@@ -55,21 +55,15 @@
     return [slice(at, at + LANES) for at in range(0, chans, LANES)]
 
 
-def front_kernel(
-    place_ref, conv_hbm, grad_hbm, weight_hbm, stats_ref, act_grad_ref, conv_ref, grad_ref,
-    weight_ref, conv_sem, grad_sem, weight_sems,
+def stats_kernel(
+    place_ref, conv_hbm, grad_hbm, weight_hbm, stats_ref, conv_ref, grad_ref, weight_ref,
+    conv_sem, grad_sem, weight_sem,
 ):
-    parts = weight_sems.shape[0]
-    wide = weight_ref.shape[1] // parts
-    columns = [slice(k * wide, (k + 1) * wide) for k in range(parts)]
     loads = [
         pltpu.make_async_copy(conv_hbm, conv_ref, conv_sem),
         pltpu.make_async_copy(grad_hbm, grad_ref, grad_sem),
+        pltpu.make_async_copy(weight_hbm, weight_ref, weight_sem),
     ]
-    for k, c in enumerate(columns):
-        loads.append(
-            pltpu.make_async_copy(weight_hbm.at[:, c], weight_ref.at[:, c], weight_sems.at[k])
-        )
     for load in loads:
         load.start()
     loads[0].wait()
@@ -87,10 +81,8 @@
             off = conv_ref[at, c].astype(F32) - mean
             spread = spread + off * off
         stats_ref[at, :] = jnp.where(left, total, jnp.sum(spread, axis=1, keepdims=True))
-    loads[1].wait()
-    for load, c in zip(loads[2:], columns):
+    for load in loads[1:]:
         load.wait()
-        act_grad_ref[:, c] = jnp.dot(grad_ref[...], weight_ref[:, c], preferred_element_type=F32)
 
 
 def turn_kernel(place_ref, grad_ref, turned_ref):
@@ -112,10 +104,13 @@
     lax.fori_loop(0, width // span, body, 0, unroll=4)
 
 
-def middle_kernel(
-    conv_ref, own_ref, peer_ref, gain_ref, shift_ref, act_grad_ref,
-    active_ref, lifted_ref, normed_ref, inv_ref, sums_ref, params_ref,
-    center_ref, total_ref, dot_ref,
+def matmul_kernel(grad_ref, weight_ref, act_grad_ref):
+    act_grad_ref[...] = jnp.dot(grad_ref[...], weight_ref[...], preferred_element_type=F32)
+
+
+def active_kernel(
+    conv_ref, own_ref, peer_ref, gain_ref, shift_ref,
+    active_ref, normed_ref, deriv_ref, inv_ref, center_ref,
 ):
     rows, chans = conv_ref.shape
     wide = 128
@@ -129,28 +124,49 @@
         inv_ref[at, :] = lax.rsqrt(variance + EPS)
     step = 32
 
-    def fold(x):
-        return jnp.sum(x.reshape(step // 8, 8, LANES), axis=0)
-
     def body(i, carry):
-        out = []
         at = pl.ds(pl.multiple_of(i * step, step), step)
         center, inv = center_ref[at, :], inv_ref[at, :]
-        total, dot = 0.0, 0.0
-        for k, c in enumerate(tiles(chans)):
+        for c in tiles(chans):
             gain, shift = gain_ref[c].reshape(1, LANES), shift_ref[c].reshape(1, LANES)
             normed = (conv_ref[at, c].astype(F32) - center) * inv
             shifted = normed * gain + shift
             sig = jax.nn.sigmoid(shifted)
             active = shifted * sig
             active_ref[at, c] = active.astype(BF16)
-            norm_grad = act_grad_ref[at, c] * (sig + active * (1.0 - sig))
+            normed_ref[at, c] = normed
+            deriv_ref[at, c] = sig + active * (1.0 - sig)
+        return carry
+
+    lax.fori_loop(0, rows // step, body, 0)
+
+
+def middle_kernel(
+    act_grad_ref, normed_ref, deriv_ref, inv_ref, gain_ref, lifted_ref, sums_ref, params_ref,
+    total_ref, dot_ref,
+):
+    rows, chans = act_grad_ref.shape
+    wide = 128
+    step = 32
+
+    def fold(x):
+        return jnp.sum(x.reshape(step // 8, 8, LANES), axis=0)
+
+    def body(i, carry):
+        out = []
+        at = pl.ds(pl.multiple_of(i * step, step), step)
+        inv = inv_ref[at, :]
+        total, dot = 0.0, 0.0
+        for k, c in enumerate(tiles(chans)):
+            normed = normed_ref[at, c]
+            norm_grad = act_grad_ref[at, c] * deriv_ref[at, c]
+            along = norm_grad * normed
+            gain = gain_ref[c].reshape(1, LANES)
             scaled = norm_grad * gain
             lifted_ref[at, c] = scaled * inv
-            normed_ref[at, c] = normed
             total = total + scaled
-            dot = dot + scaled * normed
-            out.append(carry[2 * k] + fold(norm_grad * normed))
+            dot = dot + along * gain
+            out.append(carry[2 * k] + fold(along))
             out.append(carry[2 * k + 1] + fold(norm_grad))
         total_ref[at, :] = total
         dot_ref[at, :] = dot
@@ -171,9 +187,9 @@
         )
 
 
-def project_kernel(turned_ref, active_ref, *out_refs):
+def project_kernel(which, turned_ref, active_ref, *out_refs):
     rows = out_refs[0].shape[0]
-    for k, out_ref in enumerate(out_refs):
+    for k, out_ref in zip(which, out_refs):
         out_ref[...] = jnp.dot(
             turned_ref[k * rows : (k + 1) * rows, :], active_ref[...], preferred_element_type=F32
         ).astype(BF16)
@@ -192,7 +208,9 @@
         slope_ref[at, :] = dot * scale
     at = slice(0, head_ref.shape[0])
     for c in tiles(chans):
-        head_ref[at, c] = lifted_ref[at, c] - mean_ref[at, :] - normed_ref[at, c] * slope_ref[at, :]
+        head_ref[at, c] = (
+            lifted_ref[at, c] - mean_ref[at, :] - normed_ref[at, c] * slope_ref[at, :]
+        ).astype(BF16)
 
 
 def fill_heights(heights, lanes, lifted_ref, normed_ref, mean_ref, slope_ref, halo_ref):
@@ -201,7 +219,7 @@
     heights[0:rows, :] = (
         lifted_ref[:, lanes] - mean_ref[...] - normed_ref[:, lanes] * slope_ref[...]
     )
-    heights[rows : rows + tail, :] = halo_ref[:, lanes]
+    heights[rows : rows + tail, :] = halo_ref[:, lanes].astype(F32)
 
 
 def strips(body, begin, end):
@@ -216,7 +234,7 @@
     return pl.ds(pl.multiple_of(at, LANES), LANES)
 
 
-GROUP = 4
+GROUP = 8
 
 
 def taps_kernel(
@@ -245,7 +263,9 @@
                 for q, over in enumerate(overs):
                     j = reach - over
                     products = [held[b] * there[b + q] for b in range(GROUP)]
-                    out[j] = out[j] + ((products[0] + products[1]) + (products[2] + products[3]))
+                    while len(products) > 1:
+                        products = [a + b for a, b in zip(products[::2], products[1::2])]
+                    out[j] = out[j] + products[0]
             return tuple(out)
 
         zero = jnp.zeros((8, LANES), F32)
@@ -389,22 +409,16 @@
     def previous(array):
         return lax.ppermute(array, SP, [(i, i - 1) for i in range(1, nz * n * n)])
 
-    stats, act_grad, height, grads = call(
-        front_kernel,
+    stats, height, grads, weights = call(
+        stats_kernel,
         (
-            shape((rows, LANES), F32), shape((rows, chans), F32),
-            shape(conv_out.shape, BF16), shape(out_grad.shape, BF16),
+            shape((rows, LANES), F32), shape(conv_out.shape, BF16),
+            shape(out_grad.shape, BF16), shape(proj_weight.shape, BF16),
         ),
         place, *(pltpu.with_memory_space_constraint(a, pltpu.HBM) for a in (conv_out, out_grad, proj_weight)),
-        flops=2 * rows * width * chans,
-        scratch=[
-            pltpu.VMEM(proj_weight.shape, BF16),
-            pltpu.SemaphoreType.DMA,
-            pltpu.SemaphoreType.DMA,
-            pltpu.SemaphoreType.DMA((3,)),
-        ],
+        flops=rows * chans * 100,
+        scratch=[pltpu.SemaphoreType.DMA] * 3,
         specs=[pl.BlockSpec(memory_space=pltpu.SMEM)] + [pl.BlockSpec(memory_space=pltpu.HBM)] * 3,
-        limit=12,
     )
     stats_peer = other_core(stats)
     (turned,) = call(
@@ -413,33 +427,53 @@
         place, grads,
         flops=rows * width * chans,
         specs=[pl.BlockSpec(memory_space=pltpu.SMEM)] + vmem(1),
-        limit=4,
-    )
-    active, lifted, normed, inv, sums, params = call(
-        middle_kernel,
+    )
+    active, normed, deriv, inv = call(
+        active_kernel,
         (
             shape((rows, chans), BF16), shape((rows, chans), F32), shape((rows, chans), F32),
-            shape((rows, LANES), F32), shape((rows, LANES), F32), shape((2, chans), F32),
+            shape((rows, LANES), F32),
         ),
-        height, stats, stats_peer, norm_gain, norm_shift, act_grad,
+        height, stats, stats_peer, norm_gain, norm_shift,
         flops=rows * chans * 1000,
-        scratch=[pltpu.VMEM((rows, LANES), F32)] * 3,
+        scratch=[pltpu.VMEM((rows, LANES), F32)],
+    )
+
+    def project(*which):
+        return call(
+            functools.partial(project_kernel, which),
+            (shape((width // n, chans), BF16),) * len(which),
+            turned, active,
+            flops=2 * rows * width * chans * len(which) // n,
+        )
+
+    blocks = {}
+    blocks.update(zip((1,), project(1)))
+    (act_grad,) = call(
+        matmul_kernel,
+        (shape((rows, chans), F32),),
+        grads, weights,
+        flops=2 * rows * width * chans,
+    )
+    lifted, sums, params = call(
+        middle_kernel,
+        (shape((rows, chans), F32), shape((rows, LANES), F32), shape((2, chans), F32)),
+        act_grad, normed, deriv, inv, norm_gain,
+        flops=rows * chans * 1000,
+        scratch=[pltpu.VMEM((rows, LANES), F32)] * 2,
     )
     sums_peer = other_core(sums)
-    blocks = call(
-        project_kernel,
-        (shape((width // n, chans), BF16),) * n,
-        turned, active,
-        flops=2 * rows * width * chans,
-    )
+    blocks.update(zip((2, 3, 0), project(2, 3, 0)))
     mean, slope, head = call(
         head_kernel,
-        (shape((rows, LANES), F32), shape((rows, LANES), F32), shape((tail, chans), F32)),
+        (shape((rows, LANES), F32), shape((rows, LANES), F32), shape((tail, chans), BF16)),
         lifted, normed, inv, sums, sums_peer,
         flops=rows * chans * 10,
     )
     halo = previous(head)
-    landed = [blocks[0]] + [hop(blocks[k], k, 1) for k in range(1, n)]
+    landed = [blocks[0], hop(blocks[1], 1, 1)]
+    landed.append(hop(blocks[2], 2, 1))
+    landed.append(hop(blocks[3], 3, 1))
     heights = (lifted, normed, mean, slope, halo)
     (small,) = call(
         taps_kernel,

time: 91.4 us -> 87.5 us (0.957)
  the two profiles are of different devices: /device:TPU:4 before, /device:TPU:8 now
where the time goes in v3:
time: 87.5 us; the launch traced here: 87.4 us
  waiting for transfers between devices  35.5 us (41%)
  starting transfers between devices  27.6 us (32%)
  Pallas kernels  23.4 us (27%)
    ppermute x9, waiting for transfers between devices, hop(): return lax.ppermute(array, ALL, [(index(*at), to(*at)) for at in places])  20 us
    pallas_call x13, Pallas kernels, call(): pl.pallas_call(kernel, out_shape=outs, in_specs=specs or vmem(len(args)),...  16.4 us
    ppermute x9, starting transfers between devices, hop(): return lax.ppermute(array, ALL, [(index(*at), to(*at)) for at in places])  11 us
    ppermute x3, starting transfers between devices, hop_z(): return lax.ppermute(array, 'sp_0', [(i, (i + k) % nz) for i in range(nz)])  10.3 us
    ppermute x1, waiting for transfers between devices, previous(): return lax.ppermute(array, SP, [(i, i - 1) for i in range(1, nz * n * n)])  9.42 us
    pallas_call x2, Pallas kernels, spread_part(): pl.pallas_call(functools.partial(spread_kernel, part * half), grid=(1,),...  6.96 us
    ppermute x1, waiting for transfers between devices, swap_z(): return lax.ppermute(array, 'sp_0', [(i, i ^ 1) for i in range(nz)])  4.43 us
    ppermute x1, starting transfers between devices, previous(): return lax.ppermute(array, SP, [(i, i - 1) for i in range(1, nz * n * n)])  4.15 us
  transfers between devices with their start and end apart: 16, of which 10 were waited for; matrix products, arithmetic and copies ran while one was open for 0% of the time, Pallas kernels for 18%

profile of v3, /device:TPU:8, one launch (start us, length us, event | category | flops | bytes accessed | tf_op | source)
XLA Modules:
  0.0 87.4 jit_solution(4998511919481768739)
XLA Ops:
  0.7 3.3 %shard_map.127 = (f32[512,128]{1,0:T(8,128)S(1)}, bf16[512,768]{1,0:T(8,128)(2,1)S(1)}, bf16[512,2048]{1,0:T(8,128)(2,1)S(1)}, bf16[2048,768]{1,0:T(8,128)(2,1)S(1)}) custom-call(s32[128]{0:T(128)S(1)} %add_multiply_fusion.place_ref, bf16[512,768]{1,0:T(8,128)(2,1)} %conv_hbm.1, bf16[512,2048]{1,0:T(8,128)(2,1)} %grad_hbm.1, bf16[2048,768]{1,0:T(8,128)(2,1)} %weight_hbm.1), custom_call_target="tpu_custom_call" | custom-call | flops 39321600 | bytes 12321280 | tf_op jit(solution)/shard_map/pallas_call | solution.py:29
  4.1 1.3 %shard_map.132.turned_ref = bf16[2048,512]{1,0:T(8,128)(2,1)S(1)} custom-call(s32[128]{0:T(128)S(1)} %add_multiply_fusion.place_ref, bf16[512,2048]{1,0:T(8,128)(2,1)S(1)} %get-tuple-element.41.grad_ref), custom_call_target="tpu_custom_call" | custom-call | flops 805306368 | bytes 4194816 | tf_op jit(solution)/shard_map/pallas_call | solution.py:29
  5.5 0.2 collective-permute-done.peer_ref
  5.7 1.0 %shard_map.129 = (bf16[512,768]{1,0:T(8,128)(2,1)S(1)}, f32[512,768]{1,0:T(8,128)S(1)}, f32[512,768]{1,0:T(8,128)S(1)}, f32[512,128]{1,0:T(8,128)S(1)}) custom-call(bf16[512,768]{1,0:T(8,128)(2,1)S(1)} %get-tuple-element.43.conv_ref, f32[512,128]{1,0:T(8,128)S(1)} %get-tuple-element.44.own_ref, f32[512,128]{1,0:T(8,128)S(1)} %collective-permute-done.peer_ref, ...), custom_call_target="tpu_custom_call" | custom-call | flops 393216000 | bytes 5511168 | tf_op jit(solution)/shard_map/pallas_call | solution.py:29
  6.6 0.6 shard_map.134
  7.2 1.4 %shard_map.133 = (bf16[512,768]{1,0:T(8,128)(2,1)S(1)}, bf16[512,768]{1,0:T(8,128)(2,1)S(1)}, bf16[512,768]{1,0:T(8,128)(2,1)S(1)}) custom-call(bf16[2048,512]{1,0:T(8,128)(2,1)S(1)} %shard_map.132.turned_ref, bf16[512,768]{1,0:T(8,128)(2,1)S(1)} %get-tuple-element.57.active_ref), custom_call_target="tpu_custom_call" | custom-call | flops 1207959552 | bytes 5242880 | tf_op jit(solution)/shard_map/pallas_call | solution.py:29
  8.6 3.1 %collective-permute-start.4 = (bf16[512,768]{1,0:T(8,128)(2,1)S(1)}, bf16[512,768]{1,0:T(8,128)(2,1)S(1)}, u32[]{:S(2)}, u32[]{:S(2)}) collective-permute-start(bf16[512,768]{1,0:T(8,128)(2,1)S(1)} %get-tuple-element.59), channel_id=1, source_target_pairs={{0,4},{1,17},{2,6},{3,19},{4,0},{5,21},{6,2},{7,23},{8,12},{9,25},... | collective-permute-start | bytes 2359304 | tf_op jit(solution)/shard_map/ppermute | solution.py:398
  11.7 1.1 %collective-permute-start.5 = (bf16[512,768]{1,0:T(8,128)(2,1)S(1)}, bf16[512,768]{1,0:T(8,128)(2,1)S(1)}, u32[]{:S(2)}, u32[]{:S(2)}) collective-permute-start(bf16[512,768]{1,0:T(8,128)(2,1)S(1)} %get-tuple-element.60), channel_id=1, source_target_pairs={{0,6},{1,25},{2,0},{3,27},{4,2},{5,29},{6,4},{7,31},{8,14},{9,1},{... | collective-permute-start | bytes 2359304 | tf_op jit(solution)/shard_map/ppermute | solution.py:398
  12.8 0.9 %collective-permute-start.3 = (bf16[512,768]{1,0:T(8,128)(2,1)S(1)}, bf16[512,768]{1,0:T(8,128)(2,1)S(1)}, u32[]{:S(2)}, u32[]{:S(2)}) collective-permute-start(bf16[512,768]{1,0:T(8,128)(2,1)S(1)} %shard_map.134), channel_id=1, source_target_pairs={{0,2},{1,9},{2,4},{3,11},{4,6},{5,13},{6,0},{7,15},{8,10},{9,17},{... | collective-permute-start | bytes 2359304 | tf_op jit(solution)/shard_map/ppermute | solution.py:398
  13.7 1.8 %shard_map.128.act_grad_ref = f32[512,768]{1,0:T(8,128)S(1)} custom-call(bf16[512,2048]{1,0:T(8,128)(2,1)S(1)} %get-tuple-element.41.grad_ref, bf16[2048,768]{1,0:T(8,128)(2,1)S(1)} %get-tuple-element.42.weight_ref), custom_call_target="tpu_custom_call" | custom-call | flops 1610612736 | bytes 6815744 | tf_op jit(solution)/shard_map/pallas_call | solution.py:29
  15.5 0.9 %shard_map.130 = (f32[512,768]{1,0:T(8,128)S(1)}, f32[512,128]{1,0:T(8,128)S(1)}, f32[2,768]{1,0:T(2,128)S(1)}) custom-call(f32[512,768]{1,0:T(8,128)S(1)} %shard_map.128.act_grad_ref, f32[512,768]{1,0:T(8,128)S(1)} %get-tuple-element.45.normed_ref, f32[512,768]{1,0:T(8,128)S(1)} %get-tuple-element.46.deriv_ref, f32[512,128]{1,0:T(8,128)S(1)} %get-tuple-element.47.inv_ref, ...), custom_call_target="tpu_custom_call" | custom-call | flops 393216000 | bytes 6824960 | tf_op jit(solution)/shard_map/pallas_call | solution.py:29
  16.5 1.5 %collective-permute-done.1.sums_peer_ref = f32[512,128]{1,0:T(8,128)S(1)} collective-permute-done((f32[512,128]{1,0:T(8,128)S(1)}, f32[512,128]{1,0:T(8,128)S(1)}, u32[]{:S(2)}, u32[]{:S(2)}) %collective-permute-start.1) | collective-permute-done | bytes 262176 | tf_op jit(solution)/shard_map/ppermute | solution.py:407
  18.2 4.1 %collective-permute-start.2 = (bf16[32,768]{1,0:T(8,128)(2,1)S(1)}, bf16[32,768]{1,0:T(8,128)(2,1)S(1)}, u32[]{:S(2)}, u32[]{:S(2)}) collective-permute-start(bf16[32,768]{1,0:T(8,128)(2,1)S(1)} %get-tuple-element.52), channel_id=1, source_target_pairs={{2,0},{4,2},{6,4},{8,6},{10,8},{12,10},{14,12},{16,14},{18,16},{20... | collective-permute-start | bytes 147464 | tf_op jit(solution)/shard_map/ppermute | solution.py:410
  22.4 9.4 %collective-permute-done.2.halo_ref = bf16[32,768]{1,0:T(8,128)(2,1)S(1)} collective-permute-done((bf16[32,768]{1,0:T(8,128)(2,1)S(1)}, bf16[32,768]{1,0:T(8,128)(2,1)S(1)}, u32[]{:S(2)}, u32[]{:S(2)}) %collective-permute-start.2) | collective-permute-done | bytes 49184 | tf_op jit(solution)/shard_map/ppermute | solution.py:410
  31.8 4.7 %shard_map.135.refs_4_ = bf16[40,768]{1,0:T(8,128)(2,1)S(1)} custom-call(bf16[512,768]{1,0:T(8,128)(2,1)S(1)} %copy-done, bf16[512,768]{1,0:T(8,128)(2,1)S(1)} %copy-done.1, f32[512,768]{1,0:T(8,128)S(1)} %get-tuple-element.48.lifted_ref, f32[512,768]{1,0:T(8,128)S(1)} %get-tuple-element.45.normed_ref, f32[512,128]{1,0:T(8,128)S(1)} %get-tuple-element.50.mean_ref, ...), custom_call_target="tpu_custom_call" | custom-call | flops 487587840 | bytes 5359616 | tf_op jit(solution)/shard_map/pallas_call | solution.py:29
  36.5 3.7 %collective-permute-start.8 = (bf16[40,768]{1,0:T(8,128)(2,1)S(1)}, bf16[40,768]{1,0:T(8,128)(2,1)S(1)}, u32[]{:S(2)}, u32[]{:S(2)}) collective-permute-start(bf16[40,768]{1,0:T(8,128)(2,1)S(1)} %shard_map.135.refs_4_), channel_id=1, source_target_pairs={{0,6},{1,25},{2,0},{3,27},{4,2},{5,29},{6,4},{7,31},{8,14},{9,1},{... | collective-permute-start | bytes 184328 | tf_op jit(solution)/shard_map/ppermute | solution.py:398
  40.3 5.4 %collective-permute-done.8.refs_7_ = bf16[40,768]{1,0:T(8,128)(2,1)S(1)} collective-permute-done((bf16[40,768]{1,0:T(8,128)(2,1)S(1)}, bf16[40,768]{1,0:T(8,128)(2,1)S(1)}, u32[]{:S(2)}, u32[]{:S(2)}) %collective-permute-start.8) | collective-permute-done | bytes 61472 | tf_op jit(solution)/shard_map/ppermute | solution.py:398
  45.6 1.0 %collective-permute-done.7.refs_6_ = bf16[40,768]{1,0:T(8,128)(2,1)S(1)} collective-permute-done((bf16[40,768]{1,0:T(8,128)(2,1)S(1)}, bf16[40,768]{1,0:T(8,128)(2,1)S(1)}, u32[]{:S(2)}, u32[]{:S(2)}) %collective-permute-start.7) | collective-permute-done | bytes 61472 | tf_op jit(solution)/shard_map/ppermute | solution.py:398
  46.6 5.0 %collective-permute-done.6.refs_5_ = bf16[40,768]{1,0:T(8,128)(2,1)S(1)} collective-permute-done((bf16[40,768]{1,0:T(8,128)(2,1)S(1)}, bf16[40,768]{1,0:T(8,128)(2,1)S(1)}, u32[]{:S(2)}, u32[]{:S(2)}) %collective-permute-start.6) | collective-permute-done | bytes 61472 | tf_op jit(solution)/shard_map/ppermute | solution.py:398
  51.7 0.4 shard_map.136
  52.3 1.9 %collective-permute-start.11 = (bf16[168,768]{1,0:T(8,128)(2,1)S(1)}, bf16[168,768]{1,0:T(8,128)(2,1)S(1)}, u32[]{:S(2)}, u32[]{:S(2)}) collective-permute-start(bf16[168,768]{1,0:T(8,128)(2,1)S(1)} %get-tuple-element.65), channel_id=1, source_target_pairs={{0,24},{1,7},{2,26},{3,1},{4,28},{5,3},{6,30},{7,5},{8,0},{9,15},{... | collective-permute-start | bytes 774152 | tf_op jit(solution)/shard_map/ppermute | solution.py:398
  54.2 4.3 %collective-permute-done.9.refs_1_ = bf16[168,768]{1,0:T(8,128)(2,1)S(1)} collective-permute-done((bf16[168,768]{1,0:T(8,128)(2,1)S(1)}, bf16[168,768]{1,0:T(8,128)(2,1)S(1)}, u32[]{:S(2)}, u32[]{:S(2)}) %collective-permute-start.9) | collective-permute-done | bytes 258080 | tf_op jit(solution)/shard_map/ppermute | solution.py:398
  58.5 1.7 %collective-permute-done.10.refs_2_ = bf16[168,768]{1,0:T(8,128)(2,1)S(1)} collective-permute-done((bf16[168,768]{1,0:T(8,128)(2,1)S(1)}, bf16[168,768]{1,0:T(8,128)(2,1)S(1)}, u32[]{:S(2)}, u32[]{:S(2)}) %collective-permute-start.10) | collective-permute-done | bytes 258080 | tf_op jit(solution)/shard_map/ppermute | solution.py:398
  60.2 2.5 %collective-permute-done.11.refs_3_ = bf16[168,768]{1,0:T(8,128)(2,1)S(1)} collective-permute-done((bf16[168,768]{1,0:T(8,128)(2,1)S(1)}, bf16[168,768]{1,0:T(8,128)(2,1)S(1)}, u32[]{:S(2)}, u32[]{:S(2)}) %collective-permute-start.11) | collective-permute-done | bytes 258080 | tf_op jit(solution)/shard_map/ppermute | solution.py:398
  62.9 2.0 %collective-permute-start.12 = (bf16[104,768]{1,0:T(8,128)(2,1)S(1)}, bf16[104,768]{1,0:T(8,128)(2,1)S(1)}, u32[]{:S(2)}, u32[]{:S(2)}) collective-permute-start(bf16[104,768]{1,0:T(8,128)(2,1)S(1)} %get-tuple-element.67.sent_ref), channel_id=1, source_target_pairs={{0,32},{32,0},{64,96},{96,64},{128,160},{160,128},{192,224},{224,1... | collective-permute-start | bytes 479240 | tf_op jit(solution)/shard_map/ppermute | solution.py:404
  64.9 4.4 %collective-permute-done.12.came_ref = bf16[104,768]{1,0:T(8,128)(2,1)S(1)} collective-permute-done((bf16[104,768]{1,0:T(8,128)(2,1)S(1)}, bf16[104,768]{1,0:T(8,128)(2,1)S(1)}, u32[]{:S(2)}, u32[]{:S(2)}) %collective-permute-start.12) | collective-permute-done | bytes 159776 | tf_op jit(solution)/shard_map/ppermute | solution.py:404
  69.4 2.5 %collective-permute-start.13 = (bf16[56,768]{1,0:T(8,128)(2,1)S(1)}, bf16[56,768]{1,0:T(8,128)(2,1)S(1)}, u32[]{:S(2)}, u32[]{:S(2)}) collective-permute-start(bf16[56,768]{1,0:T(8,128)(2,1)S(1)} %get-tuple-element.69), channel_id=1, source_target_pairs={{0,64},{32,96},{64,128},{96,160},{128,192},{160,224},{192,0},{224,... | collective-permute-start | bytes 258056 | tf_op jit(solution)/shard_map/ppermute | solution.py:401
  71.8 5.2 %collective-permute-start.14 = (bf16[56,768]{1,0:T(8,128)(2,1)S(1)}, bf16[56,768]{1,0:T(8,128)(2,1)S(1)}, u32[]{:S(2)}, u32[]{:S(2)}) collective-permute-start(bf16[56,768]{1,0:T(8,128)(2,1)S(1)} %get-tuple-element.70), channel_id=1, source_target_pairs={{0,128},{32,160},{64,192},{96,224},{128,0},{160,32},{192,64},{224,... | collective-permute-start | bytes 258056 | tf_op jit(solution)/shard_map/ppermute | solution.py:401
  77.0 2.7 %collective-permute-start.15 = (bf16[56,768]{1,0:T(8,128)(2,1)S(1)}, bf16[56,768]{1,0:T(8,128)(2,1)S(1)}, u32[]{:S(2)}, u32[]{:S(2)}) collective-permute-start(bf16[56,768]{1,0:T(8,128)(2,1)S(1)} %get-tuple-element.71), channel_id=1, source_target_pairs={{0,192},{32,224},{64,0},{96,32},{128,64},{160,96},{192,128},{224,1... | collective-permute-start | bytes 258056 | tf_op jit(solution)/shard_map/ppermute | solution.py:401
  79.7 3.5 %spread.2 = (bf16[512,768]{1,0:T(8,128)(2,1)}, bf16[512,768]{1,0:T(8,128)(2,1)}) custom-call(bf16[512,768]{1,0:T(8,128)(2,1)S(1)} %copy-done, bf16[512,768]{1,0:T(8,128)(2,1)S(1)} %copy-done.1, f32[512,768]{1,0:T(8,128)S(1)} %get-tuple-element.48.lifted_ref, f32[512,768]{1,0:T(8,128)S(1)} %get-tuple-element.45.normed_ref, ...), custom_call_target="tpu_custom_call" | custom-call | flops 243793920 | bytes 3932160 | tf_op jit(solution)/shard_map/spread/pallas_call | solution.py:492
  83.2 3.5 %spread.3 = (bf16[512,768]{1,0:T(8,128)(2,1)}, bf16[512,768]{1,0:T(8,128)(2,1)}) custom-call(bf16[512,768]{1,0:T(8,128)(2,1)S(1)} %copy-done, bf16[512,768]{1,0:T(8,128)(2,1)S(1)} %copy-done.1, f32[512,768]{1,0:T(8,128)S(1)} %get-tuple-element.48.lifted_ref, ...), custom_call_target="tpu_custom_call", output_to_operand_aliasing={{0}: (8, {}), {1}: (9, {})} | custom-call | flops 243793920 | bytes 3932160 | tf_op jit(solution)/shard_map/spread/pallas_call | solution.py:492
  86.7 0.7 shard_map.139
  (26 shorter events, 0.8 us)
Async XLA Ops:
  4.0 1.6 %collective-permute-start = (f32[512,128]{1,0:T(8,128)S(1)}, f32[512,128]{1,0:T(8,128)S(1)}, u32[]{:S(2)}, u32[]{:S(2)}) collective-permute-start(f32[512,128]{1,0:T(8,128)S(1)} %get-tuple-element.44.own_ref), channel_id=1, source_target_pairs={{0,1},{1,0},{2,3},{3,2},{4,5},{5,4},{6,7},{7,6},{8,9},{9,8},{10,11... | collective-permute-start | bytes 786440 | tf_op jit(solution)/shard_map/ppermute | solution.py:407
  4.1 1.5 %copy-start.3 = (f32[768]{0:T(1024)S(1)}, f32[768]{0:T(1024)}, u32[]{:S(2)}) copy-start(f32[768]{0:T(1024)} %gain_ref.3) | copy-start | bytes 9220
  4.1 1.5 %copy-start.4 = (f32[768]{0:T(1024)S(1)}, f32[768]{0:T(1024)}, u32[]{:S(2)}) copy-start(f32[768]{0:T(1024)} %shift_ref.1) | copy-start | bytes 9220
  8.6 43.1 %collective-permute-start.4 = (bf16[512,768]{1,0:T(8,128)(2,1)S(1)}, bf16[512,768]{1,0:T(8,128)(2,1)S(1)}, u32[]{:S(2)}, u32[]{:S(2)}) collective-permute-start(bf16[512,768]{1,0:T(8,128)(2,1)S(1)} %get-tuple-element.59), channel_id=1, source_target_pairs={{0,4},{1,17},{2,6},{3,19},{4,0},{5,21},{6,2},{7,23},{8,12},{9,25},... | collective-permute-start | bytes 2359304 | tf_op jit(solution)/shard_map/ppermute | solution.py:398
  11.7 40.0 %collective-permute-start.5 = (bf16[512,768]{1,0:T(8,128)(2,1)S(1)}, bf16[512,768]{1,0:T(8,128)(2,1)S(1)}, u32[]{:S(2)}, u32[]{:S(2)}) collective-permute-start(bf16[512,768]{1,0:T(8,128)(2,1)S(1)} %get-tuple-element.60), channel_id=1, source_target_pairs={{0,6},{1,25},{2,0},{3,27},{4,2},{5,29},{6,4},{7,31},{8,14},{9,1},{... | collective-permute-start | bytes 2359304 | tf_op jit(solution)/shard_map/ppermute | solution.py:398
  12.8 38.8 %collective-permute-start.3 = (bf16[512,768]{1,0:T(8,128)(2,1)S(1)}, bf16[512,768]{1,0:T(8,128)(2,1)S(1)}, u32[]{:S(2)}, u32[]{:S(2)}) collective-permute-start(bf16[512,768]{1,0:T(8,128)(2,1)S(1)} %shard_map.134), channel_id=1, source_target_pairs={{0,2},{1,9},{2,4},{3,11},{4,6},{5,13},{6,0},{7,15},{8,10},{9,17},{... | collective-permute-start | bytes 2359304 | tf_op jit(solution)/shard_map/ppermute | solution.py:398
  16.4 15.4 %copy-start = (bf16[512,768]{1,0:T(8,128)(2,1)S(1)}, bf16[512,768]{1,0:T(8,128)(2,1)}, u32[]{:S(2)}) copy-start(bf16[512,768]{1,0:T(8,128)(2,1)} %value_ref.5) | copy-start | bytes 2359300
  16.4 15.4 %copy-start.1 = (bf16[512,768]{1,0:T(8,128)(2,1)S(1)}, bf16[512,768]{1,0:T(8,128)(2,1)}, u32[]{:S(2)}) copy-start(bf16[512,768]{1,0:T(8,128)(2,1)} %gate_ref.5) | copy-start | bytes 2359300
  16.4 1.6 %collective-permute-start.1 = (f32[512,128]{1,0:T(8,128)S(1)}, f32[512,128]{1,0:T(8,128)S(1)}, u32[]{:S(2)}, u32[]{:S(2)}) collective-permute-start(f32[512,128]{1,0:T(8,128)S(1)} %get-tuple-element.49.sums_ref), channel_id=1, source_target_pairs={{0,1},{1,0},{2,3},{3,2},{4,5},{5,4},{6,7},{7,6},{8,9},{9,8},{10,11... | collective-permute-start | bytes 786440 | tf_op jit(solution)/shard_map/ppermute | solution.py:407
  18.2 13.6 %collective-permute-start.2 = (bf16[32,768]{1,0:T(8,128)(2,1)S(1)}, bf16[32,768]{1,0:T(8,128)(2,1)S(1)}, u32[]{:S(2)}, u32[]{:S(2)}) collective-permute-start(bf16[32,768]{1,0:T(8,128)(2,1)S(1)} %get-tuple-element.52), channel_id=1, source_target_pairs={{2,0},{4,2},{6,4},{8,6},{10,8},{12,10},{14,12},{16,14},{18,16},{20... | collective-permute-start | bytes 147464 | tf_op jit(solution)/shard_map/ppermute | solution.py:410
  36.5 9.1 %collective-permute-start.8 = (bf16[40,768]{1,0:T(8,128)(2,1)S(1)}, bf16[40,768]{1,0:T(8,128)(2,1)S(1)}, u32[]{:S(2)}, u32[]{:S(2)}) collective-permute-start(bf16[40,768]{1,0:T(8,128)(2,1)S(1)} %shard_map.135.refs_4_), channel_id=1, source_target_pairs={{0,6},{1,25},{2,0},{3,27},{4,2},{5,29},{6,4},{7,31},{8,14},{9,1},{... | collective-permute-start | bytes 184328 | tf_op jit(solution)/shard_map/ppermute | solution.py:398
  40.3 6.4 %collective-permute-start.7 = (bf16[40,768]{1,0:T(8,128)(2,1)S(1)}, bf16[40,768]{1,0:T(8,128)(2,1)S(1)}, u32[]{:S(2)}, u32[]{:S(2)}) collective-permute-start(bf16[40,768]{1,0:T(8,128)(2,1)S(1)} %shard_map.135.refs_4_), channel_id=1, source_target_pairs={{0,4},{1,17},{2,6},{3,19},{4,0},{5,21},{6,2},{7,23},{8,12},{9,25},... | collective-permute-start | bytes 184328 | tf_op jit(solution)/shard_map/ppermute | solution.py:398
  45.6 6.0 %collective-permute-start.6 = (bf16[40,768]{1,0:T(8,128)(2,1)S(1)}, bf16[40,768]{1,0:T(8,128)(2,1)S(1)}, u32[]{:S(2)}, u32[]{:S(2)}) collective-permute-start(bf16[40,768]{1,0:T(8,128)(2,1)S(1)} %shard_map.135.refs_4_), channel_id=1, source_target_pairs={{0,2},{1,9},{2,4},{3,11},{4,6},{5,13},{6,0},{7,15},{8,10},{9,17},{... | collective-permute-start | bytes 184328 | tf_op jit(solution)/shard_map/ppermute | solution.py:398
  51.7 28.0 %copy-start.2 = (bf16[31,768]{1,0:T(8,128)(2,1)S(1)}, bf16[31,768]{1,0:T(8,128)(2,1)}, u32[]{:S(2)}) copy-start(bf16[31,768]{1,0:T(8,128)(2,1)} %taps_ref.3) | copy-start | bytes 142852
  52.1 6.4 %collective-permute-start.9 = (bf16[168,768]{1,0:T(8,128)(2,1)S(1)}, bf16[168,768]{1,0:T(8,128)(2,1)S(1)}, u32[]{:S(2)}, u32[]{:S(2)}) collective-permute-start(bf16[168,768]{1,0:T(8,128)(2,1)S(1)} %get-tuple-element.63), channel_id=1, source_target_pairs={{0,8},{1,3},{2,10},{3,5},{4,12},{5,7},{6,14},{7,1},{8,16},{9,11},{... | collective-permute-start | bytes 774152 | tf_op jit(solution)/shard_map/ppermute | solution.py:398
  52.2 8.0 %collective-permute-start.10 = (bf16[168,768]{1,0:T(8,128)(2,1)S(1)}, bf16[168,768]{1,0:T(8,128)(2,1)S(1)}, u32[]{:S(2)}, u32[]{:S(2)}) collective-permute-start(bf16[168,768]{1,0:T(8,128)(2,1)S(1)} %get-tuple-element.64), channel_id=1, source_target_pairs={{0,16},{1,5},{2,18},{3,7},{4,20},{5,1},{6,22},{7,3},{8,24},{9,13},... | collective-permute-start | bytes 774152 | tf_op jit(solution)/shard_map/ppermute | solution.py:398
  52.3 10.4 %collective-permute-start.11 = (bf16[168,768]{1,0:T(8,128)(2,1)S(1)}, bf16[168,768]{1,0:T(8,128)(2,1)S(1)}, u32[]{:S(2)}, u32[]{:S(2)}) collective-permute-start(bf16[168,768]{1,0:T(8,128)(2,1)S(1)} %get-tuple-element.65), channel_id=1, source_target_pairs={{0,24},{1,7},{2,26},{3,1},{4,28},{5,3},{6,30},{7,5},{8,0},{9,15},{... | collective-permute-start | bytes 774152 | tf_op jit(solution)/shard_map/ppermute | solution.py:398
  62.9 6.4 %collective-permute-start.12 = (bf16[104,768]{1,0:T(8,128)(2,1)S(1)}, bf16[104,768]{1,0:T(8,128)(2,1)S(1)}, u32[]{:S(2)}, u32[]{:S(2)}) collective-permute-start(bf16[104,768]{1,0:T(8,128)(2,1)S(1)} %get-tuple-element.67.sent_ref), channel_id=1, source_target_pairs={{0,32},{32,0},{64,96},{96,64},{128,160},{160,128},{192,224},{224,1... | collective-permute-start | bytes 479240 | tf_op jit(solution)/shard_map/ppermute | solution.py:404
  69.4 17.3 %collective-permute-start.13 = (bf16[56,768]{1,0:T(8,128)(2,1)S(1)}, bf16[56,768]{1,0:T(8,128)(2,1)S(1)}, u32[]{:S(2)}, u32[]{:S(2)}) collective-permute-start(bf16[56,768]{1,0:T(8,128)(2,1)S(1)} %get-tuple-element.69), channel_id=1, source_target_pairs={{0,64},{32,96},{64,128},{96,160},{128,192},{160,224},{192,0},{224,... | collective-permute-start | bytes 258056 | tf_op jit(solution)/shard_map/ppermute | solution.py:401
  71.8 14.8 %collective-permute-start.14 = (bf16[56,768]{1,0:T(8,128)(2,1)S(1)}, bf16[56,768]{1,0:T(8,128)(2,1)S(1)}, u32[]{:S(2)}, u32[]{:S(2)}) collective-permute-start(bf16[56,768]{1,0:T(8,128)(2,1)S(1)} %get-tuple-element.70), channel_id=1, source_target_pairs={{0,128},{32,160},{64,192},{96,224},{128,0},{160,32},{192,64},{224,... | collective-permute-start | bytes 258056 | tf_op jit(solution)/shard_map/ppermute | solution.py:401
  77.0 9.6 %collective-permute-start.15 = (bf16[56,768]{1,0:T(8,128)(2,1)S(1)}, bf16[56,768]{1,0:T(8,128)(2,1)S(1)}, u32[]{:S(2)}, u32[]{:S(2)}) collective-permute-start(bf16[56,768]{1,0:T(8,128)(2,1)S(1)} %get-tuple-element.71), channel_id=1, source_target_pairs={{0,192},{32,224},{64,0},{96,32},{128,64},{160,96},{192,128},{224,1... | collective-permute-start | bytes 258056 | tf_op jit(solution)/shard_map/ppermute | solution.py:401

commit v4 on v3

--- a/solution.py
+++ b/solution.py
@@ -374,12 +374,18 @@
 
     z, y, x, core = (lax.axis_index(a) for a in ALL)
     group = lax.iota(jnp.int32, nz * n * n)
-    away_y, away_x = (group // n + n - y) % n, (group + n - x) % n
+    off_y, off_x = (group // n) % n ^ y, group % n ^ x
+
+    def pair_bits(off):
+        first = ((off == 1) | (off == 2)).astype(jnp.int32)
+        second = (off >= 2).astype(jnp.int32)
+        return jnp.where(core == 0, first, second), jnp.where(core == 0, second, first)
+
+    (now_y, then_y), (now_x, then_x) = pair_bits(off_y), pair_bits(off_x)
     to_z = group // (n * n)
-    away_z = (to_z + nz - z) % nz
     odd = (to_z + z) % 2
-    slot_z = odd * (nz // 2) + jnp.where(odd == 1, (to_z + nz - (z ^ 1)) % nz, away_z) // 2
-    ahead = jnp.where(core == 0, away_x, away_y) * n + jnp.where(core == 0, away_y, away_x)
+    slot_z = odd * (nz // 2) + (to_z + nz - (z ^ odd)) % nz // 2
+    ahead = (2 * now_y + now_x) * n + 2 * then_y + then_x
     place = (ahead * nz + slot_z) * own
 
     places = [
@@ -391,9 +397,8 @@
 
     def hop(array, k, stage):
         def to(z, y, x, c):
-            if (c == 0) == (stage == 1):
-                return index(z, y, (x + k) % n, c)
-            return index(z, (y + k) % n, x, c)
+            step = 1 if (c == 0) == (stage == 1) else 3
+            return index(z, y ^ k // 2 * step, x ^ k % 2 * step, c)
 
         return lax.ppermute(array, ALL, [(index(*at), to(*at)) for at in places])
 
@@ -448,7 +453,7 @@
         )
 
     blocks = {}
-    blocks.update(zip((1,), project(1)))
+    blocks.update(zip((1, 2), project(1, 2)))
     (act_grad,) = call(
         matmul_kernel,
         (shape((rows, chans), F32),),
@@ -463,7 +468,7 @@
         scratch=[pltpu.VMEM((rows, LANES), F32)] * 2,
     )
     sums_peer = other_core(sums)
-    blocks.update(zip((2, 3, 0), project(2, 3, 0)))
+    blocks.update(zip((3, 0), project(3, 0)))
     mean, slope, head = call(
         head_kernel,
         (shape((rows, LANES), F32), shape((rows, LANES), F32), shape((tail, chans), BF16)),

time: 87.5 us -> 85.7 us (0.979)
  the two profiles are of different devices: /device:TPU:8 before, /device:TPU:32 now
where the time goes in v4:
time: 85.7 us; the launch traced here: 85.6 us
  starting transfers between devices  32.9 us (38%)
  waiting for transfers between devices  28.4 us (33%)
  Pallas kernels  23.4 us (27%)
    pallas_call x13, Pallas kernels, call(): pl.pallas_call(kernel, out_shape=outs, in_specs=specs or vmem(len(args)),...  16.4 us
    ppermute x9, waiting for transfers between devices, hop(): return lax.ppermute(array, ALL, [(index(*at), to(*at)) for at in places])  16 us
    ppermute x3, starting transfers between devices, hop_z(): return lax.ppermute(array, 'sp_0', [(i, (i + k) % nz) for i in range(nz)])  12.6 us
    ppermute x9, starting transfers between devices, hop(): return lax.ppermute(array, ALL, [(index(*at), to(*at)) for at in places])  11.3 us
    pallas_call x2, Pallas kernels, spread_part(): pl.pallas_call(functools.partial(spread_kernel, part * half), grid=(1,),...  6.96 us
    ppermute x1, starting transfers between devices, previous(): return lax.ppermute(array, SP, [(i, i - 1) for i in range(1, nz * n * n)])  6.52 us
    ppermute x1, waiting for transfers between devices, swap_z(): return lax.ppermute(array, 'sp_0', [(i, i ^ 1) for i in range(nz)])  5.75 us
    ppermute x1, waiting for transfers between devices, previous(): return lax.ppermute(array, SP, [(i, i - 1) for i in range(1, nz * n * n)])  5.34 us
  transfers between devices with their start and end apart: 16, of which 10 were waited for; matrix products, arithmetic and copies ran while one was open for 0% of the time, Pallas kernels for 18%

profile of v4, /device:TPU:32, one launch (start us, length us, event | category | flops | bytes accessed | tf_op | source)
XLA Modules:
  0.0 85.6 jit_solution(6786992495639020951)
XLA Ops:
  0.7 3.3 %shard_map.127 = (f32[512,128]{1,0:T(8,128)S(1)}, bf16[512,768]{1,0:T(8,128)(2,1)S(1)}, bf16[512,2048]{1,0:T(8,128)(2,1)S(1)}, bf16[2048,768]{1,0:T(8,128)(2,1)S(1)}) custom-call(s32[128]{0:T(128)S(1)} %add_multiply_fusion.place_ref, bf16[512,768]{1,0:T(8,128)(2,1)} %conv_hbm.1, bf16[512,2048]{1,0:T(8,128)(2,1)} %grad_hbm.1, bf16[2048,768]{1,0:T(8,128)(2,1)} %weight_hbm.1), custom_call_target="tpu_custom_call" | custom-call | flops 39321600 | bytes 12321280 | tf_op jit(solution)/shard_map/pallas_call | solution.py:29
  4.1 1.3 %shard_map.132.turned_ref = bf16[2048,512]{1,0:T(8,128)(2,1)S(1)} custom-call(s32[128]{0:T(128)S(1)} %add_multiply_fusion.place_ref, bf16[512,2048]{1,0:T(8,128)(2,1)S(1)} %get-tuple-element.42.grad_ref), custom_call_target="tpu_custom_call" | custom-call | flops 805306368 | bytes 4194816 | tf_op jit(solution)/shard_map/pallas_call | solution.py:29
  5.7 1.0 %shard_map.129 = (bf16[512,768]{1,0:T(8,128)(2,1)S(1)}, f32[512,768]{1,0:T(8,128)S(1)}, f32[512,768]{1,0:T(8,128)S(1)}, f32[512,128]{1,0:T(8,128)S(1)}) custom-call(bf16[512,768]{1,0:T(8,128)(2,1)S(1)} %get-tuple-element.44.conv_ref, f32[512,128]{1,0:T(8,128)S(1)} %get-tuple-element.45.own_ref, f32[512,128]{1,0:T(8,128)S(1)} %collective-permute-done.peer_ref, ...), custom_call_target="tpu_custom_call" | custom-call | flops 393216000 | bytes 5511168 | tf_op jit(solution)/shard_map/pallas_call | solution.py:29
  6.6 1.0 %shard_map.134 = (bf16[512,768]{1,0:T(8,128)(2,1)S(1)}, bf16[512,768]{1,0:T(8,128)(2,1)S(1)}) custom-call(bf16[2048,512]{1,0:T(8,128)(2,1)S(1)} %shard_map.132.turned_ref, bf16[512,768]{1,0:T(8,128)(2,1)S(1)} %get-tuple-element.58.active_ref), custom_call_target="tpu_custom_call" | custom-call | flops 805306368 | bytes 4456448 | tf_op jit(solution)/shard_map/pallas_call | solution.py:29
  7.6 1.0 %shard_map.133 = (bf16[512,768]{1,0:T(8,128)(2,1)S(1)}, bf16[512,768]{1,0:T(8,128)(2,1)S(1)}) custom-call(bf16[2048,512]{1,0:T(8,128)(2,1)S(1)} %shard_map.132.turned_ref, bf16[512,768]{1,0:T(8,128)(2,1)S(1)} %get-tuple-element.58.active_ref), custom_call_target="tpu_custom_call" | custom-call | flops 805306368 | bytes 4456448 | tf_op jit(solution)/shard_map/pallas_call | solution.py:29
  8.6 1.6 %collective-permute-start.3 = (bf16[512,768]{1,0:T(8,128)(2,1)S(1)}, bf16[512,768]{1,0:T(8,128)(2,1)S(1)}, u32[]{:S(2)}, u32[]{:S(2)}) collective-permute-start(bf16[512,768]{1,0:T(8,128)(2,1)S(1)} %get-tuple-element.60), channel_id=1, source_target_pairs={{0,2},{1,7},{2,0},{3,5},{4,6},{5,3},{6,4},{7,1},{8,10},{9,15},{10,... | collective-permute-start | bytes 2359304 | tf_op jit(solution)/shard_map/ppermute | solution.py:403
  10.2 1.6 %collective-permute-start.4 = (bf16[512,768]{1,0:T(8,128)(2,1)S(1)}, bf16[512,768]{1,0:T(8,128)(2,1)S(1)}, u32[]{:S(2)}, u32[]{:S(2)}) collective-permute-start(bf16[512,768]{1,0:T(8,128)(2,1)S(1)} %get-tuple-element.61), channel_id=1, source_target_pairs={{0,8},{1,25},{2,10},{3,27},{4,12},{5,29},{6,14},{7,31},{8,0},{9,17... | collective-permute-start | bytes 2359304 | tf_op jit(solution)/shard_map/ppermute | solution.py:403
  11.7 0.4 collective-permute-start.5
  12.2 1.8 %shard_map.128.act_grad_ref = f32[512,768]{1,0:T(8,128)S(1)} custom-call(bf16[512,2048]{1,0:T(8,128)(2,1)S(1)} %get-tuple-element.42.grad_ref, bf16[2048,768]{1,0:T(8,128)(2,1)S(1)} %get-tuple-element.43.weight_ref), custom_call_target="tpu_custom_call" | custom-call | flops 1610612736 | bytes 6815744 | tf_op jit(solution)/shard_map/pallas_call | solution.py:29
  14.0 0.9 %shard_map.130 = (f32[512,768]{1,0:T(8,128)S(1)}, f32[512,128]{1,0:T(8,128)S(1)}, f32[2,768]{1,0:T(2,128)S(1)}) custom-call(f32[512,768]{1,0:T(8,128)S(1)} %shard_map.128.act_grad_ref, f32[512,768]{1,0:T(8,128)S(1)} %get-tuple-element.46.normed_ref, f32[512,768]{1,0:T(8,128)S(1)} %get-tuple-element.47.deriv_ref, f32[512,128]{1,0:T(8,128)S(1)} %get-tuple-element.48.inv_ref, ...), custom_call_target="tpu_custom_call" | custom-call | flops 393216000 | bytes 6824960 | tf_op jit(solution)/shard_map/pallas_call | solution.py:29
  14.9 2.1 %collective-permute-start.1 = (f32[512,128]{1,0:T(8,128)S(1)}, f32[512,128]{1,0:T(8,128)S(1)}, u32[]{:S(2)}, u32[]{:S(2)}) collective-permute-start(f32[512,128]{1,0:T(8,128)S(1)} %get-tuple-element.50.sums_ref), channel_id=1, source_target_pairs={{0,1},{1,0},{2,3},{3,2},{4,5},{5,4},{6,7},{7,6},{8,9},{9,8},{10,11... | collective-permute-start | bytes 786440 | tf_op jit(solution)/shard_map/ppermute | solution.py:412
  17.0 1.2 %collective-permute-done.1.sums_peer_ref = f32[512,128]{1,0:T(8,128)S(1)} collective-permute-done((f32[512,128]{1,0:T(8,128)S(1)}, f32[512,128]{1,0:T(8,128)S(1)}, u32[]{:S(2)}, u32[]{:S(2)}) %collective-permute-start.1) | collective-permute-done | bytes 262176 | tf_op jit(solution)/shard_map/ppermute | solution.py:412
  18.3 6.5 %collective-permute-start.2 = (bf16[32,768]{1,0:T(8,128)(2,1)S(1)}, bf16[32,768]{1,0:T(8,128)(2,1)S(1)}, u32[]{:S(2)}, u32[]{:S(2)}) collective-permute-start(bf16[32,768]{1,0:T(8,128)(2,1)S(1)} %get-tuple-element.53), channel_id=1, source_target_pairs={{2,0},{4,2},{6,4},{8,6},{10,8},{12,10},{14,12},{16,14},{18,16},{20... | collective-permute-start | bytes 147464 | tf_op jit(solution)/shard_map/ppermute | solution.py:415
  24.9 5.3 %collective-permute-done.2.halo_ref = bf16[32,768]{1,0:T(8,128)(2,1)S(1)} collective-permute-done((bf16[32,768]{1,0:T(8,128)(2,1)S(1)}, bf16[32,768]{1,0:T(8,128)(2,1)S(1)}, u32[]{:S(2)}, u32[]{:S(2)}) %collective-permute-start.2) | collective-permute-done | bytes 49184 | tf_op jit(solution)/shard_map/ppermute | solution.py:415
  30.2 4.7 %shard_map.135.refs_4_ = bf16[40,768]{1,0:T(8,128)(2,1)S(1)} custom-call(bf16[512,768]{1,0:T(8,128)(2,1)S(1)} %copy-done, bf16[512,768]{1,0:T(8,128)(2,1)S(1)} %copy-done.1, f32[512,768]{1,0:T(8,128)S(1)} %get-tuple-element.49.lifted_ref, f32[512,768]{1,0:T(8,128)S(1)} %get-tuple-element.46.normed_ref, f32[512,128]{1,0:T(8,128)S(1)} %get-tuple-element.51.mean_ref, ...), custom_call_target="tpu_custom_call" | custom-call | flops 487587840 | bytes 5359616 | tf_op jit(solution)/shard_map/pallas_call | solution.py:29
  35.0 0.6 collective-permute-start.8
  35.6 1.1 %collective-permute-start.7 = (bf16[40,768]{1,0:T(8,128)(2,1)S(1)}, bf16[40,768]{1,0:T(8,128)(2,1)S(1)}, u32[]{:S(2)}, u32[]{:S(2)}) collective-permute-start(bf16[40,768]{1,0:T(8,128)(2,1)S(1)} %shard_map.135.refs_4_), channel_id=1, source_target_pairs={{0,8},{1,25},{2,10},{3,27},{4,12},{5,29},{6,14},{7,31},{8,0},{9,17... | collective-permute-start | bytes 184328 | tf_op jit(solution)/shard_map/ppermute | solution.py:403
  36.7 3.5 %collective-permute-done.8.refs_7_ = bf16[40,768]{1,0:T(8,128)(2,1)S(1)} collective-permute-done((bf16[40,768]{1,0:T(8,128)(2,1)S(1)}, bf16[40,768]{1,0:T(8,128)(2,1)S(1)}, u32[]{:S(2)}, u32[]{:S(2)}) %collective-permute-start.8) | collective-permute-done | bytes 61472 | tf_op jit(solution)/shard_map/ppermute | solution.py:403
  40.5 4.0 %collective-permute-done.6.refs_5_ = bf16[40,768]{1,0:T(8,128)(2,1)S(1)} collective-permute-done((bf16[40,768]{1,0:T(8,128)(2,1)S(1)}, bf16[40,768]{1,0:T(8,128)(2,1)S(1)}, u32[]{:S(2)}, u32[]{:S(2)}) %collective-permute-start.6) | collective-permute-done | bytes 61472 | tf_op jit(solution)/shard_map/ppermute | solution.py:403
  44.9 1.7 %collective-permute-start.9 = (bf16[168,768]{1,0:T(8,128)(2,1)S(1)}, bf16[168,768]{1,0:T(8,128)(2,1)S(1)}, u32[]{:S(2)}, u32[]{:S(2)}) collective-permute-start(bf16[168,768]{1,0:T(8,128)(2,1)S(1)} %get-tuple-element.65), channel_id=1, source_target_pairs={{0,6},{1,3},{2,4},{3,1},{4,2},{5,7},{6,0},{7,5},{8,14},{9,11},{10,... | collective-permute-start | bytes 774152 | tf_op jit(solution)/shard_map/ppermute | solution.py:403
  46.6 2.9 %collective-permute-start.10 = (bf16[168,768]{1,0:T(8,128)(2,1)S(1)}, bf16[168,768]{1,0:T(8,128)(2,1)S(1)}, u32[]{:S(2)}, u32[]{:S(2)}) collective-permute-start(bf16[168,768]{1,0:T(8,128)(2,1)S(1)} %get-tuple-element.66), channel_id=1, source_target_pairs={{0,24},{1,9},{2,26},{3,11},{4,28},{5,13},{6,30},{7,15},{8,16},{9,1... | collective-permute-start | bytes 774152 | tf_op jit(solution)/shard_map/ppermute | solution.py:403
  49.5 1.4 %collective-permute-start.11 = (bf16[168,768]{1,0:T(8,128)(2,1)S(1)}, bf16[168,768]{1,0:T(8,128)(2,1)S(1)}, u32[]{:S(2)}, u32[]{:S(2)}) collective-permute-start(bf16[168,768]{1,0:T(8,128)(2,1)S(1)} %get-tuple-element.67), channel_id=1, source_target_pairs={{0,30},{1,11},{2,28},{3,9},{4,26},{5,15},{6,24},{7,13},{8,22},{9,3... | collective-permute-start | bytes 774152 | tf_op jit(solution)/shard_map/ppermute | solution.py:403
  50.9 1.6 %collective-permute-done.9.refs_1_ = bf16[168,768]{1,0:T(8,128)(2,1)S(1)} collective-permute-done((bf16[168,768]{1,0:T(8,128)(2,1)S(1)}, bf16[168,768]{1,0:T(8,128)(2,1)S(1)}, u32[]{:S(2)}, u32[]{:S(2)}) %collective-permute-start.9) | collective-permute-done | bytes 258080 | tf_op jit(solution)/shard_map/ppermute | solution.py:403
  52.6 3.6 %collective-permute-done.10.refs_2_ = bf16[168,768]{1,0:T(8,128)(2,1)S(1)} collective-permute-done((bf16[168,768]{1,0:T(8,128)(2,1)S(1)}, bf16[168,768]{1,0:T(8,128)(2,1)S(1)}, u32[]{:S(2)}, u32[]{:S(2)}) %collective-permute-start.10) | collective-permute-done | bytes 258080 | tf_op jit(solution)/shard_map/ppermute | solution.py:403
  56.1 3.0 %collective-permute-done.11.refs_3_ = bf16[168,768]{1,0:T(8,128)(2,1)S(1)} collective-permute-done((bf16[168,768]{1,0:T(8,128)(2,1)S(1)}, bf16[168,768]{1,0:T(8,128)(2,1)S(1)}, u32[]{:S(2)}, u32[]{:S(2)}) %collective-permute-start.11) | collective-permute-done | bytes 258080 | tf_op jit(solution)/shard_map/ppermute | solution.py:403
  59.5 5.8 %collective-permute-done.12.came_ref = bf16[104,768]{1,0:T(8,128)(2,1)S(1)} collective-permute-done((bf16[104,768]{1,0:T(8,128)(2,1)S(1)}, bf16[104,768]{1,0:T(8,128)(2,1)S(1)}, u32[]{:S(2)}, u32[]{:S(2)}) %collective-permute-start.12) | collective-permute-done | bytes 159776 | tf_op jit(solution)/shard_map/ppermute | solution.py:409
  65.3 5.4 %collective-permute-start.13 = (bf16[56,768]{1,0:T(8,128)(2,1)S(1)}, bf16[56,768]{1,0:T(8,128)(2,1)S(1)}, u32[]{:S(2)}, u32[]{:S(2)}) collective-permute-start(bf16[56,768]{1,0:T(8,128)(2,1)S(1)} %get-tuple-element.71), channel_id=1, source_target_pairs={{0,64},{32,96},{64,128},{96,160},{128,192},{160,224},{192,0},{224,... | collective-permute-start | bytes 258056 | tf_op jit(solution)/shard_map/ppermute | solution.py:406
  70.6 3.2 %collective-permute-start.14 = (bf16[56,768]{1,0:T(8,128)(2,1)S(1)}, bf16[56,768]{1,0:T(8,128)(2,1)S(1)}, u32[]{:S(2)}, u32[]{:S(2)}) collective-permute-start(bf16[56,768]{1,0:T(8,128)(2,1)S(1)} %get-tuple-element.72), channel_id=1, source_target_pairs={{0,128},{32,160},{64,192},{96,224},{128,0},{160,32},{192,64},{224,... | collective-permute-start | bytes 258056 | tf_op jit(solution)/shard_map/ppermute | solution.py:406
  73.9 4.0 %collective-permute-start.15 = (bf16[56,768]{1,0:T(8,128)(2,1)S(1)}, bf16[56,768]{1,0:T(8,128)(2,1)S(1)}, u32[]{:S(2)}, u32[]{:S(2)}) collective-permute-start(bf16[56,768]{1,0:T(8,128)(2,1)S(1)} %get-tuple-element.73), channel_id=1, source_target_pairs={{0,192},{32,224},{64,0},{96,32},{128,64},{160,96},{192,128},{224,1... | collective-permute-start | bytes 258056 | tf_op jit(solution)/shard_map/ppermute | solution.py:406
  77.9 3.5 %spread.2 = (bf16[512,768]{1,0:T(8,128)(2,1)}, bf16[512,768]{1,0:T(8,128)(2,1)}) custom-call(bf16[512,768]{1,0:T(8,128)(2,1)S(1)} %copy-done, bf16[512,768]{1,0:T(8,128)(2,1)S(1)} %copy-done.1, f32[512,768]{1,0:T(8,128)S(1)} %get-tuple-element.49.lifted_ref, f32[512,768]{1,0:T(8,128)S(1)} %get-tuple-element.46.normed_ref, ...), custom_call_target="tpu_custom_call" | custom-call | flops 243793920 | bytes 3932160 | tf_op jit(solution)/shard_map/spread/pallas_call | solution.py:497
  81.3 3.5 %spread.3 = (bf16[512,768]{1,0:T(8,128)(2,1)}, bf16[512,768]{1,0:T(8,128)(2,1)}) custom-call(bf16[512,768]{1,0:T(8,128)(2,1)S(1)} %copy-done, bf16[512,768]{1,0:T(8,128)(2,1)S(1)} %copy-done.1, f32[512,768]{1,0:T(8,128)S(1)} %get-tuple-element.49.lifted_ref, ...), custom_call_target="tpu_custom_call", output_to_operand_aliasing={{0}: (8, {}), {1}: (9, {})} | custom-call | flops 243793920 | bytes 3932160 | tf_op jit(solution)/shard_map/spread/pallas_call | solution.py:497
  84.9 0.7 shard_map.139
  (26 shorter events, 1.5 us)
Async XLA Ops:
  4.0 1.6 %collective-permute-start = (f32[512,128]{1,0:T(8,128)S(1)}, f32[512,128]{1,0:T(8,128)S(1)}, u32[]{:S(2)}, u32[]{:S(2)}) collective-permute-start(f32[512,128]{1,0:T(8,128)S(1)} %get-tuple-element.45.own_ref), channel_id=1, source_target_pairs={{0,1},{1,0},{2,3},{3,2},{4,5},{5,4},{6,7},{7,6},{8,9},{9,8},{10,11... | collective-permute-start | bytes 786440 | tf_op jit(solution)/shard_map/ppermute | solution.py:412
  4.1 1.5 %copy-start.3 = (f32[768]{0:T(1024)S(1)}, f32[768]{0:T(1024)}, u32[]{:S(2)}) copy-start(f32[768]{0:T(1024)} %gain_ref.3) | copy-start | bytes 9220
  4.1 1.5 %copy-start.4 = (f32[768]{0:T(1024)S(1)}, f32[768]{0:T(1024)}, u32[]{:S(2)}) copy-start(f32[768]{0:T(1024)} %shift_ref.1) | copy-start | bytes 9220
  8.6 35.9 %collective-permute-start.3 = (bf16[512,768]{1,0:T(8,128)(2,1)S(1)}, bf16[512,768]{1,0:T(8,128)(2,1)S(1)}, u32[]{:S(2)}, u32[]{:S(2)}) collective-permute-start(bf16[512,768]{1,0:T(8,128)(2,1)S(1)} %get-tuple-element.60), channel_id=1, source_target_pairs={{0,2},{1,7},{2,0},{3,5},{4,6},{5,3},{6,4},{7,1},{8,10},{9,15},{10,... | collective-permute-start | bytes 2359304 | tf_op jit(solution)/shard_map/ppermute | solution.py:403
  10.2 34.3 %collective-permute-start.4 = (bf16[512,768]{1,0:T(8,128)(2,1)S(1)}, bf16[512,768]{1,0:T(8,128)(2,1)S(1)}, u32[]{:S(2)}, u32[]{:S(2)}) collective-permute-start(bf16[512,768]{1,0:T(8,128)(2,1)S(1)} %get-tuple-element.61), channel_id=1, source_target_pairs={{0,8},{1,25},{2,10},{3,27},{4,12},{5,29},{6,14},{7,31},{8,0},{9,17... | collective-permute-start | bytes 2359304 | tf_op jit(solution)/shard_map/ppermute | solution.py:403
  11.7 32.7 %collective-permute-start.5 = (bf16[512,768]{1,0:T(8,128)(2,1)S(1)}, bf16[512,768]{1,0:T(8,128)(2,1)S(1)}, u32[]{:S(2)}, u32[]{:S(2)}) collective-permute-start(bf16[512,768]{1,0:T(8,128)(2,1)S(1)} %get-tuple-element.62), channel_id=1, source_target_pairs={{0,10},{1,31},{2,8},{3,29},{4,14},{5,27},{6,12},{7,25},{8,2},{9,23... | collective-permute-start | bytes 2359304 | tf_op jit(solution)/shard_map/ppermute | solution.py:403
  14.9 15.3 %copy-start = (bf16[512,768]{1,0:T(8,128)(2,1)S(1)}, bf16[512,768]{1,0:T(8,128)(2,1)}, u32[]{:S(2)}) copy-start(bf16[512,768]{1,0:T(8,128)(2,1)} %value_ref.5) | copy-start | bytes 2359300
  14.9 15.3 %copy-start.1 = (bf16[512,768]{1,0:T(8,128)(2,1)S(1)}, bf16[512,768]{1,0:T(8,128)(2,1)}, u32[]{:S(2)}) copy-start(bf16[512,768]{1,0:T(8,128)(2,1)} %gate_ref.5) | copy-start | bytes 2359300
  14.9 3.3 %collective-permute-start.1 = (f32[512,128]{1,0:T(8,128)S(1)}, f32[512,128]{1,0:T(8,128)S(1)}, u32[]{:S(2)}, u32[]{:S(2)}) collective-permute-start(f32[512,128]{1,0:T(8,128)S(1)} %get-tuple-element.50.sums_ref), channel_id=1, source_target_pairs={{0,1},{1,0},{2,3},{3,2},{4,5},{5,4},{6,7},{7,6},{8,9},{9,8},{10,11... | collective-permute-start | bytes 786440 | tf_op jit(solution)/shard_map/ppermute | solution.py:412
  18.3 11.9 %collective-permute-start.2 = (bf16[32,768]{1,0:T(8,128)(2,1)S(1)}, bf16[32,768]{1,0:T(8,128)(2,1)S(1)}, u32[]{:S(2)}, u32[]{:S(2)}) collective-permute-start(bf16[32,768]{1,0:T(8,128)(2,1)S(1)} %get-tuple-element.53), channel_id=1, source_target_pairs={{2,0},{4,2},{6,4},{8,6},{10,8},{12,10},{14,12},{16,14},{18,16},{20... | collective-permute-start | bytes 147464 | tf_op jit(solution)/shard_map/ppermute | solution.py:415
  35.0 5.3 %collective-permute-start.8 = (bf16[40,768]{1,0:T(8,128)(2,1)S(1)}, bf16[40,768]{1,0:T(8,128)(2,1)S(1)}, u32[]{:S(2)}, u32[]{:S(2)}) collective-permute-start(bf16[40,768]{1,0:T(8,128)(2,1)S(1)} %shard_map.135.refs_4_), channel_id=1, source_target_pairs={{0,10},{1,31},{2,8},{3,29},{4,14},{5,27},{6,12},{7,25},{8,2},{9,23... | collective-permute-start | bytes 184328 | tf_op jit(solution)/shard_map/ppermute | solution.py:403
  35.6 4.9 %collective-permute-start.7 = (bf16[40,768]{1,0:T(8,128)(2,1)S(1)}, bf16[40,768]{1,0:T(8,128)(2,1)S(1)}, u32[]{:S(2)}, u32[]{:S(2)}) collective-permute-start(bf16[40,768]{1,0:T(8,128)(2,1)S(1)} %shard_map.135.refs_4_), channel_id=1, source_target_pairs={{0,8},{1,25},{2,10},{3,27},{4,12},{5,29},{6,14},{7,31},{8,0},{9,17... | collective-permute-start | bytes 184328 | tf_op jit(solution)/shard_map/ppermute | solution.py:403
  40.3 4.2 %collective-permute-start.6 = (bf16[40,768]{1,0:T(8,128)(2,1)S(1)}, bf16[40,768]{1,0:T(8,128)(2,1)S(1)}, u32[]{:S(2)}, u32[]{:S(2)}) collective-permute-start(bf16[40,768]{1,0:T(8,128)(2,1)S(1)} %shard_map.135.refs_4_), channel_id=1, source_target_pairs={{0,2},{1,7},{2,0},{3,5},{4,6},{5,3},{6,4},{7,1},{8,10},{9,15},{10,... | collective-permute-start | bytes 184328 | tf_op jit(solution)/shard_map/ppermute | solution.py:403
  44.5 33.4 %copy-start.2 = (bf16[31,768]{1,0:T(8,128)(2,1)S(1)}, bf16[31,768]{1,0:T(8,128)(2,1)}, u32[]{:S(2)}) copy-start(bf16[31,768]{1,0:T(8,128)(2,1)} %taps_ref.3) | copy-start | bytes 142852
  44.9 7.6 %collective-permute-start.9 = (bf16[168,768]{1,0:T(8,128)(2,1)S(1)}, bf16[168,768]{1,0:T(8,128)(2,1)S(1)}, u32[]{:S(2)}, u32[]{:S(2)}) collective-permute-start(bf16[168,768]{1,0:T(8,128)(2,1)S(1)} %get-tuple-element.65), channel_id=1, source_target_pairs={{0,6},{1,3},{2,4},{3,1},{4,2},{5,7},{6,0},{7,5},{8,14},{9,11},{10,... | collective-permute-start | bytes 774152 | tf_op jit(solution)/shard_map/ppermute | solution.py:403
  46.6 9.6 %collective-permute-start.10 = (bf16[168,768]{1,0:T(8,128)(2,1)S(1)}, bf16[168,768]{1,0:T(8,128)(2,1)S(1)}, u32[]{:S(2)}, u32[]{:S(2)}) collective-permute-start(bf16[168,768]{1,0:T(8,128)(2,1)S(1)} %get-tuple-element.66), channel_id=1, source_target_pairs={{0,24},{1,9},{2,26},{3,11},{4,28},{5,13},{6,30},{7,15},{8,16},{9,1... | collective-permute-start | bytes 774152 | tf_op jit(solution)/shard_map/ppermute | solution.py:403
  49.5 9.6 %collective-permute-start.11 = (bf16[168,768]{1,0:T(8,128)(2,1)S(1)}, bf16[168,768]{1,0:T(8,128)(2,1)S(1)}, u32[]{:S(2)}, u32[]{:S(2)}) collective-permute-start(bf16[168,768]{1,0:T(8,128)(2,1)S(1)} %get-tuple-element.67), channel_id=1, source_target_pairs={{0,30},{1,11},{2,28},{3,9},{4,26},{5,15},{6,24},{7,13},{8,22},{9,3... | collective-permute-start | bytes 774152 | tf_op jit(solution)/shard_map/ppermute | solution.py:403
  59.3 5.9 %collective-permute-start.12 = (bf16[104,768]{1,0:T(8,128)(2,1)S(1)}, bf16[104,768]{1,0:T(8,128)(2,1)S(1)}, u32[]{:S(2)}, u32[]{:S(2)}) collective-permute-start(bf16[104,768]{1,0:T(8,128)(2,1)S(1)} %get-tuple-element.69.sent_ref), channel_id=1, source_target_pairs={{0,32},{32,0},{64,96},{96,64},{128,160},{160,128},{192,224},{224,1... | collective-permute-start | bytes 479240 | tf_op jit(solution)/shard_map/ppermute | solution.py:409
  65.3 19.6 %collective-permute-start.13 = (bf16[56,768]{1,0:T(8,128)(2,1)S(1)}, bf16[56,768]{1,0:T(8,128)(2,1)S(1)}, u32[]{:S(2)}, u32[]{:S(2)}) collective-permute-start(bf16[56,768]{1,0:T(8,128)(2,1)S(1)} %get-tuple-element.71), channel_id=1, source_target_pairs={{0,64},{32,96},{64,128},{96,160},{128,192},{160,224},{192,0},{224,... | collective-permute-start | bytes 258056 | tf_op jit(solution)/shard_map/ppermute | solution.py:406
  70.6 14.2 %collective-permute-start.14 = (bf16[56,768]{1,0:T(8,128)(2,1)S(1)}, bf16[56,768]{1,0:T(8,128)(2,1)S(1)}, u32[]{:S(2)}, u32[]{:S(2)}) collective-permute-start(bf16[56,768]{1,0:T(8,128)(2,1)S(1)} %get-tuple-element.72), channel_id=1, source_target_pairs={{0,128},{32,160},{64,192},{96,224},{128,0},{160,32},{192,64},{224,... | collective-permute-start | bytes 258056 | tf_op jit(solution)/shard_map/ppermute | solution.py:406
  73.9 11.0 %collective-permute-start.15 = (bf16[56,768]{1,0:T(8,128)(2,1)S(1)}, bf16[56,768]{1,0:T(8,128)(2,1)S(1)}, u32[]{:S(2)}, u32[]{:S(2)}) collective-permute-start(bf16[56,768]{1,0:T(8,128)(2,1)S(1)} %get-tuple-element.73), channel_id=1, source_target_pairs={{0,192},{32,224},{64,0},{96,32},{128,64},{160,96},{192,128},{224,1... | collective-permute-start | bytes 258056 | tf_op jit(solution)/shard_map/ppermute | solution.py:406

commit v5 on v4

--- a/solution.py
+++ b/solution.py
@@ -56,13 +56,11 @@
 
 
 def stats_kernel(
-    place_ref, conv_hbm, grad_hbm, weight_hbm, stats_ref, conv_ref, grad_ref, weight_ref,
-    conv_sem, grad_sem, weight_sem,
+    place_ref, conv_hbm, grad_hbm, stats_ref, conv_ref, grad_ref, conv_sem, grad_sem
 ):
     loads = [
         pltpu.make_async_copy(conv_hbm, conv_ref, conv_sem),
         pltpu.make_async_copy(grad_hbm, grad_ref, grad_sem),
-        pltpu.make_async_copy(weight_hbm, weight_ref, weight_sem),
     ]
     for load in loads:
         load.start()
@@ -81,8 +79,7 @@
             off = conv_ref[at, c].astype(F32) - mean
             spread = spread + off * off
         stats_ref[at, :] = jnp.where(left, total, jnp.sum(spread, axis=1, keepdims=True))
-    for load in loads[1:]:
-        load.wait()
+    loads[1].wait()
 
 
 def turn_kernel(place_ref, grad_ref, turned_ref):
@@ -414,16 +411,15 @@
     def previous(array):
         return lax.ppermute(array, SP, [(i, i - 1) for i in range(1, nz * n * n)])
 
-    stats, height, grads, weights = call(
+    stats, height, grads = call(
         stats_kernel,
         (
-            shape((rows, LANES), F32), shape(conv_out.shape, BF16),
-            shape(out_grad.shape, BF16), shape(proj_weight.shape, BF16),
+            shape((rows, LANES), F32), shape(conv_out.shape, BF16), shape(out_grad.shape, BF16),
         ),
-        place, *(pltpu.with_memory_space_constraint(a, pltpu.HBM) for a in (conv_out, out_grad, proj_weight)),
+        place, *(pltpu.with_memory_space_constraint(a, pltpu.HBM) for a in (conv_out, out_grad)),
         flops=rows * chans * 100,
-        scratch=[pltpu.SemaphoreType.DMA] * 3,
-        specs=[pl.BlockSpec(memory_space=pltpu.SMEM)] + [pl.BlockSpec(memory_space=pltpu.HBM)] * 3,
+        scratch=[pltpu.SemaphoreType.DMA] * 2,
+        specs=[pl.BlockSpec(memory_space=pltpu.SMEM)] + [pl.BlockSpec(memory_space=pltpu.HBM)] * 2,
     )
     stats_peer = other_core(stats)
     (turned,) = call(
@@ -457,7 +453,7 @@
     (act_grad,) = call(
         matmul_kernel,
         (shape((rows, chans), F32),),
-        grads, weights,
+        grads, proj_weight,
         flops=2 * rows * width * chans,
     )
     lifted, sums, params = call(

time: 85.7 us -> 84.8 us (0.989)
  Pallas kernels: 23.4 us -> 22.4 us
    pallas_call x13, Pallas kernels: 16.4 us -> 15.5 us  [call(): pl.pallas_call(kernel, out_shape=outs, in_specs=specs or vmem(len(args)),...]
  transfers between devices with their start and end apart: 16 -> 16, of which waited for: 10 -> 10; matrix products, arithmetic and copies ran while one was open for 0% -> 0% of each run, Pallas kernels for 18% -> 19%
where the time goes in v5:
time: 84.8 us; the launch traced here: 84.6 us
  starting transfers between devices  32.9 us (39%)
  waiting for transfers between devices  28.4 us (33%)
  Pallas kernels  22.4 us (26%)
    ppermute x9, waiting for transfers between devices, hop(): return lax.ppermute(array, ALL, [(index(*at), to(*at)) for at in places])  16 us
    pallas_call x13, Pallas kernels, call(): pl.pallas_call(kernel, out_shape=outs, in_specs=specs or vmem(len(args)),...  15.5 us
    ppermute x3, starting transfers between devices, hop_z(): return lax.ppermute(array, 'sp_0', [(i, (i + k) % nz) for i in range(nz)])  12.6 us
    ppermute x9, starting transfers between devices, hop(): return lax.ppermute(array, ALL, [(index(*at), to(*at)) for at in places])  11.3 us
    pallas_call x2, Pallas kernels, spread_part(): pl.pallas_call(functools.partial(spread_kernel, part * half), grid=(1,),...  6.96 us
    ppermute x1, starting transfers between devices, previous(): return lax.ppermute(array, SP, [(i, i - 1) for i in range(1, nz * n * n)])  6.52 us
    ppermute x1, waiting for transfers between devices, swap_z(): return lax.ppermute(array, 'sp_0', [(i, i ^ 1) for i in range(nz)])  5.75 us
    ppermute x1, waiting for transfers between devices, previous(): return lax.ppermute(array, SP, [(i, i - 1) for i in range(1, nz * n * n)])  5.34 us
  transfers between devices with their start and end apart: 16, of which 10 were waited for; matrix products, arithmetic and copies ran while one was open for 0% of the time, Pallas kernels for 19%

profile of v5, /device:TPU:32, one launch (start us, length us, event | category | flops | bytes accessed | tf_op | source)
XLA Modules:
  0.0 84.6 jit_solution(13775473636390738492)
XLA Ops:
  0.7 2.4 %shard_map.127 = (f32[512,128]{1,0:T(8,128)S(1)}, bf16[512,768]{1,0:T(8,128)(2,1)S(1)}, bf16[512,2048]{1,0:T(8,128)(2,1)S(1)}) custom-call(s32[128]{0:T(128)S(1)} %add_multiply_fusion.place_ref, bf16[512,768]{1,0:T(8,128)(2,1)} %conv_hbm.1, bf16[512,2048]{1,0:T(8,128)(2,1)} %grad_hbm.1), custom_call_target="tpu_custom_call" | custom-call | flops 39321600 | bytes 6029824 | tf_op jit(solution)/shard_map/pallas_call | solution.py:29
  3.2 1.3 %shard_map.132.turned_ref = bf16[2048,512]{1,0:T(8,128)(2,1)S(1)} custom-call(s32[128]{0:T(128)S(1)} %add_multiply_fusion.place_ref, bf16[512,2048]{1,0:T(8,128)(2,1)S(1)} %get-tuple-element.41.grad_ref), custom_call_target="tpu_custom_call" | custom-call | flops 805306368 | bytes 4194816 | tf_op jit(solution)/shard_map/pallas_call | solution.py:29
  4.7 0.9 %shard_map.129 = (bf16[512,768]{1,0:T(8,128)(2,1)S(1)}, f32[512,768]{1,0:T(8,128)S(1)}, f32[512,768]{1,0:T(8,128)S(1)}, f32[512,128]{1,0:T(8,128)S(1)}) custom-call(bf16[512,768]{1,0:T(8,128)(2,1)S(1)} %get-tuple-element.42.conv_ref, f32[512,128]{1,0:T(8,128)S(1)} %get-tuple-element.43.own_ref, f32[512,128]{1,0:T(8,128)S(1)} %collective-permute-done.peer_ref, ...), custom_call_target="tpu_custom_call" | custom-call | flops 393216000 | bytes 5511168 | tf_op jit(solution)/shard_map/pallas_call | solution.py:29
  5.7 1.0 %shard_map.134 = (bf16[512,768]{1,0:T(8,128)(2,1)S(1)}, bf16[512,768]{1,0:T(8,128)(2,1)S(1)}) custom-call(bf16[2048,512]{1,0:T(8,128)(2,1)S(1)} %shard_map.132.turned_ref, bf16[512,768]{1,0:T(8,128)(2,1)S(1)} %get-tuple-element.56.active_ref), custom_call_target="tpu_custom_call" | custom-call | flops 805306368 | bytes 4456448 | tf_op jit(solution)/shard_map/pallas_call | solution.py:29
  6.7 1.0 %shard_map.133 = (bf16[512,768]{1,0:T(8,128)(2,1)S(1)}, bf16[512,768]{1,0:T(8,128)(2,1)S(1)}) custom-call(bf16[2048,512]{1,0:T(8,128)(2,1)S(1)} %shard_map.132.turned_ref, bf16[512,768]{1,0:T(8,128)(2,1)S(1)} %get-tuple-element.56.active_ref), custom_call_target="tpu_custom_call" | custom-call | flops 805306368 | bytes 4456448 | tf_op jit(solution)/shard_map/pallas_call | solution.py:29
  7.7 1.6 %collective-permute-start.3 = (bf16[512,768]{1,0:T(8,128)(2,1)S(1)}, bf16[512,768]{1,0:T(8,128)(2,1)S(1)}, u32[]{:S(2)}, u32[]{:S(2)}) collective-permute-start(bf16[512,768]{1,0:T(8,128)(2,1)S(1)} %get-tuple-element.58), channel_id=1, source_target_pairs={{0,2},{1,7},{2,0},{3,5},{4,6},{5,3},{6,4},{7,1},{8,10},{9,15},{10,... | collective-permute-start | bytes 2359304 | tf_op jit(solution)/shard_map/ppermute | solution.py:400
  9.2 1.6 %collective-permute-start.4 = (bf16[512,768]{1,0:T(8,128)(2,1)S(1)}, bf16[512,768]{1,0:T(8,128)(2,1)S(1)}, u32[]{:S(2)}, u32[]{:S(2)}) collective-permute-start(bf16[512,768]{1,0:T(8,128)(2,1)S(1)} %get-tuple-element.59), channel_id=1, source_target_pairs={{0,8},{1,25},{2,10},{3,27},{4,12},{5,29},{6,14},{7,31},{8,0},{9,17... | collective-permute-start | bytes 2359304 | tf_op jit(solution)/shard_map/ppermute | solution.py:400
  10.8 0.4 collective-permute-start.5
  11.2 1.8 %shard_map.128.act_grad_ref = f32[512,768]{1,0:T(8,128)S(1)} custom-call(bf16[512,2048]{1,0:T(8,128)(2,1)S(1)} %get-tuple-element.41.grad_ref, bf16[2048,768]{1,0:T(8,128)(2,1)S(1)} %copy-done.2), custom_call_target="tpu_custom_call" | custom-call | flops 1610612736 | bytes 6815744 | tf_op jit(solution)/shard_map/pallas_call | solution.py:29
  13.0 0.9 %shard_map.130 = (f32[512,768]{1,0:T(8,128)S(1)}, f32[512,128]{1,0:T(8,128)S(1)}, f32[2,768]{1,0:T(2,128)S(1)}) custom-call(f32[512,768]{1,0:T(8,128)S(1)} %shard_map.128.act_grad_ref, f32[512,768]{1,0:T(8,128)S(1)} %get-tuple-element.44.normed_ref, f32[512,768]{1,0:T(8,128)S(1)} %get-tuple-element.45.deriv_ref, f32[512,128]{1,0:T(8,128)S(1)} %get-tuple-element.46.inv_ref, ...), custom_call_target="tpu_custom_call" | custom-call | flops 393216000 | bytes 6824960 | tf_op jit(solution)/shard_map/pallas_call | solution.py:29
  13.9 2.1 %collective-permute-start.1 = (f32[512,128]{1,0:T(8,128)S(1)}, f32[512,128]{1,0:T(8,128)S(1)}, u32[]{:S(2)}, u32[]{:S(2)}) collective-permute-start(f32[512,128]{1,0:T(8,128)S(1)} %get-tuple-element.48.sums_ref), channel_id=1, source_target_pairs={{0,1},{1,0},{2,3},{3,2},{4,5},{5,4},{6,7},{7,6},{8,9},{9,8},{10,11... | collective-permute-start | bytes 786440 | tf_op jit(solution)/shard_map/ppermute | solution.py:409
  16.1 1.2 %collective-permute-done.1.sums_peer_ref = f32[512,128]{1,0:T(8,128)S(1)} collective-permute-done((f32[512,128]{1,0:T(8,128)S(1)}, f32[512,128]{1,0:T(8,128)S(1)}, u32[]{:S(2)}, u32[]{:S(2)}) %collective-permute-start.1) | collective-permute-done | bytes 262176 | tf_op jit(solution)/shard_map/ppermute | solution.py:409
  17.4 6.5 %collective-permute-start.2 = (bf16[32,768]{1,0:T(8,128)(2,1)S(1)}, bf16[32,768]{1,0:T(8,128)(2,1)S(1)}, u32[]{:S(2)}, u32[]{:S(2)}) collective-permute-start(bf16[32,768]{1,0:T(8,128)(2,1)S(1)} %get-tuple-element.51), channel_id=1, source_target_pairs={{2,0},{4,2},{6,4},{8,6},{10,8},{12,10},{14,12},{16,14},{18,16},{20... | collective-permute-start | bytes 147464 | tf_op jit(solution)/shard_map/ppermute | solution.py:412
  23.9 5.3 %collective-permute-done.2.halo_ref = bf16[32,768]{1,0:T(8,128)(2,1)S(1)} collective-permute-done((bf16[32,768]{1,0:T(8,128)(2,1)S(1)}, bf16[32,768]{1,0:T(8,128)(2,1)S(1)}, u32[]{:S(2)}, u32[]{:S(2)}) %collective-permute-start.2) | collective-permute-done | bytes 49184 | tf_op jit(solution)/shard_map/ppermute | solution.py:412
  29.3 4.7 %shard_map.135.refs_4_ = bf16[40,768]{1,0:T(8,128)(2,1)S(1)} custom-call(bf16[512,768]{1,0:T(8,128)(2,1)S(1)} %copy-done, bf16[512,768]{1,0:T(8,128)(2,1)S(1)} %copy-done.1, f32[512,768]{1,0:T(8,128)S(1)} %get-tuple-element.47.lifted_ref, f32[512,768]{1,0:T(8,128)S(1)} %get-tuple-element.44.normed_ref, f32[512,128]{1,0:T(8,128)S(1)} %get-tuple-element.49.mean_ref, ...), custom_call_target="tpu_custom_call" | custom-call | flops 487587840 | bytes 5359616 | tf_op jit(solution)/shard_map/pallas_call | solution.py:29
  34.0 0.6 collective-permute-start.8
  34.7 1.1 %collective-permute-start.7 = (bf16[40,768]{1,0:T(8,128)(2,1)S(1)}, bf16[40,768]{1,0:T(8,128)(2,1)S(1)}, u32[]{:S(2)}, u32[]{:S(2)}) collective-permute-start(bf16[40,768]{1,0:T(8,128)(2,1)S(1)} %shard_map.135.refs_4_), channel_id=1, source_target_pairs={{0,8},{1,25},{2,10},{3,27},{4,12},{5,29},{6,14},{7,31},{8,0},{9,17... | collective-permute-start | bytes 184328 | tf_op jit(solution)/shard_map/ppermute | solution.py:400
  35.8 3.5 %collective-permute-done.8.refs_7_ = bf16[40,768]{1,0:T(8,128)(2,1)S(1)} collective-permute-done((bf16[40,768]{1,0:T(8,128)(2,1)S(1)}, bf16[40,768]{1,0:T(8,128)(2,1)S(1)}, u32[]{:S(2)}, u32[]{:S(2)}) %collective-permute-start.8) | collective-permute-done | bytes 61472 | tf_op jit(solution)/shard_map/ppermute | solution.py:400
  39.5 4.0 %collective-permute-done.6.refs_5_ = bf16[40,768]{1,0:T(8,128)(2,1)S(1)} collective-permute-done((bf16[40,768]{1,0:T(8,128)(2,1)S(1)}, bf16[40,768]{1,0:T(8,128)(2,1)S(1)}, u32[]{:S(2)}, u32[]{:S(2)}) %collective-permute-start.6) | collective-permute-done | bytes 61472 | tf_op jit(solution)/shard_map/ppermute | solution.py:400
  44.0 1.6 %collective-permute-start.9 = (bf16[168,768]{1,0:T(8,128)(2,1)S(1)}, bf16[168,768]{1,0:T(8,128)(2,1)S(1)}, u32[]{:S(2)}, u32[]{:S(2)}) collective-permute-start(bf16[168,768]{1,0:T(8,128)(2,1)S(1)} %get-tuple-element.63), channel_id=1, source_target_pairs={{0,6},{1,3},{2,4},{3,1},{4,2},{5,7},{6,0},{7,5},{8,14},{9,11},{10,... | collective-permute-start | bytes 774152 | tf_op jit(solution)/shard_map/ppermute | solution.py:400
  45.6 2.9 %collective-permute-start.10 = (bf16[168,768]{1,0:T(8,128)(2,1)S(1)}, bf16[168,768]{1,0:T(8,128)(2,1)S(1)}, u32[]{:S(2)}, u32[]{:S(2)}) collective-permute-start(bf16[168,768]{1,0:T(8,128)(2,1)S(1)} %get-tuple-element.64), channel_id=1, source_target_pairs={{0,24},{1,9},{2,26},{3,11},{4,28},{5,13},{6,30},{7,15},{8,16},{9,1... | collective-permute-start | bytes 774152 | tf_op jit(solution)/shard_map/ppermute | solution.py:400
  48.6 1.4 %collective-permute-start.11 = (bf16[168,768]{1,0:T(8,128)(2,1)S(1)}, bf16[168,768]{1,0:T(8,128)(2,1)S(1)}, u32[]{:S(2)}, u32[]{:S(2)}) collective-permute-start(bf16[168,768]{1,0:T(8,128)(2,1)S(1)} %get-tuple-element.65), channel_id=1, source_target_pairs={{0,30},{1,11},{2,28},{3,9},{4,26},{5,15},{6,24},{7,13},{8,22},{9,3... | collective-permute-start | bytes 774152 | tf_op jit(solution)/shard_map/ppermute | solution.py:400
  50.0 1.6 %collective-permute-done.9.refs_1_ = bf16[168,768]{1,0:T(8,128)(2,1)S(1)} collective-permute-done((bf16[168,768]{1,0:T(8,128)(2,1)S(1)}, bf16[168,768]{1,0:T(8,128)(2,1)S(1)}, u32[]{:S(2)}, u32[]{:S(2)}) %collective-permute-start.9) | collective-permute-done | bytes 258080 | tf_op jit(solution)/shard_map/ppermute | solution.py:400
  51.6 3.6 %collective-permute-done.10.refs_2_ = bf16[168,768]{1,0:T(8,128)(2,1)S(1)} collective-permute-done((bf16[168,768]{1,0:T(8,128)(2,1)S(1)}, bf16[168,768]{1,0:T(8,128)(2,1)S(1)}, u32[]{:S(2)}, u32[]{:S(2)}) %collective-permute-start.10) | collective-permute-done | bytes 258080 | tf_op jit(solution)/shard_map/ppermute | solution.py:400
  55.2 3.0 %collective-permute-done.11.refs_3_ = bf16[168,768]{1,0:T(8,128)(2,1)S(1)} collective-permute-done((bf16[168,768]{1,0:T(8,128)(2,1)S(1)}, bf16[168,768]{1,0:T(8,128)(2,1)S(1)}, u32[]{:S(2)}, u32[]{:S(2)}) %collective-permute-start.11) | collective-permute-done | bytes 258080 | tf_op jit(solution)/shard_map/ppermute | solution.py:400
  58.5 5.8 %collective-permute-done.12.came_ref = bf16[104,768]{1,0:T(8,128)(2,1)S(1)} collective-permute-done((bf16[104,768]{1,0:T(8,128)(2,1)S(1)}, bf16[104,768]{1,0:T(8,128)(2,1)S(1)}, u32[]{:S(2)}, u32[]{:S(2)}) %collective-permute-start.12) | collective-permute-done | bytes 159776 | tf_op jit(solution)/shard_map/ppermute | solution.py:406
  64.3 5.4 %collective-permute-start.13 = (bf16[56,768]{1,0:T(8,128)(2,1)S(1)}, bf16[56,768]{1,0:T(8,128)(2,1)S(1)}, u32[]{:S(2)}, u32[]{:S(2)}) collective-permute-start(bf16[56,768]{1,0:T(8,128)(2,1)S(1)} %get-tuple-element.69), channel_id=1, source_target_pairs={{0,64},{32,96},{64,128},{96,160},{128,192},{160,224},{192,0},{224,... | collective-permute-start | bytes 258056 | tf_op jit(solution)/shard_map/ppermute | solution.py:403
  69.7 3.2 %collective-permute-start.14 = (bf16[56,768]{1,0:T(8,128)(2,1)S(1)}, bf16[56,768]{1,0:T(8,128)(2,1)S(1)}, u32[]{:S(2)}, u32[]{:S(2)}) collective-permute-start(bf16[56,768]{1,0:T(8,128)(2,1)S(1)} %get-tuple-element.70), channel_id=1, source_target_pairs={{0,128},{32,160},{64,192},{96,224},{128,0},{160,32},{192,64},{224,... | collective-permute-start | bytes 258056 | tf_op jit(solution)/shard_map/ppermute | solution.py:403
  72.9 4.0 %collective-permute-start.15 = (bf16[56,768]{1,0:T(8,128)(2,1)S(1)}, bf16[56,768]{1,0:T(8,128)(2,1)S(1)}, u32[]{:S(2)}, u32[]{:S(2)}) collective-permute-start(bf16[56,768]{1,0:T(8,128)(2,1)S(1)} %get-tuple-element.71), channel_id=1, source_target_pairs={{0,192},{32,224},{64,0},{96,32},{128,64},{160,96},{192,128},{224,1... | collective-permute-start | bytes 258056 | tf_op jit(solution)/shard_map/ppermute | solution.py:403
  76.9 3.5 %spread.2 = (bf16[512,768]{1,0:T(8,128)(2,1)}, bf16[512,768]{1,0:T(8,128)(2,1)}) custom-call(bf16[512,768]{1,0:T(8,128)(2,1)S(1)} %copy-done, bf16[512,768]{1,0:T(8,128)(2,1)S(1)} %copy-done.1, f32[512,768]{1,0:T(8,128)S(1)} %get-tuple-element.47.lifted_ref, f32[512,768]{1,0:T(8,128)S(1)} %get-tuple-element.44.normed_ref, ...), custom_call_target="tpu_custom_call" | custom-call | flops 243793920 | bytes 3932160 | tf_op jit(solution)/shard_map/spread/pallas_call | solution.py:493
  80.4 3.5 %spread.3 = (bf16[512,768]{1,0:T(8,128)(2,1)}, bf16[512,768]{1,0:T(8,128)(2,1)}) custom-call(bf16[512,768]{1,0:T(8,128)(2,1)S(1)} %copy-done, bf16[512,768]{1,0:T(8,128)(2,1)S(1)} %copy-done.1, f32[512,768]{1,0:T(8,128)S(1)} %get-tuple-element.47.lifted_ref, ...), custom_call_target="tpu_custom_call", output_to_operand_aliasing={{0}: (8, {}), {1}: (9, {})} | custom-call | flops 243793920 | bytes 3932160 | tf_op jit(solution)/shard_map/spread/pallas_call | solution.py:493
  83.9 0.7 shard_map.139
  (28 shorter events, 1.5 us)
Async XLA Ops:
  3.1 1.6 %collective-permute-start = (f32[512,128]{1,0:T(8,128)S(1)}, f32[512,128]{1,0:T(8,128)S(1)}, u32[]{:S(2)}, u32[]{:S(2)}) collective-permute-start(f32[512,128]{1,0:T(8,128)S(1)} %get-tuple-element.43.own_ref), channel_id=1, source_target_pairs={{0,1},{1,0},{2,3},{3,2},{4,5},{5,4},{6,7},{7,6},{8,9},{9,8},{10,11... | collective-permute-start | bytes 786440 | tf_op jit(solution)/shard_map/ppermute | solution.py:409
  3.2 1.5 %copy-start.4 = (f32[768]{0:T(1024)S(1)}, f32[768]{0:T(1024)}, u32[]{:S(2)}) copy-start(f32[768]{0:T(1024)} %gain_ref.3) | copy-start | bytes 9220
  3.2 1.5 %copy-start.5 = (f32[768]{0:T(1024)S(1)}, f32[768]{0:T(1024)}, u32[]{:S(2)}) copy-start(f32[768]{0:T(1024)} %shift_ref.1) | copy-start | bytes 9220
  5.7 5.6 %copy-start.2 = (bf16[2048,768]{1,0:T(8,128)(2,1)S(1)}, bf16[2048,768]{1,0:T(8,128)(2,1)}, u32[]{:S(2)}) copy-start(bf16[2048,768]{1,0:T(8,128)(2,1)} %weight_ref.1) | copy-start | bytes 9437188
  7.7 35.9 %collective-permute-start.3 = (bf16[512,768]{1,0:T(8,128)(2,1)S(1)}, bf16[512,768]{1,0:T(8,128)(2,1)S(1)}, u32[]{:S(2)}, u32[]{:S(2)}) collective-permute-start(bf16[512,768]{1,0:T(8,128)(2,1)S(1)} %get-tuple-element.58), channel_id=1, source_target_pairs={{0,2},{1,7},{2,0},{3,5},{4,6},{5,3},{6,4},{7,1},{8,10},{9,15},{10,... | collective-permute-start | bytes 2359304 | tf_op jit(solution)/shard_map/ppermute | solution.py:400
  9.2 34.3 %collective-permute-start.4 = (bf16[512,768]{1,0:T(8,128)(2,1)S(1)}, bf16[512,768]{1,0:T(8,128)(2,1)S(1)}, u32[]{:S(2)}, u32[]{:S(2)}) collective-permute-start(bf16[512,768]{1,0:T(8,128)(2,1)S(1)} %get-tuple-element.59), channel_id=1, source_target_pairs={{0,8},{1,25},{2,10},{3,27},{4,12},{5,29},{6,14},{7,31},{8,0},{9,17... | collective-permute-start | bytes 2359304 | tf_op jit(solution)/shard_map/ppermute | solution.py:400
  10.8 32.7 %collective-permute-start.5 = (bf16[512,768]{1,0:T(8,128)(2,1)S(1)}, bf16[512,768]{1,0:T(8,128)(2,1)S(1)}, u32[]{:S(2)}, u32[]{:S(2)}) collective-permute-start(bf16[512,768]{1,0:T(8,128)(2,1)S(1)} %get-tuple-element.60), channel_id=1, source_target_pairs={{0,10},{1,31},{2,8},{3,29},{4,14},{5,27},{6,12},{7,25},{8,2},{9,23... | collective-permute-start | bytes 2359304 | tf_op jit(solution)/shard_map/ppermute | solution.py:400
  13.9 15.3 %copy-start = (bf16[512,768]{1,0:T(8,128)(2,1)S(1)}, bf16[512,768]{1,0:T(8,128)(2,1)}, u32[]{:S(2)}) copy-start(bf16[512,768]{1,0:T(8,128)(2,1)} %value_ref.5) | copy-start | bytes 2359300
  13.9 15.3 %copy-start.1 = (bf16[512,768]{1,0:T(8,128)(2,1)S(1)}, bf16[512,768]{1,0:T(8,128)(2,1)}, u32[]{:S(2)}) copy-start(bf16[512,768]{1,0:T(8,128)(2,1)} %gate_ref.5) | copy-start | bytes 2359300
  13.9 3.3 %collective-permute-start.1 = (f32[512,128]{1,0:T(8,128)S(1)}, f32[512,128]{1,0:T(8,128)S(1)}, u32[]{:S(2)}, u32[]{:S(2)}) collective-permute-start(f32[512,128]{1,0:T(8,128)S(1)} %get-tuple-element.48.sums_ref), channel_id=1, source_target_pairs={{0,1},{1,0},{2,3},{3,2},{4,5},{5,4},{6,7},{7,6},{8,9},{9,8},{10,11... | collective-permute-start | bytes 786440 | tf_op jit(solution)/shard_map/ppermute | solution.py:409
  17.4 11.9 %collective-permute-start.2 = (bf16[32,768]{1,0:T(8,128)(2,1)S(1)}, bf16[32,768]{1,0:T(8,128)(2,1)S(1)}, u32[]{:S(2)}, u32[]{:S(2)}) collective-permute-start(bf16[32,768]{1,0:T(8,128)(2,1)S(1)} %get-tuple-element.51), channel_id=1, source_target_pairs={{2,0},{4,2},{6,4},{8,6},{10,8},{12,10},{14,12},{16,14},{18,16},{20... | collective-permute-start | bytes 147464 | tf_op jit(solution)/shard_map/ppermute | solution.py:412
  34.0 5.3 %collective-permute-start.8 = (bf16[40,768]{1,0:T(8,128)(2,1)S(1)}, bf16[40,768]{1,0:T(8,128)(2,1)S(1)}, u32[]{:S(2)}, u32[]{:S(2)}) collective-permute-start(bf16[40,768]{1,0:T(8,128)(2,1)S(1)} %shard_map.135.refs_4_), channel_id=1, source_target_pairs={{0,10},{1,31},{2,8},{3,29},{4,14},{5,27},{6,12},{7,25},{8,2},{9,23... | collective-permute-start | bytes 184328 | tf_op jit(solution)/shard_map/ppermute | solution.py:400
  34.7 4.9 %collective-permute-start.7 = (bf16[40,768]{1,0:T(8,128)(2,1)S(1)}, bf16[40,768]{1,0:T(8,128)(2,1)S(1)}, u32[]{:S(2)}, u32[]{:S(2)}) collective-permute-start(bf16[40,768]{1,0:T(8,128)(2,1)S(1)} %shard_map.135.refs_4_), channel_id=1, source_target_pairs={{0,8},{1,25},{2,10},{3,27},{4,12},{5,29},{6,14},{7,31},{8,0},{9,17... | collective-permute-start | bytes 184328 | tf_op jit(solution)/shard_map/ppermute | solution.py:400
  39.3 4.2 %collective-permute-start.6 = (bf16[40,768]{1,0:T(8,128)(2,1)S(1)}, bf16[40,768]{1,0:T(8,128)(2,1)S(1)}, u32[]{:S(2)}, u32[]{:S(2)}) collective-permute-start(bf16[40,768]{1,0:T(8,128)(2,1)S(1)} %shard_map.135.refs_4_), channel_id=1, source_target_pairs={{0,2},{1,7},{2,0},{3,5},{4,6},{5,3},{6,4},{7,1},{8,10},{9,15},{10,... | collective-permute-start | bytes 184328 | tf_op jit(solution)/shard_map/ppermute | solution.py:400
  43.6 33.4 %copy-start.3 = (bf16[31,768]{1,0:T(8,128)(2,1)S(1)}, bf16[31,768]{1,0:T(8,128)(2,1)}, u32[]{:S(2)}) copy-start(bf16[31,768]{1,0:T(8,128)(2,1)} %taps_ref.3) | copy-start | bytes 142852
  44.0 7.6 %collective-permute-start.9 = (bf16[168,768]{1,0:T(8,128)(2,1)S(1)}, bf16[168,768]{1,0:T(8,128)(2,1)S(1)}, u32[]{:S(2)}, u32[]{:S(2)}) collective-permute-start(bf16[168,768]{1,0:T(8,128)(2,1)S(1)} %get-tuple-element.63), channel_id=1, source_target_pairs={{0,6},{1,3},{2,4},{3,1},{4,2},{5,7},{6,0},{7,5},{8,14},{9,11},{10,... | collective-permute-start | bytes 774152 | tf_op jit(solution)/shard_map/ppermute | solution.py:400
  45.6 9.6 %collective-permute-start.10 = (bf16[168,768]{1,0:T(8,128)(2,1)S(1)}, bf16[168,768]{1,0:T(8,128)(2,1)S(1)}, u32[]{:S(2)}, u32[]{:S(2)}) collective-permute-start(bf16[168,768]{1,0:T(8,128)(2,1)S(1)} %get-tuple-element.64), channel_id=1, source_target_pairs={{0,24},{1,9},{2,26},{3,11},{4,28},{5,13},{6,30},{7,15},{8,16},{9,1... | collective-permute-start | bytes 774152 | tf_op jit(solution)/shard_map/ppermute | solution.py:400
  48.6 9.6 %collective-permute-start.11 = (bf16[168,768]{1,0:T(8,128)(2,1)S(1)}, bf16[168,768]{1,0:T(8,128)(2,1)S(1)}, u32[]{:S(2)}, u32[]{:S(2)}) collective-permute-start(bf16[168,768]{1,0:T(8,128)(2,1)S(1)} %get-tuple-element.65), channel_id=1, source_target_pairs={{0,30},{1,11},{2,28},{3,9},{4,26},{5,15},{6,24},{7,13},{8,22},{9,3... | collective-permute-start | bytes 774152 | tf_op jit(solution)/shard_map/ppermute | solution.py:400
  58.3 5.9 %collective-permute-start.12 = (bf16[104,768]{1,0:T(8,128)(2,1)S(1)}, bf16[104,768]{1,0:T(8,128)(2,1)S(1)}, u32[]{:S(2)}, u32[]{:S(2)}) collective-permute-start(bf16[104,768]{1,0:T(8,128)(2,1)S(1)} %get-tuple-element.67.sent_ref), channel_id=1, source_target_pairs={{0,32},{32,0},{64,96},{96,64},{128,160},{160,128},{192,224},{224,1... | collective-permute-start | bytes 479240 | tf_op jit(solution)/shard_map/ppermute | solution.py:406
  64.3 19.6 %collective-permute-start.13 = (bf16[56,768]{1,0:T(8,128)(2,1)S(1)}, bf16[56,768]{1,0:T(8,128)(2,1)S(1)}, u32[]{:S(2)}, u32[]{:S(2)}) collective-permute-start(bf16[56,768]{1,0:T(8,128)(2,1)S(1)} %get-tuple-element.69), channel_id=1, source_target_pairs={{0,64},{32,96},{64,128},{96,160},{128,192},{160,224},{192,0},{224,... | collective-permute-start | bytes 258056 | tf_op jit(solution)/shard_map/ppermute | solution.py:403
  69.7 14.2 %collective-permute-start.14 = (bf16[56,768]{1,0:T(8,128)(2,1)S(1)}, bf16[56,768]{1,0:T(8,128)(2,1)S(1)}, u32[]{:S(2)}, u32[]{:S(2)}) collective-permute-start(bf16[56,768]{1,0:T(8,128)(2,1)S(1)} %get-tuple-element.70), channel_id=1, source_target_pairs={{0,128},{32,160},{64,192},{96,224},{128,0},{160,32},{192,64},{224,... | collective-permute-start | bytes 258056 | tf_op jit(solution)/shard_map/ppermute | solution.py:403
  72.9 11.0 %collective-permute-start.15 = (bf16[56,768]{1,0:T(8,128)(2,1)S(1)}, bf16[56,768]{1,0:T(8,128)(2,1)S(1)}, u32[]{:S(2)}, u32[]{:S(2)}) collective-permute-start(bf16[56,768]{1,0:T(8,128)(2,1)S(1)} %get-tuple-element.71), channel_id=1, source_target_pairs={{0,192},{32,224},{64,0},{96,32},{128,64},{160,96},{192,128},{224,1... | collective-permute-start | bytes 258056 | tf_op jit(solution)/shard_map/ppermute | solution.py:403

commit v6 on v5

--- a/solution.py
+++ b/solution.py
@@ -517,7 +517,8 @@
         *landed, *smalls,
         flops=width * chans * 100,
     )
-    then = [second[0]] + [hop(second[k], k, 2) for k in range(1, n)]
+    then_long = hop(second[3], 3, 2)
+    then = [second[0], hop(second[1], 1, 2), hop(second[2], 2, 2), then_long]
     keep, send = call(
         third_kernel,
         (shape((part // 2, chans), F32), shape((part // 2 + extra, chans), BF16)),
@@ -531,7 +532,8 @@
         keep, send, came,
         flops=width * chans * 10,
     )
-    fars = [fourth[0]] + [hop_z(fourth[k], 2 * k) for k in range(1, nz // 2)]
+    long = hop_z(fourth[2], 4)
+    fars = [fourth[0], hop_z(fourth[1], 2), long, hop_z(fourth[3], 6)]
     grad_proj, grad_taps, grad_gain, grad_shift = call(
         functools.partial(last_kernel, taps),
         (shape((own, chans), F32), shape((taps, chans), F32), shape((chans,), F32), shape((chans,), F32)),

time: 84.8 us -> 84.8 us (level)
  no operation moved by 1% of the time
where the time goes in v6:
time: 84.8 us; the launch traced here: 84.6 us
  starting transfers between devices  32.9 us (39%)
  waiting for transfers between devices  28.4 us (33%)
  Pallas kernels  22.4 us (26%)
    ppermute x9, waiting for transfers between devices, hop(): return lax.ppermute(array, ALL, [(index(*at), to(*at)) for at in places])  16 us
    pallas_call x13, Pallas kernels, call(): pl.pallas_call(kernel, out_shape=outs, in_specs=specs or vmem(len(args)),...  15.5 us
    ppermute x3, starting transfers between devices, hop_z(): return lax.ppermute(array, 'sp_0', [(i, (i + k) % nz) for i in range(nz)])  12.6 us
    ppermute x9, starting transfers between devices, hop(): return lax.ppermute(array, ALL, [(index(*at), to(*at)) for at in places])  11.3 us
    pallas_call x2, Pallas kernels, spread_part(): pl.pallas_call(functools.partial(spread_kernel, part * half), grid=(1,),...  6.96 us
    ppermute x1, starting transfers between devices, previous(): return lax.ppermute(array, SP, [(i, i - 1) for i in range(1, nz * n * n)])  6.52 us
    ppermute x1, waiting for transfers between devices, swap_z(): return lax.ppermute(array, 'sp_0', [(i, i ^ 1) for i in range(nz)])  5.75 us
    ppermute x1, waiting for transfers between devices, previous(): return lax.ppermute(array, SP, [(i, i - 1) for i in range(1, nz * n * n)])  5.34 us
  transfers between devices with their start and end apart: 16, of which 10 were waited for; matrix products, arithmetic and copies ran while one was open for 0% of the time, Pallas kernels for 19%

profile of v6, /device:TPU:32, one launch (start us, length us, event | category | flops | bytes accessed | tf_op | source)
XLA Modules:
  0.0 84.6 jit_solution(13775473636390738492)
XLA Ops:
  0.7 2.4 %shard_map.127 = (f32[512,128]{1,0:T(8,128)S(1)}, bf16[512,768]{1,0:T(8,128)(2,1)S(1)}, bf16[512,2048]{1,0:T(8,128)(2,1)S(1)}) custom-call(s32[128]{0:T(128)S(1)} %add_multiply_fusion.place_ref, bf16[512,768]{1,0:T(8,128)(2,1)} %conv_hbm.1, bf16[512,2048]{1,0:T(8,128)(2,1)} %grad_hbm.1), custom_call_target="tpu_custom_call" | custom-call | flops 39321600 | bytes 6029824 | tf_op jit(solution)/shard_map/pallas_call | solution.py:29
  3.2 1.3 %shard_map.132.turned_ref = bf16[2048,512]{1,0:T(8,128)(2,1)S(1)} custom-call(s32[128]{0:T(128)S(1)} %add_multiply_fusion.place_ref, bf16[512,2048]{1,0:T(8,128)(2,1)S(1)} %get-tuple-element.41.grad_ref), custom_call_target="tpu_custom_call" | custom-call | flops 805306368 | bytes 4194816 | tf_op jit(solution)/shard_map/pallas_call | solution.py:29
  4.7 0.9 %shard_map.129 = (bf16[512,768]{1,0:T(8,128)(2,1)S(1)}, f32[512,768]{1,0:T(8,128)S(1)}, f32[512,768]{1,0:T(8,128)S(1)}, f32[512,128]{1,0:T(8,128)S(1)}) custom-call(bf16[512,768]{1,0:T(8,128)(2,1)S(1)} %get-tuple-element.42.conv_ref, f32[512,128]{1,0:T(8,128)S(1)} %get-tuple-element.43.own_ref, f32[512,128]{1,0:T(8,128)S(1)} %collective-permute-done.peer_ref, ...), custom_call_target="tpu_custom_call" | custom-call | flops 393216000 | bytes 5511168 | tf_op jit(solution)/shard_map/pallas_call | solution.py:29
  5.7 1.0 %shard_map.134 = (bf16[512,768]{1,0:T(8,128)(2,1)S(1)}, bf16[512,768]{1,0:T(8,128)(2,1)S(1)}) custom-call(bf16[2048,512]{1,0:T(8,128)(2,1)S(1)} %shard_map.132.turned_ref, bf16[512,768]{1,0:T(8,128)(2,1)S(1)} %get-tuple-element.56.active_ref), custom_call_target="tpu_custom_call" | custom-call | flops 805306368 | bytes 4456448 | tf_op jit(solution)/shard_map/pallas_call | solution.py:29
  6.7 1.0 %shard_map.133 = (bf16[512,768]{1,0:T(8,128)(2,1)S(1)}, bf16[512,768]{1,0:T(8,128)(2,1)S(1)}) custom-call(bf16[2048,512]{1,0:T(8,128)(2,1)S(1)} %shard_map.132.turned_ref, bf16[512,768]{1,0:T(8,128)(2,1)S(1)} %get-tuple-element.56.active_ref), custom_call_target="tpu_custom_call" | custom-call | flops 805306368 | bytes 4456448 | tf_op jit(solution)/shard_map/pallas_call | solution.py:29
  7.7 1.6 %collective-permute-start.3 = (bf16[512,768]{1,0:T(8,128)(2,1)S(1)}, bf16[512,768]{1,0:T(8,128)(2,1)S(1)}, u32[]{:S(2)}, u32[]{:S(2)}) collective-permute-start(bf16[512,768]{1,0:T(8,128)(2,1)S(1)} %get-tuple-element.58), channel_id=1, source_target_pairs={{0,2},{1,7},{2,0},{3,5},{4,6},{5,3},{6,4},{7,1},{8,10},{9,15},{10,... | collective-permute-start | bytes 2359304 | tf_op jit(solution)/shard_map/ppermute | solution.py:400
  9.2 1.6 %collective-permute-start.4 = (bf16[512,768]{1,0:T(8,128)(2,1)S(1)}, bf16[512,768]{1,0:T(8,128)(2,1)S(1)}, u32[]{:S(2)}, u32[]{:S(2)}) collective-permute-start(bf16[512,768]{1,0:T(8,128)(2,1)S(1)} %get-tuple-element.59), channel_id=1, source_target_pairs={{0,8},{1,25},{2,10},{3,27},{4,12},{5,29},{6,14},{7,31},{8,0},{9,17... | collective-permute-start | bytes 2359304 | tf_op jit(solution)/shard_map/ppermute | solution.py:400
  10.8 0.4 collective-permute-start.5
  11.2 1.8 %shard_map.128.act_grad_ref = f32[512,768]{1,0:T(8,128)S(1)} custom-call(bf16[512,2048]{1,0:T(8,128)(2,1)S(1)} %get-tuple-element.41.grad_ref, bf16[2048,768]{1,0:T(8,128)(2,1)S(1)} %copy-done.2), custom_call_target="tpu_custom_call" | custom-call | flops 1610612736 | bytes 6815744 | tf_op jit(solution)/shard_map/pallas_call | solution.py:29
  13.0 0.9 %shard_map.130 = (f32[512,768]{1,0:T(8,128)S(1)}, f32[512,128]{1,0:T(8,128)S(1)}, f32[2,768]{1,0:T(2,128)S(1)}) custom-call(f32[512,768]{1,0:T(8,128)S(1)} %shard_map.128.act_grad_ref, f32[512,768]{1,0:T(8,128)S(1)} %get-tuple-element.44.normed_ref, f32[512,768]{1,0:T(8,128)S(1)} %get-tuple-element.45.deriv_ref, f32[512,128]{1,0:T(8,128)S(1)} %get-tuple-element.46.inv_ref, ...), custom_call_target="tpu_custom_call" | custom-call | flops 393216000 | bytes 6824960 | tf_op jit(solution)/shard_map/pallas_call | solution.py:29
  13.9 2.1 %collective-permute-start.1 = (f32[512,128]{1,0:T(8,128)S(1)}, f32[512,128]{1,0:T(8,128)S(1)}, u32[]{:S(2)}, u32[]{:S(2)}) collective-permute-start(f32[512,128]{1,0:T(8,128)S(1)} %get-tuple-element.48.sums_ref), channel_id=1, source_target_pairs={{0,1},{1,0},{2,3},{3,2},{4,5},{5,4},{6,7},{7,6},{8,9},{9,8},{10,11... | collective-permute-start | bytes 786440 | tf_op jit(solution)/shard_map/ppermute | solution.py:409
  16.1 1.2 %collective-permute-done.1.sums_peer_ref = f32[512,128]{1,0:T(8,128)S(1)} collective-permute-done((f32[512,128]{1,0:T(8,128)S(1)}, f32[512,128]{1,0:T(8,128)S(1)}, u32[]{:S(2)}, u32[]{:S(2)}) %collective-permute-start.1) | collective-permute-done | bytes 262176 | tf_op jit(solution)/shard_map/ppermute | solution.py:409
  17.4 6.5 %collective-permute-start.2 = (bf16[32,768]{1,0:T(8,128)(2,1)S(1)}, bf16[32,768]{1,0:T(8,128)(2,1)S(1)}, u32[]{:S(2)}, u32[]{:S(2)}) collective-permute-start(bf16[32,768]{1,0:T(8,128)(2,1)S(1)} %get-tuple-element.51), channel_id=1, source_target_pairs={{2,0},{4,2},{6,4},{8,6},{10,8},{12,10},{14,12},{16,14},{18,16},{20... | collective-permute-start | bytes 147464 | tf_op jit(solution)/shard_map/ppermute | solution.py:412
  23.9 5.3 %collective-permute-done.2.halo_ref = bf16[32,768]{1,0:T(8,128)(2,1)S(1)} collective-permute-done((bf16[32,768]{1,0:T(8,128)(2,1)S(1)}, bf16[32,768]{1,0:T(8,128)(2,1)S(1)}, u32[]{:S(2)}, u32[]{:S(2)}) %collective-permute-start.2) | collective-permute-done | bytes 49184 | tf_op jit(solution)/shard_map/ppermute | solution.py:412
  29.3 4.7 %shard_map.135.refs_4_ = bf16[40,768]{1,0:T(8,128)(2,1)S(1)} custom-call(bf16[512,768]{1,0:T(8,128)(2,1)S(1)} %copy-done, bf16[512,768]{1,0:T(8,128)(2,1)S(1)} %copy-done.1, f32[512,768]{1,0:T(8,128)S(1)} %get-tuple-element.47.lifted_ref, f32[512,768]{1,0:T(8,128)S(1)} %get-tuple-element.44.normed_ref, f32[512,128]{1,0:T(8,128)S(1)} %get-tuple-element.49.mean_ref, ...), custom_call_target="tpu_custom_call" | custom-call | flops 487587840 | bytes 5359616 | tf_op jit(solution)/shard_map/pallas_call | solution.py:29
  34.0 0.6 collective-permute-start.8
  34.7 1.1 %collective-permute-start.7 = (bf16[40,768]{1,0:T(8,128)(2,1)S(1)}, bf16[40,768]{1,0:T(8,128)(2,1)S(1)}, u32[]{:S(2)}, u32[]{:S(2)}) collective-permute-start(bf16[40,768]{1,0:T(8,128)(2,1)S(1)} %shard_map.135.refs_4_), channel_id=1, source_target_pairs={{0,8},{1,25},{2,10},{3,27},{4,12},{5,29},{6,14},{7,31},{8,0},{9,17... | collective-permute-start | bytes 184328 | tf_op jit(solution)/shard_map/ppermute | solution.py:400
  35.8 3.5 %collective-permute-done.8.refs_7_ = bf16[40,768]{1,0:T(8,128)(2,1)S(1)} collective-permute-done((bf16[40,768]{1,0:T(8,128)(2,1)S(1)}, bf16[40,768]{1,0:T(8,128)(2,1)S(1)}, u32[]{:S(2)}, u32[]{:S(2)}) %collective-permute-start.8) | collective-permute-done | bytes 61472 | tf_op jit(solution)/shard_map/ppermute | solution.py:400
  39.5 4.0 %collective-permute-done.6.refs_5_ = bf16[40,768]{1,0:T(8,128)(2,1)S(1)} collective-permute-done((bf16[40,768]{1,0:T(8,128)(2,1)S(1)}, bf16[40,768]{1,0:T(8,128)(2,1)S(1)}, u32[]{:S(2)}, u32[]{:S(2)}) %collective-permute-start.6) | collective-permute-done | bytes 61472 | tf_op jit(solution)/shard_map/ppermute | solution.py:400
  44.0 1.6 %collective-permute-start.9 = (bf16[168,768]{1,0:T(8,128)(2,1)S(1)}, bf16[168,768]{1,0:T(8,128)(2,1)S(1)}, u32[]{:S(2)}, u32[]{:S(2)}) collective-permute-start(bf16[168,768]{1,0:T(8,128)(2,1)S(1)} %get-tuple-element.63), channel_id=1, source_target_pairs={{0,6},{1,3},{2,4},{3,1},{4,2},{5,7},{6,0},{7,5},{8,14},{9,11},{10,... | collective-permute-start | bytes 774152 | tf_op jit(solution)/shard_map/ppermute | solution.py:400
  45.6 2.9 %collective-permute-start.10 = (bf16[168,768]{1,0:T(8,128)(2,1)S(1)}, bf16[168,768]{1,0:T(8,128)(2,1)S(1)}, u32[]{:S(2)}, u32[]{:S(2)}) collective-permute-start(bf16[168,768]{1,0:T(8,128)(2,1)S(1)} %get-tuple-element.64), channel_id=1, source_target_pairs={{0,24},{1,9},{2,26},{3,11},{4,28},{5,13},{6,30},{7,15},{8,16},{9,1... | collective-permute-start | bytes 774152 | tf_op jit(solution)/shard_map/ppermute | solution.py:400
  48.6 1.4 %collective-permute-start.11 = (bf16[168,768]{1,0:T(8,128)(2,1)S(1)}, bf16[168,768]{1,0:T(8,128)(2,1)S(1)}, u32[]{:S(2)}, u32[]{:S(2)}) collective-permute-start(bf16[168,768]{1,0:T(8,128)(2,1)S(1)} %get-tuple-element.65), channel_id=1, source_target_pairs={{0,30},{1,11},{2,28},{3,9},{4,26},{5,15},{6,24},{7,13},{8,22},{9,3... | collective-permute-start | bytes 774152 | tf_op jit(solution)/shard_map/ppermute | solution.py:400
  50.0 1.6 %collective-permute-done.9.refs_1_ = bf16[168,768]{1,0:T(8,128)(2,1)S(1)} collective-permute-done((bf16[168,768]{1,0:T(8,128)(2,1)S(1)}, bf16[168,768]{1,0:T(8,128)(2,1)S(1)}, u32[]{:S(2)}, u32[]{:S(2)}) %collective-permute-start.9) | collective-permute-done | bytes 258080 | tf_op jit(solution)/shard_map/ppermute | solution.py:400
  51.6 3.6 %collective-permute-done.10.refs_2_ = bf16[168,768]{1,0:T(8,128)(2,1)S(1)} collective-permute-done((bf16[168,768]{1,0:T(8,128)(2,1)S(1)}, bf16[168,768]{1,0:T(8,128)(2,1)S(1)}, u32[]{:S(2)}, u32[]{:S(2)}) %collective-permute-start.10) | collective-permute-done | bytes 258080 | tf_op jit(solution)/shard_map/ppermute | solution.py:400
  55.2 3.0 %collective-permute-done.11.refs_3_ = bf16[168,768]{1,0:T(8,128)(2,1)S(1)} collective-permute-done((bf16[168,768]{1,0:T(8,128)(2,1)S(1)}, bf16[168,768]{1,0:T(8,128)(2,1)S(1)}, u32[]{:S(2)}, u32[]{:S(2)}) %collective-permute-start.11) | collective-permute-done | bytes 258080 | tf_op jit(solution)/shard_map/ppermute | solution.py:400
  58.5 5.8 %collective-permute-done.12.came_ref = bf16[104,768]{1,0:T(8,128)(2,1)S(1)} collective-permute-done((bf16[104,768]{1,0:T(8,128)(2,1)S(1)}, bf16[104,768]{1,0:T(8,128)(2,1)S(1)}, u32[]{:S(2)}, u32[]{:S(2)}) %collective-permute-start.12) | collective-permute-done | bytes 159776 | tf_op jit(solution)/shard_map/ppermute | solution.py:406
  64.3 5.4 %collective-permute-start.13 = (bf16[56,768]{1,0:T(8,128)(2,1)S(1)}, bf16[56,768]{1,0:T(8,128)(2,1)S(1)}, u32[]{:S(2)}, u32[]{:S(2)}) collective-permute-start(bf16[56,768]{1,0:T(8,128)(2,1)S(1)} %get-tuple-element.69), channel_id=1, source_target_pairs={{0,64},{32,96},{64,128},{96,160},{128,192},{160,224},{192,0},{224,... | collective-permute-start | bytes 258056 | tf_op jit(solution)/shard_map/ppermute | solution.py:403
  69.7 3.2 %collective-permute-start.14 = (bf16[56,768]{1,0:T(8,128)(2,1)S(1)}, bf16[56,768]{1,0:T(8,128)(2,1)S(1)}, u32[]{:S(2)}, u32[]{:S(2)}) collective-permute-start(bf16[56,768]{1,0:T(8,128)(2,1)S(1)} %get-tuple-element.70), channel_id=1, source_target_pairs={{0,128},{32,160},{64,192},{96,224},{128,0},{160,32},{192,64},{224,... | collective-permute-start | bytes 258056 | tf_op jit(solution)/shard_map/ppermute | solution.py:403
  72.9 4.0 %collective-permute-start.15 = (bf16[56,768]{1,0:T(8,128)(2,1)S(1)}, bf16[56,768]{1,0:T(8,128)(2,1)S(1)}, u32[]{:S(2)}, u32[]{:S(2)}) collective-permute-start(bf16[56,768]{1,0:T(8,128)(2,1)S(1)} %get-tuple-element.71), channel_id=1, source_target_pairs={{0,192},{32,224},{64,0},{96,32},{128,64},{160,96},{192,128},{224,1... | collective-permute-start | bytes 258056 | tf_op jit(solution)/shard_map/ppermute | solution.py:403
  76.9 3.5 %spread.2 = (bf16[512,768]{1,0:T(8,128)(2,1)}, bf16[512,768]{1,0:T(8,128)(2,1)}) custom-call(bf16[512,768]{1,0:T(8,128)(2,1)S(1)} %copy-done, bf16[512,768]{1,0:T(8,128)(2,1)S(1)} %copy-done.1, f32[512,768]{1,0:T(8,128)S(1)} %get-tuple-element.47.lifted_ref, f32[512,768]{1,0:T(8,128)S(1)} %get-tuple-element.44.normed_ref, ...), custom_call_target="tpu_custom_call" | custom-call | flops 243793920 | bytes 3932160 | tf_op jit(solution)/shard_map/spread/pallas_call | solution.py:493
  80.4 3.5 %spread.3 = (bf16[512,768]{1,0:T(8,128)(2,1)}, bf16[512,768]{1,0:T(8,128)(2,1)}) custom-call(bf16[512,768]{1,0:T(8,128)(2,1)S(1)} %copy-done, bf16[512,768]{1,0:T(8,128)(2,1)S(1)} %copy-done.1, f32[512,768]{1,0:T(8,128)S(1)} %get-tuple-element.47.lifted_ref, ...), custom_call_target="tpu_custom_call", output_to_operand_aliasing={{0}: (8, {}), {1}: (9, {})} | custom-call | flops 243793920 | bytes 3932160 | tf_op jit(solution)/shard_map/spread/pallas_call | solution.py:493
  83.9 0.7 shard_map.139
  (28 shorter events, 1.5 us)
Async XLA Ops:
  3.1 1.6 %collective-permute-start = (f32[512,128]{1,0:T(8,128)S(1)}, f32[512,128]{1,0:T(8,128)S(1)}, u32[]{:S(2)}, u32[]{:S(2)}) collective-permute-start(f32[512,128]{1,0:T(8,128)S(1)} %get-tuple-element.43.own_ref), channel_id=1, source_target_pairs={{0,1},{1,0},{2,3},{3,2},{4,5},{5,4},{6,7},{7,6},{8,9},{9,8},{10,11... | collective-permute-start | bytes 786440 | tf_op jit(solution)/shard_map/ppermute | solution.py:409
  3.2 1.5 %copy-start.4 = (f32[768]{0:T(1024)S(1)}, f32[768]{0:T(1024)}, u32[]{:S(2)}) copy-start(f32[768]{0:T(1024)} %gain_ref.3) | copy-start | bytes 9220
  3.2 1.5 %copy-start.5 = (f32[768]{0:T(1024)S(1)}, f32[768]{0:T(1024)}, u32[]{:S(2)}) copy-start(f32[768]{0:T(1024)} %shift_ref.1) | copy-start | bytes 9220
  5.7 5.6 %copy-start.2 = (bf16[2048,768]{1,0:T(8,128)(2,1)S(1)}, bf16[2048,768]{1,0:T(8,128)(2,1)}, u32[]{:S(2)}) copy-start(bf16[2048,768]{1,0:T(8,128)(2,1)} %weight_ref.1) | copy-start | bytes 9437188
  7.7 35.9 %collective-permute-start.3 = (bf16[512,768]{1,0:T(8,128)(2,1)S(1)}, bf16[512,768]{1,0:T(8,128)(2,1)S(1)}, u32[]{:S(2)}, u32[]{:S(2)}) collective-permute-start(bf16[512,768]{1,0:T(8,128)(2,1)S(1)} %get-tuple-element.58), channel_id=1, source_target_pairs={{0,2},{1,7},{2,0},{3,5},{4,6},{5,3},{6,4},{7,1},{8,10},{9,15},{10,... | collective-permute-start | bytes 2359304 | tf_op jit(solution)/shard_map/ppermute | solution.py:400
  9.2 34.3 %collective-permute-start.4 = (bf16[512,768]{1,0:T(8,128)(2,1)S(1)}, bf16[512,768]{1,0:T(8,128)(2,1)S(1)}, u32[]{:S(2)}, u32[]{:S(2)}) collective-permute-start(bf16[512,768]{1,0:T(8,128)(2,1)S(1)} %get-tuple-element.59), channel_id=1, source_target_pairs={{0,8},{1,25},{2,10},{3,27},{4,12},{5,29},{6,14},{7,31},{8,0},{9,17... | collective-permute-start | bytes 2359304 | tf_op jit(solution)/shard_map/ppermute | solution.py:400
  10.8 32.7 %collective-permute-start.5 = (bf16[512,768]{1,0:T(8,128)(2,1)S(1)}, bf16[512,768]{1,0:T(8,128)(2,1)S(1)}, u32[]{:S(2)}, u32[]{:S(2)}) collective-permute-start(bf16[512,768]{1,0:T(8,128)(2,1)S(1)} %get-tuple-element.60), channel_id=1, source_target_pairs={{0,10},{1,31},{2,8},{3,29},{4,14},{5,27},{6,12},{7,25},{8,2},{9,23... | collective-permute-start | bytes 2359304 | tf_op jit(solution)/shard_map/ppermute | solution.py:400
  13.9 15.3 %copy-start = (bf16[512,768]{1,0:T(8,128)(2,1)S(1)}, bf16[512,768]{1,0:T(8,128)(2,1)}, u32[]{:S(2)}) copy-start(bf16[512,768]{1,0:T(8,128)(2,1)} %value_ref.5) | copy-start | bytes 2359300
  13.9 15.3 %copy-start.1 = (bf16[512,768]{1,0:T(8,128)(2,1)S(1)}, bf16[512,768]{1,0:T(8,128)(2,1)}, u32[]{:S(2)}) copy-start(bf16[512,768]{1,0:T(8,128)(2,1)} %gate_ref.5) | copy-start | bytes 2359300
  13.9 3.3 %collective-permute-start.1 = (f32[512,128]{1,0:T(8,128)S(1)}, f32[512,128]{1,0:T(8,128)S(1)}, u32[]{:S(2)}, u32[]{:S(2)}) collective-permute-start(f32[512,128]{1,0:T(8,128)S(1)} %get-tuple-element.48.sums_ref), channel_id=1, source_target_pairs={{0,1},{1,0},{2,3},{3,2},{4,5},{5,4},{6,7},{7,6},{8,9},{9,8},{10,11... | collective-permute-start | bytes 786440 | tf_op jit(solution)/shard_map/ppermute | solution.py:409
  17.4 11.9 %collective-permute-start.2 = (bf16[32,768]{1,0:T(8,128)(2,1)S(1)}, bf16[32,768]{1,0:T(8,128)(2,1)S(1)}, u32[]{:S(2)}, u32[]{:S(2)}) collective-permute-start(bf16[32,768]{1,0:T(8,128)(2,1)S(1)} %get-tuple-element.51), channel_id=1, source_target_pairs={{2,0},{4,2},{6,4},{8,6},{10,8},{12,10},{14,12},{16,14},{18,16},{20... | collective-permute-start | bytes 147464 | tf_op jit(solution)/shard_map/ppermute | solution.py:412
  34.0 5.3 %collective-permute-start.8 = (bf16[40,768]{1,0:T(8,128)(2,1)S(1)}, bf16[40,768]{1,0:T(8,128)(2,1)S(1)}, u32[]{:S(2)}, u32[]{:S(2)}) collective-permute-start(bf16[40,768]{1,0:T(8,128)(2,1)S(1)} %shard_map.135.refs_4_), channel_id=1, source_target_pairs={{0,10},{1,31},{2,8},{3,29},{4,14},{5,27},{6,12},{7,25},{8,2},{9,23... | collective-permute-start | bytes 184328 | tf_op jit(solution)/shard_map/ppermute | solution.py:400
  34.7 4.9 %collective-permute-start.7 = (bf16[40,768]{1,0:T(8,128)(2,1)S(1)}, bf16[40,768]{1,0:T(8,128)(2,1)S(1)}, u32[]{:S(2)}, u32[]{:S(2)}) collective-permute-start(bf16[40,768]{1,0:T(8,128)(2,1)S(1)} %shard_map.135.refs_4_), channel_id=1, source_target_pairs={{0,8},{1,25},{2,10},{3,27},{4,12},{5,29},{6,14},{7,31},{8,0},{9,17... | collective-permute-start | bytes 184328 | tf_op jit(solution)/shard_map/ppermute | solution.py:400
  39.3 4.2 %collective-permute-start.6 = (bf16[40,768]{1,0:T(8,128)(2,1)S(1)}, bf16[40,768]{1,0:T(8,128)(2,1)S(1)}, u32[]{:S(2)}, u32[]{:S(2)}) collective-permute-start(bf16[40,768]{1,0:T(8,128)(2,1)S(1)} %shard_map.135.refs_4_), channel_id=1, source_target_pairs={{0,2},{1,7},{2,0},{3,5},{4,6},{5,3},{6,4},{7,1},{8,10},{9,15},{10,... | collective-permute-start | bytes 184328 | tf_op jit(solution)/shard_map/ppermute | solution.py:400
  43.6 33.4 %copy-start.3 = (bf16[31,768]{1,0:T(8,128)(2,1)S(1)}, bf16[31,768]{1,0:T(8,128)(2,1)}, u32[]{:S(2)}) copy-start(bf16[31,768]{1,0:T(8,128)(2,1)} %taps_ref.3) | copy-start | bytes 142852
  44.0 7.6 %collective-permute-start.9 = (bf16[168,768]{1,0:T(8,128)(2,1)S(1)}, bf16[168,768]{1,0:T(8,128)(2,1)S(1)}, u32[]{:S(2)}, u32[]{:S(2)}) collective-permute-start(bf16[168,768]{1,0:T(8,128)(2,1)S(1)} %get-tuple-element.63), channel_id=1, source_target_pairs={{0,6},{1,3},{2,4},{3,1},{4,2},{5,7},{6,0},{7,5},{8,14},{9,11},{10,... | collective-permute-start | bytes 774152 | tf_op jit(solution)/shard_map/ppermute | solution.py:400
  45.6 9.6 %collective-permute-start.10 = (bf16[168,768]{1,0:T(8,128)(2,1)S(1)}, bf16[168,768]{1,0:T(8,128)(2,1)S(1)}, u32[]{:S(2)}, u32[]{:S(2)}) collective-permute-start(bf16[168,768]{1,0:T(8,128)(2,1)S(1)} %get-tuple-element.64), channel_id=1, source_target_pairs={{0,24},{1,9},{2,26},{3,11},{4,28},{5,13},{6,30},{7,15},{8,16},{9,1... | collective-permute-start | bytes 774152 | tf_op jit(solution)/shard_map/ppermute | solution.py:400
  48.6 9.6 %collective-permute-start.11 = (bf16[168,768]{1,0:T(8,128)(2,1)S(1)}, bf16[168,768]{1,0:T(8,128)(2,1)S(1)}, u32[]{:S(2)}, u32[]{:S(2)}) collective-permute-start(bf16[168,768]{1,0:T(8,128)(2,1)S(1)} %get-tuple-element.65), channel_id=1, source_target_pairs={{0,30},{1,11},{2,28},{3,9},{4,26},{5,15},{6,24},{7,13},{8,22},{9,3... | collective-permute-start | bytes 774152 | tf_op jit(solution)/shard_map/ppermute | solution.py:400
  58.3 5.9 %collective-permute-start.12 = (bf16[104,768]{1,0:T(8,128)(2,1)S(1)}, bf16[104,768]{1,0:T(8,128)(2,1)S(1)}, u32[]{:S(2)}, u32[]{:S(2)}) collective-permute-start(bf16[104,768]{1,0:T(8,128)(2,1)S(1)} %get-tuple-element.67.sent_ref), channel_id=1, source_target_pairs={{0,32},{32,0},{64,96},{96,64},{128,160},{160,128},{192,224},{224,1... | collective-permute-start | bytes 479240 | tf_op jit(solution)/shard_map/ppermute | solution.py:406
  64.3 19.6 %collective-permute-start.13 = (bf16[56,768]{1,0:T(8,128)(2,1)S(1)}, bf16[56,768]{1,0:T(8,128)(2,1)S(1)}, u32[]{:S(2)}, u32[]{:S(2)}) collective-permute-start(bf16[56,768]{1,0:T(8,128)(2,1)S(1)} %get-tuple-element.69), channel_id=1, source_target_pairs={{0,64},{32,96},{64,128},{96,160},{128,192},{160,224},{192,0},{224,... | collective-permute-start | bytes 258056 | tf_op jit(solution)/shard_map/ppermute | solution.py:403
  69.7 14.2 %collective-permute-start.14 = (bf16[56,768]{1,0:T(8,128)(2,1)S(1)}, bf16[56,768]{1,0:T(8,128)(2,1)S(1)}, u32[]{:S(2)}, u32[]{:S(2)}) collective-permute-start(bf16[56,768]{1,0:T(8,128)(2,1)S(1)} %get-tuple-element.70), channel_id=1, source_target_pairs={{0,128},{32,160},{64,192},{96,224},{128,0},{160,32},{192,64},{224,... | collective-permute-start | bytes 258056 | tf_op jit(solution)/shard_map/ppermute | solution.py:403
  72.9 11.0 %collective-permute-start.15 = (bf16[56,768]{1,0:T(8,128)(2,1)S(1)}, bf16[56,768]{1,0:T(8,128)(2,1)S(1)}, u32[]{:S(2)}, u32[]{:S(2)}) collective-permute-start(bf16[56,768]{1,0:T(8,128)(2,1)S(1)} %get-tuple-element.71), channel_id=1, source_target_pairs={{0,192},{32,224},{64,0},{96,32},{128,64},{160,96},{192,128},{224,1... | collective-permute-start | bytes 258056 | tf_op jit(solution)/shard_map/ppermute | solution.py:403
